TPU v7x, 32 devices: a whole 2x2x4 slice. The times are simulated.
32 devices in a mesh: sp: 16 (over z, y, x), tp: 2 (over core).
Axes of the slice: x: 2, y: 2, z: 4, core: 2. Of those that a mesh axis runs over, the one named last changes fastest.
Arguments:
- tokens: bfloat16 [2048, 2048], P('sp', 'tp'), may hold values from -6 to 6
- norm_gain: float32 [2048], replicated, may hold values from 0.1 to 1.9
- w_value: bfloat16 [2048, 2048], P('sp', 'tp'), may hold values from -0.125 to 0.125
- w_gate: bfloat16 [2048, 2048], P('sp', 'tp'), may hold values from -0.125 to 0.125
- conv_taps: bfloat16 [31, 2048], P(None, 'tp'), may hold values from -1 to 1
- conv_gain: float32 [2048], P('tp'), may hold values from 0.1 to 1.9
- w_query: bfloat16 [2048, 3072], P(None, 'tp'), may hold values from -5.303301 to 5.303301
- latent_down_weight: bfloat16 [2048, 512], P('sp'), may hold values from -0.125 to 0.125
- latent_norm_gain: float32 [512], replicated, may hold values from 0.1 to 1.9
- w_rope_key: bfloat16 [2048, 64], P('sp'), may hold values from -0.125 to 0.125
- key_up_weight: bfloat16 [512, 2048], P(None, 'tp'), may hold values from -0.5 to 0.5
- value_up_weight: bfloat16 [512, 2048], P(None, 'tp'), may hold values from -0.25 to 0.25
- w_merge_conv: bfloat16 [2048, 2048], P('tp'), may hold values from -0.09375 to 0.09375
- w_merge_attn: bfloat16 [2048, 2048], P('tp'), may hold values from -0.28125 to 0.28125
Outputs:
- merged: bfloat16 [2048, 2048], P(('sp', 'tp'))
- log_sums: float32 [2048, 16], P('sp', 'tp')
All inputs are finite; a program needn't handle non-finite values.
Results may differ from a plain program's by a relative error of at most 0.025.
The roundings to bfloat16 on the way count: a program that leaves them out, or rounds other values in their place, can miss the bound.
Values may be sent and summed in bfloat16 or wider, within the bound.
No kernel may reach another device: no remote copies, remote signals or barrier semaphores. Data moves between devices by JAX's collectives and lax.ppermute only.
A program may use at most 64 MiB of HBM per device.

v0:
```python
import functools
import math

import jax
import jax.numpy as jnp
from jax import lax
from jax.experimental import pallas as pl
from jax.experimental.pallas import tpu as pltpu
from jax.sharding import PartitionSpec as P


PLAIN_QK_WIDTH = 128
QK_ROPE = 64
VALUE_HEAD_WIDTH = 128


epsilon = 1e-06
rope_base = 10000.0
masked_score = -1e30


def angles_at(positions, width):
    inverse = rope_base ** (-2.0 * jnp.arange(width // 2, dtype=jnp.float32) / width)
    return positions[:, None] * inverse[None, :]


class Place:
    def __init__(self):
        self.sp_count = lax.axis_size("sp")
        self.tp_count = lax.axis_size("tp")
        self.inner = math.gcd(self.sp_count, 4)
        self.outer = self.sp_count // self.inner

    def indices(self):
        index = lax.axis_index("sp")
        return index // self.inner, index % self.inner, lax.axis_index("tp")

    def outer_swap(self, block, mask):
        mask = mask * self.inner
        return lax.ppermute(block, "sp", [(i, i ^ mask) for i in range(self.sp_count)])

    def inner_swap(self, block, mask):
        return lax.ppermute(block, "sp", [(i, i ^ mask) for i in range(self.sp_count)])

    def tp_shift(self, block, distance):
        route = [(i, (i + distance) % self.tp_count) for i in range(self.tp_count)]
        return lax.ppermute(block, "tp", route)

    def outer_gather(self, block):
        return [block] + [self.outer_swap(block, j) for j in range(1, self.outer)]

    def inner_gather(self, block):
        return [block] + [self.inner_swap(block, k) for k in range(1, self.inner)]

    def tp_gather(self, blocks):
        return [blocks] + [
            [self.tp_shift(b, t) for b in blocks] for t in range(1, self.tp_count)
        ]


def behind(index, distance, count):
    return lax.rem(index - distance + count, count)


def untangled(blocks, index):
    bit = 1
    while bit < len(blocks):
        flag = (index & bit) > 0
        blocks = [jnp.where(flag, blocks[i ^ bit], b) for i, b in enumerate(blocks)]
        bit *= 2
    return blocks


def copy_all(pairs, sem):
    copies = [pltpu.make_async_copy(s, d, sem.at[n]) for n, (s, d) in enumerate(pairs)]
    for c in copies:
        c.start()
    return copies


def any_specs(n):
    return [pl.BlockSpec(memory_space=pl.ANY)] * n


def whole_vmem():
    return pl.BlockSpec(memory_space=pltpu.VMEM)


def turned(first, second, cosine, sine):
    return jnp.concatenate(
        [first * cosine - second * sine, first * sine + second * cosine], axis=-1
    ).astype(jnp.bfloat16)


def query_kernel(rank, normed_ref, w_ref, up_ref, cos_ref, sin_ref, out_ref, w, up, sem):
    heads, count, _ = out_ref.shape
    plain, half = PLAIN_QK_WIDTH, QK_ROPE // 2
    head = plain + QK_ROPE
    span = 2 * head
    pairs = heads // 2
    copies = copy_all(
        [
            (w_ref.at[:, p * span : (p + 1) * span], w.at[:, p * span : (p + 1) * span])
            for p in range(pairs)
        ]
        + [(up_ref, up)],
        sem,
    )
    cosine, sine = cos_ref[:count], sin_ref[:count]
    for p in range(pairs):
        copies[p].wait()
        query = jnp.dot(
            normed_ref[...], w[:, p * span : (p + 1) * span], preferred_element_type=jnp.float32
        ).astype(jnp.bfloat16)
        if p == 0:
            copies[pairs].wait()
        for i in range(2):
            h = 2 * p + i
            own = query[:, i * head : (i + 1) * head]
            out_ref[h, :, :rank] = lax.dot_general(
                own[:, :plain],
                up[:, h * plain : (h + 1) * plain],
                (((1,), (1,)), ((), ())),
                preferred_element_type=jnp.float32,
            ).astype(jnp.bfloat16)
            rope = own[:, plain:].astype(jnp.float32)
            out_ref[h, :, rank:] = turned(rope[:, :half], rope[:, half:], cosine, sine)


def latent_kernel(place, rank, share, *refs):
    outer, inner, tp = place.outer, place.inner, place.tp_count
    tables = tp if share else 1
    n_rows, n_w = outer, tables * inner
    row_refs, w_refs = refs[:n_rows], refs[n_rows : n_rows + n_w]
    gain_ref, cos_ref, sin_ref, out_ref, rows, weight, sem_r, sem_w = refs[n_rows + n_w :]
    zi, xi, ti = place.indices()
    piece = w_refs[0].shape[1]
    block = piece * tables
    count = row_refs[0].shape[0]
    pairs = []
    for t in range(tables):
        owner = behind(ti, t, tp) if share else 0
        for k in range(inner):
            for j in range(outer):
                start = ((zi ^ j) * inner + (xi ^ k)) * block + owner * piece
                pairs.append(
                    (
                        w_refs[t * inner + k].at[j],
                        weight.at[pl.ds(pl.multiple_of(start, piece), piece)],
                    )
                )
    w_copies = copy_all(pairs, sem_w)
    r_copies = copy_all(
        [(row_refs[j], rows.at[pl.ds(j * count, count)]) for j in range(outer)], sem_r
    )
    for c in w_copies + r_copies:
        c.wait()
    pre = jnp.dot(rows[...], weight[...], preferred_element_type=jnp.float32)
    plain = pre[:, :rank]
    scale = lax.rsqrt(jnp.mean(plain * plain, axis=-1, keepdims=True) + epsilon)
    out_ref[:, :rank] = (plain * scale * gain_ref[...]).astype(jnp.bfloat16)
    rope = pre[:, rank:]
    half = rope.shape[1] // 2
    total = outer * count
    cosine, sine = cos_ref[cos_ref.shape[0] - total :], sin_ref[sin_ref.shape[0] - total :]
    out_ref[:, rank:] = turned(rope[:, :half], rope[:, half:], cosine, sine)


def gated_kernel(place, *refs):
    outer, inner, tp = place.outer, place.inner, place.tp_count
    n_rows = tp * outer
    row_refs, w_refs = refs[:n_rows], refs[n_rows : n_rows + inner]
    outs = refs[n_rows + inner : n_rows + inner + outer]
    rows, weight, sem_r, sem_w = refs[n_rows + inner + outer :]
    zi, xi, ti = place.indices()
    block = w_refs[0].shape[1]
    count = row_refs[0].shape[0]
    pairs = []
    for k in range(inner):
        for j in range(outer):
            start = ((zi ^ j) * inner + (xi ^ k)) * block
            pairs.append(
                (w_refs[k].at[j], weight.at[pl.ds(pl.multiple_of(start, block), block)])
            )
    w_copies = copy_all(pairs, sem_w)
    pairs = []
    for t in range(tp):
        owner = behind(ti, t, tp)
        for j in range(outer):
            start = j * tp * count + owner * count
            pairs.append(
                (
                    row_refs[t * outer + j],
                    rows.at[pl.ds(pl.multiple_of(start, count), count)],
                )
            )
    r_copies = copy_all(pairs, sem_r)
    for c in w_copies + r_copies:
        c.wait()
    chunk = tp * count
    width = outs[0].shape[1]
    for j in range(outer):
        pre = jnp.dot(
            rows[pl.ds(j * chunk, chunk)], weight[...], preferred_element_type=jnp.float32
        )
        value, gate = pre[:, :width], pre[:, width:]
        outs[j][...] = (value * jax.nn.sigmoid(gate)).astype(jnp.bfloat16)


def attention_kernel(place, scale, rank, q_ref, up_ref, *refs):
    outer, inner, tp = place.outer, place.inner, place.tp_count
    n_k = tp * inner
    key_refs = refs[:n_k]
    out_ref, lse_ref, keys, sem = refs[n_k:]
    zi, xi, ti = place.indices()
    heads, count, depth = q_ref.shape
    piece = key_refs[0].shape[0]
    share = piece // outer
    copies = copy_all(
        [(key_refs[n], keys.at[pl.ds(n * piece, piece)]) for n in range(n_k)], sem
    )
    lane = lax.broadcasted_iota(jnp.int32, (1, piece), 1)
    back = zi ^ lax.shift_right_logical(lane, share.bit_length() - 1)
    within = jnp.bitwise_and(lane, share - 1)
    parts = []
    for t in range(tp):
        owner = behind(ti, t, tp)
        for k in range(inner):
            parts.append((back * inner + (xi ^ k)) * count + owner * share + within)
    key_index = jnp.concatenate(parts, axis=1)
    first_row = (zi * inner + xi) * count
    together = math.gcd(heads, 4)
    size = together * count
    query_index = lax.broadcasted_iota(jnp.int32, (count, 1), 0) + first_row
    allowed = key_index <= jnp.concatenate([query_index] * together, axis=0)
    width = VALUE_HEAD_WIDTH
    sums = []
    for c in copies:
        c.wait()
    for g in range(heads // together):
        queries = q_ref[g * together : (g + 1) * together].reshape(size, depth)
        scores = lax.dot_general(
            queries, keys[...], (((1,), (1,)), ((), ())), preferred_element_type=jnp.float32
        )
        scores = jnp.where(allowed, scores, masked_score)
        top = jnp.max(scores, axis=-1, keepdims=True)
        weights = jnp.exp2((scores - top) * (scale * math.log2(math.e)))
        total = jnp.sum(weights, axis=-1, keepdims=True)
        weighted = jnp.dot(
            weights.astype(jnp.bfloat16), keys[:, :rank], preferred_element_type=jnp.float32
        )
        latent_out = (weighted / total).astype(jnp.bfloat16)
        group_sums = top * scale + jnp.log(total)
        for i in range(together):
            h = g * together + i
            part = slice(i * count, (i + 1) * count)
            sums.append(group_sums[part])
            out_ref[:, h * width : (h + 1) * width] = jnp.dot(
                latent_out[part],
                up_ref[:, h * width : (h + 1) * width],
                preferred_element_type=jnp.float32,
            ).astype(jnp.bfloat16)
    spare = [jnp.zeros((count, 128 - heads), jnp.float32)]
    lse_ref[...] = jnp.concatenate(sums + spare, axis=1).T[:heads]


def local(
    tokens,
    norm_gain,
    w_value,
    w_gate,
    conv_taps,
    conv_gain,
    w_query,
    latent_down_weight,
    latent_norm_gain,
    w_rope_key,
    key_up_weight,
    value_up_weight,
    w_merge_conv,
    w_merge_attn,
):
    place = Place()
    outer, inner, tp_count = place.outer, place.inner, place.tp_count
    zi, xi, ti = place.indices()
    row_count = tokens.shape[0]
    share = row_count // tp_count
    depth = latent_down_weight.shape[0]
    rank = latent_down_weight.shape[1]

    split_rows = depth % (16 * tp_count) == 0
    own_table = jnp.concatenate([latent_down_weight, w_rope_key], axis=1)
    if split_rows:
        piece = depth // tp_count
        own_table = lax.dynamic_slice_in_dim(own_table, ti * piece, piece, 0)
    own_table, w_value, w_gate = lax.optimization_barrier((own_table, w_value, w_gate))
    table_parts = place.outer_gather(own_table)

    width = w_value.shape[1] // outer
    columns = []
    for j in range(outer):
        start = (zi ^ j) * width
        block = jnp.concatenate(
            [
                lax.dynamic_slice_in_dim(w_value, start, width, 1),
                lax.dynamic_slice_in_dim(w_gate, start, width, 1),
            ],
            axis=1,
        )
        columns.append(block if j == 0 else place.outer_swap(block, j))

    table = jnp.stack(table_parts)
    table, tokens = lax.optimization_barrier((table, tokens))
    tables = place.inner_gather(table)

    gathered = lax.all_gather(tokens, "tp", axis=1, tiled=True)
    features = gathered.astype(jnp.float32)
    normed = (
        features
        * lax.rsqrt(jnp.mean(features * features, axis=-1, keepdims=True) + epsilon)
        * norm_gain
    ).astype(jnp.bfloat16)

    own_rows = lax.dynamic_slice_in_dim(normed, ti * share, share, 0)
    rows = place.outer_gather(own_rows)
    weight_block = jnp.stack(columns)
    weight_block, query_rows = lax.optimization_barrier((weight_block, normed))
    weight_blocks = place.inner_gather(weight_block)

    bf16 = jnp.bfloat16
    model = normed.shape[1]
    head_count = key_up_weight.shape[1] // PLAIN_QK_WIDTH
    query_index = lax.axis_index("sp") * row_count + jnp.arange(row_count, dtype=jnp.int32)
    back = zi ^ jnp.arange(outer, dtype=jnp.int32)
    key_index = (
        ((back * inner + xi) * row_count + ti * share)[:, None]
        + jnp.arange(share, dtype=jnp.int32)[None, :]
    ).reshape(-1)
    angles = angles_at(
        jnp.concatenate([query_index, key_index]).astype(jnp.float32), QK_ROPE
    )
    cosine, sine = jnp.cos(angles), jnp.sin(angles)

    query_width = w_query.shape[1]
    queries = pl.pallas_call(
        functools.partial(query_kernel, rank),
        out_shape=jax.ShapeDtypeStruct((head_count, row_count, rank + QK_ROPE), bf16),
        in_specs=[whole_vmem()] + [pl.BlockSpec(memory_space=pltpu.HBM)] * 2 + [whole_vmem()] * 2,
        out_specs=whole_vmem(),
        scratch_shapes=[
            pltpu.VMEM((model, query_width), bf16),
            pltpu.VMEM(key_up_weight.shape, bf16),
            pltpu.SemaphoreType.DMA((head_count // 2 + 1,)),
        ],
        compiler_params=pltpu.CompilerParams(vmem_limit_bytes=52 << 20),
        cost_estimate=pl.CostEstimate(
            flops=2 * row_count * model * query_width,
            bytes_accessed=2 * model * query_width,
            transcendentals=0,
        ),
        name="queries",
    )(query_rows, w_query, key_up_weight, cosine, sine)

    rows, tables, _ = lax.optimization_barrier((rows, tables, queries))
    if split_rows:
        tables = sum(place.tp_gather(tables), [])

    latent = pl.pallas_call(
        functools.partial(latent_kernel, place, rank, split_rows),
        out_shape=jax.ShapeDtypeStruct((outer * share, rank + QK_ROPE), bf16),
        in_specs=any_specs(outer + len(tables)) + [whole_vmem()] * 3,
        out_specs=whole_vmem(),
        scratch_shapes=[
            pltpu.VMEM((outer * share, model), bf16),
            pltpu.VMEM((model, rank + QK_ROPE), bf16),
            pltpu.SemaphoreType.DMA((outer,)),
            pltpu.SemaphoreType.DMA((len(tables) * outer,)),
        ],
        compiler_params=pltpu.CompilerParams(vmem_limit_bytes=16 << 20),
        cost_estimate=pl.CostEstimate(
            flops=2 * outer * share * model * (rank + QK_ROPE),
            bytes_accessed=2 * model * (rank + QK_ROPE + outer * share),
            transcendentals=0,
        ),
        name="latents",
    )(*rows, *tables, latent_norm_gain[None, :], cosine, sine)
    _, *weight_blocks = lax.optimization_barrier((latent, *weight_blocks))
    latents = place.inner_gather(latent)
    latents = sum(place.tp_gather(latents), [])

    all_rows = sum(place.tp_gather(rows), [])
    gated = pl.pallas_call(
        functools.partial(gated_kernel, place),
        out_shape=[jax.ShapeDtypeStruct((row_count, width), bf16)] * outer,
        in_specs=any_specs(len(all_rows) + inner),
        out_specs=[whole_vmem()] * outer,
        scratch_shapes=[
            pltpu.VMEM((outer * row_count, model), bf16),
            pltpu.VMEM((model, 2 * width), bf16),
            pltpu.SemaphoreType.DMA((len(all_rows),)),
            pltpu.SemaphoreType.DMA((inner * outer,)),
        ],
        compiler_params=pltpu.CompilerParams(vmem_limit_bytes=24 << 20),
        cost_estimate=pl.CostEstimate(
            flops=4 * outer * row_count * model * width,
            bytes_accessed=2 * model * (2 * width + outer * row_count),
            transcendentals=outer * row_count * width,
        ),
        name="gated",
    )(*all_rows, *weight_blocks)
    home = [gated[0]] + [place.outer_swap(gated[j], j) for j in range(1, outer)]
    gated_rows = jnp.concatenate(untangled(home, zi), axis=1)

    conv_reach = conv_taps.shape[0] - 1
    prior_rows = lax.ppermute(
        gated_rows[row_count - conv_reach :],
        "sp",
        [(i, i + 1) for i in range(place.sp_count - 1)],
    )
    padded = jnp.concatenate([prior_rows, gated_rows], axis=0).astype(jnp.float32)
    mixed = jnp.zeros(gated_rows.shape, jnp.float32)
    for tap_index in range(conv_taps.shape[0]):
        mixed = (
            mixed
            + conv_taps[tap_index].astype(jnp.float32) * padded[tap_index : tap_index + row_count]
        )
    channel_total = mixed.shape[1] * tp_count
    stats = jnp.stack([jnp.sum(mixed, axis=1), jnp.sum(mixed * mixed, axis=1)])
    stat_sum, stat_squares = sum(
        [place.tp_shift(stats, t) for t in range(1, tp_count)], start=stats
    )
    channel_mean = stat_sum / channel_total
    channel_var = stat_squares / channel_total - channel_mean * channel_mean
    conv_out = jax.nn.silu(
        (mixed - channel_mean[:, None]) * lax.rsqrt(channel_var + epsilon)[:, None] * conv_gain
    ).astype(bf16)

    score_scale = (PLAIN_QK_WIDTH + QK_ROPE) ** (-0.5)
    key_total = place.sp_count * row_count
    attention, log_sums = pl.pallas_call(
        functools.partial(attention_kernel, place, score_scale, rank),
        out_shape=[
            jax.ShapeDtypeStruct((row_count, head_count * VALUE_HEAD_WIDTH), bf16),
            jax.ShapeDtypeStruct((head_count, row_count), jnp.float32),
        ],
        in_specs=[whole_vmem()] * 2 + any_specs(len(latents)),
        out_specs=[whole_vmem()] * 2,
        scratch_shapes=[
            pltpu.VMEM((key_total, rank + QK_ROPE), bf16),
            pltpu.SemaphoreType.DMA((len(latents),)),
        ],
        compiler_params=pltpu.CompilerParams(vmem_limit_bytes=40 << 20),
        cost_estimate=pl.CostEstimate(
            flops=2 * row_count * head_count * key_total * (2 * rank + QK_ROPE),
            bytes_accessed=2 * key_total * (rank + QK_ROPE),
            transcendentals=row_count * head_count * key_total,
        ),
        name="attention",
    )(queries, value_up_weight, *latents)

    partial = (
        jnp.dot(conv_out, w_merge_conv, preferred_element_type=jnp.float32)
        + jnp.dot(attention, w_merge_attn, preferred_element_type=jnp.float32)
    ).astype(bf16)
    merged = lax.dynamic_slice_in_dim(partial, ti * share, share, 0).astype(jnp.float32)
    for t in range(1, tp_count):
        away = lax.dynamic_slice_in_dim(partial, lax.rem(ti + t, tp_count) * share, share, 0)
        merged = merged + place.tp_shift(away, t).astype(jnp.float32)
    return (merged.astype(bf16), log_sums.T)


def solution(mesh):
    return jax.shard_map(
        local,
        mesh=mesh,
        in_specs=(
            P("sp", "tp"),
            P(),
            P("sp", "tp"),
            P("sp", "tp"),
            P(None, "tp"),
            P("tp"),
            P(None, "tp"),
            P("sp", None),
            P(),
            P("sp", None),
            P(None, "tp"),
            P(None, "tp"),
            P("tp", None),
            P("tp", None),
        ),
        out_specs=(P(("sp", "tp"), None), P("sp", "tp")),
        check_vma=False,
    )
```

profile of v0, /device:TPU:0, one launch (start us, length us, event | category | flops | bytes accessed | tf_op | source)
XLA Modules:
  0.0 134.3 jit_solution(8114907193074522735)
XLA Ops:
  2.4 3.1 %collective-permute-start = (bf16[64,576]{1,0:T(8,128)(2,1)S(1)}, bf16[64,576]{1,0:T(8,128)(2,1)S(1)}, u32[]{:S(2)}, u32[]{:S(2)}) collective-permute-start(bf16[64,576]{1,0:T(8,128)(2,1)S(1)} %fusion.39), channel_id=1, source_target_pairs={{0,8},{2,10},{4,12},{6,14},{8,0},{10,2},{12,4},{14,6},{16,24},{18,... | collective-permute-start | bytes 221192 | tf_op jit(solution)/shard_map/ppermute | solution.py:40
  5.5 2.6 %collective-permute-start.1 = (bf16[64,576]{1,0:T(8,128)(2,1)S(1)}, bf16[64,576]{1,0:T(8,128)(2,1)S(1)}, u32[]{:S(2)}, u32[]{:S(2)}) collective-permute-start(bf16[64,576]{1,0:T(8,128)(2,1)S(1)} %fusion.39), channel_id=1, source_target_pairs={{0,16},{2,18},{4,20},{6,22},{8,24},{10,26},{12,28},{14,30},{16,0},... | collective-permute-start | bytes 221192 | tf_op jit(solution)/shard_map/ppermute | solution.py:40
  10.2 3.6 %collective-permute-start.10 = (bf16[128,512]{1,0:T(8,128)(2,1)S(1)}, bf16[128,512]{1,0:T(8,128)(2,1)S(1)}, u32[]{:S(2)}, u32[]{:S(2)}) collective-permute-start(bf16[128,512]{1,0:T(8,128)(2,1)S(1)} %pad_maximum_fusion.3), channel_id=1, source_target_pairs={{0,16},{2,18},{4,20},{6,22},{8,24},{10,26},{12,28},{14,30},{16,0},... | collective-permute-start | bytes 393224 | tf_op jit(solution)/shard_map/ppermute | solution.py:40
  15.3 2.4 %all_gather.3 = bf16[128,2048]{1,0:T(8,128)(2,1)S(1)} all-gather(bf16[128,1024]{1,0:T(8,128)(2,1)} %param.14), channel_id=1, replica_groups=mesh['sp'=16,'tp'=2] {'tp'}, dimensions={1}, use_global_device_ids=true | all-gather | bytes 786432 | tf_op jit(solution)/shard_map/all_gather | solution.py:316
  18.1 6.7 %collective-permute-start.3 = (bf16[64,2048]{1,0:T(8,128)(2,1)S(1)}, bf16[64,2048]{1,0:T(8,128)(2,1)S(1)}, u32[]{:S(2)}, u32[]{:S(2)}) collective-permute-start(bf16[64,2048]{1,0:T(8,128)(2,1)S(1)} %constant_dynamic-slice_fusion.9.refs_0_), channel_id=1, source_target_pairs={{0,8},{2,10},{4,12},{6,14},{8,0},{10,2},{12,4},{14,6},{16,24},{18,... | collective-permute-start | bytes 786440 | tf_op jit(solution)/shard_map/ppermute | solution.py:40
  24.8 2.1 %collective-permute-start.4 = (bf16[64,2048]{1,0:T(8,128)(2,1)S(1)}, bf16[64,2048]{1,0:T(8,128)(2,1)S(1)}, u32[]{:S(2)}, u32[]{:S(2)}) collective-permute-start(bf16[64,2048]{1,0:T(8,128)(2,1)S(1)} %constant_dynamic-slice_fusion.9.refs_0_), channel_id=1, source_target_pairs={{0,16},{2,18},{4,20},{6,22},{8,24},{10,26},{12,28},{14,30},{16,0},... | collective-permute-start | bytes 786440 | tf_op jit(solution)/shard_map/ppermute | solution.py:40
  31.5 5.5 %collective-permute-done.3.refs_1_ = bf16[64,2048]{1,0:T(8,128)(2,1)S(1)} collective-permute-done((bf16[64,2048]{1,0:T(8,128)(2,1)S(1)}, bf16[64,2048]{1,0:T(8,128)(2,1)S(1)}, u32[]{:S(2)}, u32[]{:S(2)}) %collective-permute-start.3) | collective-permute-done | bytes 262176 | tf_op jit(solution)/shard_map/ppermute | solution.py:40
  38.4 7.7 %collective-permute-done.4.refs_2_ = bf16[64,2048]{1,0:T(8,128)(2,1)S(1)} collective-permute-done((bf16[64,2048]{1,0:T(8,128)(2,1)S(1)}, bf16[64,2048]{1,0:T(8,128)(2,1)S(1)}, u32[]{:S(2)}, u32[]{:S(2)}) %collective-permute-start.4) | collective-permute-done | bytes 262176 | tf_op jit(solution)/shard_map/ppermute | solution.py:40
  49.8 5.5 %queries.1.q_ref = bf16[8,128,576]{2,1,0:T(8,128)(2,1)} custom-call(bf16[128,2048]{1,0:T(8,128)(2,1)S(1)} %fusion.3.normed_ref, bf16[2048,1536]{1,0:T(8,128)(2,1)} %w_ref.1, bf16[512,1024]{1,0:T(8,128)(2,1)S(1)} %copy-done.1, f32[384,32]{1,0:T(8,128)S(1)} %get-tuple-element.99.cos_ref.refs_13_, f32[384,32]{1,0:T(8,128)S(1)} %get-tuple-element.98.sin_ref.refs_14_), custom_call_target="tpu_custom_call" | custom-call | flops 805306368 | bytes 6291456 | tf_op jit(solution)/shard_map/queries/pallas_call | solution.py:345
  55.4 4.3 %collective-permute-done.7.refs_6_ = bf16[4,64,576]{2,1,0:T(8,128)(2,1)S(1)} collective-permute-done((bf16[4,64,576]{2,1,0:T(8,128)(2,1)S(1)}, bf16[4,64,576]{2,1,0:T(8,128)(2,1)S(1)}, u32[]{:S(2)}, u32[]{:S(2)}) %collective-permute-start.7) | collective-permute-done | bytes 294944 | tf_op jit(solution)/shard_map/ppermute | solution.py:43
  60.7 2.1 %collective-permute-start.22 = (bf16[4,128,512]{2,1,0:T(8,128)(2,1)S(1)}, bf16[4,128,512]{2,1,0:T(8,128)(2,1)S(1)}, u32[]{:S(2)}, u32[]{:S(2)}) collective-permute-start(bf16[4,128,512]{2,1,0:T(8,128)(2,1)S(1)} %pad_maximum_fusion.refs_8_), channel_id=1, source_target_pairs={{0,6},{2,4},{4,2},{6,0},{8,14},{10,12},{12,10},{14,8},{16,22},{18,... | collective-permute-start | bytes 1572872 | tf_op jit(solution)/shard_map/ppermute | solution.py:43
  63.9 5.7 %latents.1.refs_0_ = bf16[256,576]{1,0:T(8,128)(2,1)S(1)} custom-call(bf16[64,2048]{1,0:T(8,128)(2,1)S(1)} %constant_dynamic-slice_fusion.9.refs_0_, bf16[64,2048]{1,0:T(8,128)(2,1)S(1)} %collective-permute-done.3.refs_1_, bf16[64,2048]{1,0:T(8,128)(2,1)S(1)} %collective-permute-done.4.refs_2_, bf16[64,2048]{1,0:T(8,128)(2,1)S(1)} %collective-permute-done.5.refs_3_, ...), custom_call_target="tpu_custom_call" | custom-call | flops 603979776 | bytes 3407872 | tf_op jit(solution)/shard_map/latents/pallas_call | solution.py:368
  69.6 5.9 %collective-permute-done.22.refs_11_ = bf16[4,128,512]{2,1,0:T(8,128)(2,1)S(1)} collective-permute-done((bf16[4,128,512]{2,1,0:T(8,128)(2,1)S(1)}, bf16[4,128,512]{2,1,0:T(8,128)(2,1)S(1)}, u32[]{:S(2)}, u32[]{:S(2)}) %collective-permute-start.22) | collective-permute-done | bytes 524320 | tf_op jit(solution)/shard_map/ppermute | solution.py:43
  75.5 4.7 %gated.1 = (bf16[128,256]{1,0:T(8,128)(2,1)S(1)}, bf16[128,256]{1,0:T(8,128)(2,1)S(1)}, bf16[128,256]{1,0:T(8,128)(2,1)S(1)}, bf16[128,256]{1,0:T(8,128)(2,1)S(1)}) custom-call(bf16[64,2048]{1,0:T(8,128)(2,1)S(1)} %constant_dynamic-slice_fusion.9.refs_0_, bf16[64,2048]{1,0:T(8,128)(2,1)S(1)} %collective-permute-done.3.refs_1_, ...), custom_call_target="tpu_custom_call" | custom-call | flops 1073741824 | bytes 4194304 | tf_op jit(solution)/shard_map/gated/pallas_call | solution.py:392
  80.3 4.6 %collective-permute-start.23 = (bf16[128,256]{1,0:T(8,128)(2,1)S(1)}, bf16[128,256]{1,0:T(8,128)(2,1)S(1)}, u32[]{:S(2)}, u32[]{:S(2)}) collective-permute-start(bf16[128,256]{1,0:T(8,128)(2,1)S(1)} %get-tuple-element.46), channel_id=1, source_target_pairs={{0,24},{2,26},{4,28},{6,30},{8,16},{10,18},{12,20},{14,22},{16,8},... | collective-permute-start | bytes 196616 | tf_op jit(solution)/shard_map/ppermute | solution.py:40
  85.6 1.8 %collective-permute-done.23 = bf16[128,256]{1,0:T(8,128)(2,1)S(1)} collective-permute-done((bf16[128,256]{1,0:T(8,128)(2,1)S(1)}, bf16[128,256]{1,0:T(8,128)(2,1)S(1)}, u32[]{:S(2)}, u32[]{:S(2)}) %collective-permute-start.23) | collective-permute-done | bytes 65568 | tf_op jit(solution)/shard_map/ppermute | solution.py:40
  87.4 2.6 %collective-permute-done.24 = bf16[128,256]{1,0:T(8,128)(2,1)S(1)} collective-permute-done((bf16[128,256]{1,0:T(8,128)(2,1)S(1)}, bf16[128,256]{1,0:T(8,128)(2,1)S(1)}, u32[]{:S(2)}, u32[]{:S(2)}) %collective-permute-start.24) | collective-permute-done | bytes 65568 | tf_op jit(solution)/shard_map/ppermute | solution.py:40
  90.2 3.6 %collective-permute-start.26 = (bf16[30,1024]{1,0:T(8,128)(2,1)S(1)}, bf16[30,1024]{1,0:T(8,128)(2,1)S(1)}, u32[]{:S(2)}, u32[]{:S(2)}) collective-permute-start(bf16[30,1024]{1,0:T(8,128)(2,1)S(1)} %pad_maximum_fusion.5), channel_id=1, source_target_pairs={{0,2},{2,4},{4,6},{6,8},{8,10},{10,12},{12,14},{14,16},{16,18},{18... | collective-permute-start | bytes 184328 | tf_op jit(solution)/shard_map/ppermute | solution.py:415
  95.6 2.9 %fusion.44 = (f32[128]{0:T(128)S(1)}, f32[128]{0:T(128)S(1)}, f32[128,1024]{1,0:T(8,128)S(1)}) fusion(f32[158,1024]{1,0:T(8,128)S(1)} %maximum_convert_fusion, f32[1024]{0:T(1024)S(1)} %bitcast.94, f32[1024]{0:T(1024)S(1)} %bitcast.95, f32[1024]{0:T(1024)S(1)} %bitcast.66, f32[1024]{0:T(1024)S(1)} %bitcast.67, f32[1024]{0:T(1024)S(1)} %bitcast.68, ...), kind=kLoop, calls=%fused_computation.153 | loop fusion | flops 8388352 | bytes 16905216 | tf_op jit(solution)/shard_map/reduce_sum | solution.py:428
  98.7 2.4 %collective-permute-start.28 = (bf16[256,576]{1,0:T(8,128)(2,1)S(1)}, bf16[256,576]{1,0:T(8,128)(2,1)S(1)}, u32[]{:S(2)}, u32[]{:S(2)}) collective-permute-start(bf16[256,576]{1,0:T(8,128)(2,1)S(1)} %latents.1.refs_0_), channel_id=1, source_target_pairs={{0,2},{2,0},{4,6},{6,4},{8,10},{10,8},{12,14},{14,12},{16,18},{18,... | collective-permute-start | bytes 884744 | tf_op jit(solution)/shard_map/ppermute | solution.py:43
  103.5 6.1 %collective-permute-done.28.refs_1_ = bf16[256,576]{1,0:T(8,128)(2,1)S(1)} collective-permute-done((bf16[256,576]{1,0:T(8,128)(2,1)S(1)}, bf16[256,576]{1,0:T(8,128)(2,1)S(1)}, u32[]{:S(2)}, u32[]{:S(2)}) %collective-permute-start.28) | collective-permute-done | bytes 294944 | tf_op jit(solution)/shard_map/ppermute | solution.py:43
  109.6 7.3 %collective-permute-done.29.refs_2_ = bf16[256,576]{1,0:T(8,128)(2,1)S(1)} collective-permute-done((bf16[256,576]{1,0:T(8,128)(2,1)S(1)}, bf16[256,576]{1,0:T(8,128)(2,1)S(1)}, u32[]{:S(2)}, u32[]{:S(2)}) %collective-permute-start.29) | collective-permute-done | bytes 294944 | tf_op jit(solution)/shard_map/ppermute | solution.py:43
  118.5 3.1 %fusion.34 = f32[128,2048]{1,0:T(8,128)S(1)} fusion(bf16[1024,2048]{1,0:T(8,128)(2,1)} %param.26, f32[128,1024]{1,0:T(8,128)S(1)} %get-tuple-element.54, f32[1024]{0:T(1024)S(1)} %copy-done.7, f32[128]{0:T(128)S(1)} %fusion.41, f32[128]{0:T(128)S(1)} %multiply_bitcast_fusion), kind=kOutput, calls=%fused_computation.76 | convolution fusion | flops 537919488 | bytes 5772288 | tf_op jit(solution)/shard_map/dot_general | solution.py:462
  121.6 9.3 %attention.1 = (bf16[128,1024]{1,0:T(8,128)(2,1)S(1)}, f32[8,128]{1,0:T(8,128)}) custom-call(bf16[8,128,576]{2,1,0:T(8,128)(2,1)S(1)} %copy-done, bf16[512,1024]{1,0:T(8,128)(2,1)S(1)} %copy-done.3, bf16[256,576]{1,0:T(8,128)(2,1)S(1)} %latents.1.refs_0_, bf16[256,576]{1,0:T(8,128)(2,1)S(1)} %collective-permute-done.28.refs_1_, ...), custom_call_target="tpu_custom_call" | custom-call | flops 4563402752 | bytes 2359296 | tf_op jit(solution)/shard_map/attention/pallas_call | solution.py:440
  (103 shorter events, 27.7 us)
Async XLA Ops:
  2.4 11.5 %collective-permute-start = (bf16[64,576]{1,0:T(8,128)(2,1)S(1)}, bf16[64,576]{1,0:T(8,128)(2,1)S(1)}, u32[]{:S(2)}, u32[]{:S(2)}) collective-permute-start(bf16[64,576]{1,0:T(8,128)(2,1)S(1)} %fusion.39), channel_id=1, source_target_pairs={{0,8},{2,10},{4,12},{6,14},{8,0},{10,2},{12,4},{14,6},{16,24},{18,... | collective-permute-start | bytes 221192 | tf_op jit(solution)/shard_map/ppermute | solution.py:40
  5.5 8.8 %collective-permute-start.1 = (bf16[64,576]{1,0:T(8,128)(2,1)S(1)}, bf16[64,576]{1,0:T(8,128)(2,1)S(1)}, u32[]{:S(2)}, u32[]{:S(2)}) collective-permute-start(bf16[64,576]{1,0:T(8,128)(2,1)S(1)} %fusion.39), channel_id=1, source_target_pairs={{0,16},{2,18},{4,20},{6,22},{8,24},{10,26},{12,28},{14,30},{16,0},... | collective-permute-start | bytes 221192 | tf_op jit(solution)/shard_map/ppermute | solution.py:40
  9.2 17.7 %collective-permute-start.9 = (bf16[128,512]{1,0:T(8,128)(2,1)S(1)}, bf16[128,512]{1,0:T(8,128)(2,1)S(1)}, u32[]{:S(2)}, u32[]{:S(2)}) collective-permute-start(bf16[128,512]{1,0:T(8,128)(2,1)S(1)} %pad_maximum_fusion.2), channel_id=1, source_target_pairs={{0,8},{2,10},{4,12},{6,14},{8,0},{10,2},{12,4},{14,6},{16,24},{18,... | collective-permute-start | bytes 393224 | tf_op jit(solution)/shard_map/ppermute | solution.py:40
  10.2 18.1 %collective-permute-start.10 = (bf16[128,512]{1,0:T(8,128)(2,1)S(1)}, bf16[128,512]{1,0:T(8,128)(2,1)S(1)}, u32[]{:S(2)}, u32[]{:S(2)}) collective-permute-start(bf16[128,512]{1,0:T(8,128)(2,1)S(1)} %pad_maximum_fusion.3), channel_id=1, source_target_pairs={{0,16},{2,18},{4,20},{6,22},{8,24},{10,26},{12,28},{14,30},{16,0},... | collective-permute-start | bytes 393224 | tf_op jit(solution)/shard_map/ppermute | solution.py:40
  14.0 14.3 %collective-permute-start.11 = (bf16[128,512]{1,0:T(8,128)(2,1)S(1)}, bf16[128,512]{1,0:T(8,128)(2,1)S(1)}, u32[]{:S(2)}, u32[]{:S(2)}) collective-permute-start(bf16[128,512]{1,0:T(8,128)(2,1)S(1)} %pad_maximum_fusion.4), channel_id=1, source_target_pairs={{0,24},{2,26},{4,28},{6,30},{8,16},{10,18},{12,20},{14,22},{16,8},... | collective-permute-start | bytes 393224 | tf_op jit(solution)/shard_map/ppermute | solution.py:40
  18.1 18.8 %collective-permute-start.3 = (bf16[64,2048]{1,0:T(8,128)(2,1)S(1)}, bf16[64,2048]{1,0:T(8,128)(2,1)S(1)}, u32[]{:S(2)}, u32[]{:S(2)}) collective-permute-start(bf16[64,2048]{1,0:T(8,128)(2,1)S(1)} %constant_dynamic-slice_fusion.9.refs_0_), channel_id=1, source_target_pairs={{0,8},{2,10},{4,12},{6,14},{8,0},{10,2},{12,4},{14,6},{16,24},{18,... | collective-permute-start | bytes 786440 | tf_op jit(solution)/shard_map/ppermute | solution.py:40
  24.8 21.3 %collective-permute-start.4 = (bf16[64,2048]{1,0:T(8,128)(2,1)S(1)}, bf16[64,2048]{1,0:T(8,128)(2,1)S(1)}, u32[]{:S(2)}, u32[]{:S(2)}) collective-permute-start(bf16[64,2048]{1,0:T(8,128)(2,1)S(1)} %constant_dynamic-slice_fusion.9.refs_0_), channel_id=1, source_target_pairs={{0,16},{2,18},{4,20},{6,22},{8,24},{10,26},{12,28},{14,30},{16,0},... | collective-permute-start | bytes 786440 | tf_op jit(solution)/shard_map/ppermute | solution.py:40
  26.9 20.7 %collective-permute-start.5 = (bf16[64,2048]{1,0:T(8,128)(2,1)S(1)}, bf16[64,2048]{1,0:T(8,128)(2,1)S(1)}, u32[]{:S(2)}, u32[]{:S(2)}) collective-permute-start(bf16[64,2048]{1,0:T(8,128)(2,1)S(1)} %constant_dynamic-slice_fusion.9.refs_0_), channel_id=1, source_target_pairs={{0,24},{2,26},{4,28},{6,30},{8,16},{10,18},{12,20},{14,22},{16,8},... | collective-permute-start | bytes 786440 | tf_op jit(solution)/shard_map/ppermute | solution.py:40
  28.4 31.8 %collective-permute-start.20 = (bf16[4,128,512]{2,1,0:T(8,128)(2,1)S(1)}, bf16[4,128,512]{2,1,0:T(8,128)(2,1)S(1)}, u32[]{:S(2)}, u32[]{:S(2)}) collective-permute-start(bf16[4,128,512]{2,1,0:T(8,128)(2,1)S(1)} %pad_maximum_fusion.refs_8_), channel_id=1, source_target_pairs={{0,2},{2,0},{4,6},{6,4},{8,10},{10,8},{12,14},{14,12},{16,18},{18,... | collective-permute-start | bytes 1572872 | tf_op jit(solution)/shard_map/ppermute | solution.py:43
  29.9 30.8 %collective-permute-start.21 = (bf16[4,128,512]{2,1,0:T(8,128)(2,1)S(1)}, bf16[4,128,512]{2,1,0:T(8,128)(2,1)S(1)}, u32[]{:S(2)}, u32[]{:S(2)}) collective-permute-start(bf16[4,128,512]{2,1,0:T(8,128)(2,1)S(1)} %pad_maximum_fusion.refs_8_), channel_id=1, source_target_pairs={{0,4},{2,6},{4,0},{6,2},{8,12},{10,14},{12,8},{14,10},{16,20},{18,... | collective-permute-start | bytes 1572872 | tf_op jit(solution)/shard_map/ppermute | solution.py:43
  36.9 18.4 %collective-permute-start.6 = (bf16[4,64,576]{2,1,0:T(8,128)(2,1)S(1)}, bf16[4,64,576]{2,1,0:T(8,128)(2,1)S(1)}, u32[]{:S(2)}, u32[]{:S(2)}) collective-permute-start(bf16[4,64,576]{2,1,0:T(8,128)(2,1)S(1)} %pad_maximum_fusion.1.refs_4_), channel_id=1, source_target_pairs={{0,2},{2,0},{4,6},{6,4},{8,10},{10,8},{12,14},{14,12},{16,18},{18,... | collective-permute-start | bytes 884744 | tf_op jit(solution)/shard_map/ppermute | solution.py:43
  46.1 13.6 %collective-permute-start.7 = (bf16[4,64,576]{2,1,0:T(8,128)(2,1)S(1)}, bf16[4,64,576]{2,1,0:T(8,128)(2,1)S(1)}, u32[]{:S(2)}, u32[]{:S(2)}) collective-permute-start(bf16[4,64,576]{2,1,0:T(8,128)(2,1)S(1)} %pad_maximum_fusion.1.refs_4_), channel_id=1, source_target_pairs={{0,4},{2,6},{4,0},{6,2},{8,12},{10,14},{12,8},{14,10},{16,20},{18,... | collective-permute-start | bytes 884744 | tf_op jit(solution)/shard_map/ppermute | solution.py:43
  47.6 12.1 %collective-permute-start.8 = (bf16[4,64,576]{2,1,0:T(8,128)(2,1)S(1)}, bf16[4,64,576]{2,1,0:T(8,128)(2,1)S(1)}, u32[]{:S(2)}, u32[]{:S(2)}) collective-permute-start(bf16[4,64,576]{2,1,0:T(8,128)(2,1)S(1)} %pad_maximum_fusion.1.refs_4_), channel_id=1, source_target_pairs={{0,6},{2,4},{4,2},{6,0},{8,14},{10,12},{12,10},{14,8},{16,22},{18,... | collective-permute-start | bytes 884744 | tf_op jit(solution)/shard_map/ppermute | solution.py:43
  60.7 14.8 %collective-permute-start.22 = (bf16[4,128,512]{2,1,0:T(8,128)(2,1)S(1)}, bf16[4,128,512]{2,1,0:T(8,128)(2,1)S(1)}, u32[]{:S(2)}, u32[]{:S(2)}) collective-permute-start(bf16[4,128,512]{2,1,0:T(8,128)(2,1)S(1)} %pad_maximum_fusion.refs_8_), channel_id=1, source_target_pairs={{0,6},{2,4},{4,2},{6,0},{8,14},{10,12},{12,10},{14,8},{16,22},{18,... | collective-permute-start | bytes 1572872 | tf_op jit(solution)/shard_map/ppermute | solution.py:43
  62.8 12.7 %collective-permute-start.12 = (bf16[64,2048]{1,0:T(8,128)(2,1)S(1)}, bf16[64,2048]{1,0:T(8,128)(2,1)S(1)}, u32[]{:S(2)}, u32[]{:S(2)}) collective-permute-start(bf16[64,2048]{1,0:T(8,128)(2,1)S(1)} %constant_dynamic-slice_fusion.9.refs_0_), channel_id=1, source_target_pairs={{0,1},{1,0},{2,3},{3,2},{4,5},{5,4},{6,7},{7,6},{8,9},{9,8},{10,11... | collective-permute-start | bytes 786440 | tf_op jit(solution)/shard_map/ppermute | solution.py:47
  62.8 12.7 %collective-permute-start.13 = (bf16[64,2048]{1,0:T(8,128)(2,1)S(1)}, bf16[64,2048]{1,0:T(8,128)(2,1)S(1)}, u32[]{:S(2)}, u32[]{:S(2)}) collective-permute-start(bf16[64,2048]{1,0:T(8,128)(2,1)S(1)} %collective-permute-done.3.refs_1_), channel_id=1, source_target_pairs={{0,1},{1,0},{2,3},{3,2},{4,5},{5,4},{6,7},{7,6},{8,9},{9,8},{10,11... | collective-permute-start | bytes 786440 | tf_op jit(solution)/shard_map/ppermute | solution.py:47
  63.3 12.2 %collective-permute-start.14 = (bf16[64,2048]{1,0:T(8,128)(2,1)S(1)}, bf16[64,2048]{1,0:T(8,128)(2,1)S(1)}, u32[]{:S(2)}, u32[]{:S(2)}) collective-permute-start(bf16[64,2048]{1,0:T(8,128)(2,1)S(1)} %collective-permute-done.4.refs_2_), channel_id=1, source_target_pairs={{0,1},{1,0},{2,3},{3,2},{4,5},{5,4},{6,7},{7,6},{8,9},{9,8},{10,11... | collective-permute-start | bytes 786440 | tf_op jit(solution)/shard_map/ppermute | solution.py:47
  63.4 12.1 %collective-permute-start.15 = (bf16[64,2048]{1,0:T(8,128)(2,1)S(1)}, bf16[64,2048]{1,0:T(8,128)(2,1)S(1)}, u32[]{:S(2)}, u32[]{:S(2)}) collective-permute-start(bf16[64,2048]{1,0:T(8,128)(2,1)S(1)} %collective-permute-done.5.refs_3_), channel_id=1, source_target_pairs={{0,1},{1,0},{2,3},{3,2},{4,5},{5,4},{6,7},{7,6},{8,9},{9,8},{10,11... | collective-permute-start | bytes 786440 | tf_op jit(solution)/shard_map/ppermute | solution.py:47
  80.3 7.1 %collective-permute-start.23 = (bf16[128,256]{1,0:T(8,128)(2,1)S(1)}, bf16[128,256]{1,0:T(8,128)(2,1)S(1)}, u32[]{:S(2)}, u32[]{:S(2)}) collective-permute-start(bf16[128,256]{1,0:T(8,128)(2,1)S(1)} %get-tuple-element.46), channel_id=1, source_target_pairs={{0,24},{2,26},{4,28},{6,30},{8,16},{10,18},{12,20},{14,22},{16,8},... | collective-permute-start | bytes 196616 | tf_op jit(solution)/shard_map/ppermute | solution.py:40
  98.7 11.0 %collective-permute-start.28 = (bf16[256,576]{1,0:T(8,128)(2,1)S(1)}, bf16[256,576]{1,0:T(8,128)(2,1)S(1)}, u32[]{:S(2)}, u32[]{:S(2)}) collective-permute-start(bf16[256,576]{1,0:T(8,128)(2,1)S(1)} %latents.1.refs_0_), channel_id=1, source_target_pairs={{0,2},{2,0},{4,6},{6,4},{8,10},{10,8},{12,14},{14,12},{16,18},{18,... | collective-permute-start | bytes 884744 | tf_op jit(solution)/shard_map/ppermute | solution.py:43
  101.1 15.8 %collective-permute-start.29 = (bf16[256,576]{1,0:T(8,128)(2,1)S(1)}, bf16[256,576]{1,0:T(8,128)(2,1)S(1)}, u32[]{:S(2)}, u32[]{:S(2)}) collective-permute-start(bf16[256,576]{1,0:T(8,128)(2,1)S(1)} %latents.1.refs_0_), channel_id=1, source_target_pairs={{0,4},{2,6},{4,0},{6,2},{8,12},{10,14},{12,8},{14,10},{16,20},{18,... | collective-permute-start | bytes 884744 | tf_op jit(solution)/shard_map/ppermute | solution.py:43
  102.6 15.9 %collective-permute-start.30 = (bf16[256,576]{1,0:T(8,128)(2,1)S(1)}, bf16[256,576]{1,0:T(8,128)(2,1)S(1)}, u32[]{:S(2)}, u32[]{:S(2)}) collective-permute-start(bf16[256,576]{1,0:T(8,128)(2,1)S(1)} %latents.1.refs_0_), channel_id=1, source_target_pairs={{0,6},{2,4},{4,2},{6,0},{8,14},{10,12},{12,10},{14,8},{16,22},{18,... | collective-permute-start | bytes 884744 | tf_op jit(solution)/shard_map/ppermute | solution.py:43
  103.5 18.1 %collective-permute-start.31 = (bf16[256,576]{1,0:T(8,128)(2,1)S(1)}, bf16[256,576]{1,0:T(8,128)(2,1)S(1)}, u32[]{:S(2)}, u32[]{:S(2)}) collective-permute-start(bf16[256,576]{1,0:T(8,128)(2,1)S(1)} %latents.1.refs_0_), channel_id=1, source_target_pairs={{0,1},{1,0},{2,3},{3,2},{4,5},{5,4},{6,7},{7,6},{8,9},{9,8},{10,11... | collective-permute-start | bytes 884744 | tf_op jit(solution)/shard_map/ppermute | solution.py:47
  109.6 12.0 %collective-permute-start.32 = (bf16[256,576]{1,0:T(8,128)(2,1)S(1)}, bf16[256,576]{1,0:T(8,128)(2,1)S(1)}, u32[]{:S(2)}, u32[]{:S(2)}) collective-permute-start(bf16[256,576]{1,0:T(8,128)(2,1)S(1)} %collective-permute-done.28.refs_1_), channel_id=1, source_target_pairs={{0,1},{1,0},{2,3},{3,2},{4,5},{5,4},{6,7},{7,6},{8,9},{9,8},{10,11... | collective-permute-start | bytes 884744 | tf_op jit(solution)/shard_map/ppermute | solution.py:47
  (20 other events, 230.6 us)
where the time goes:
time: 135 us; the launch traced here: 134 us
  waiting for transfers between devices  47 us (35%)
  starting transfers between devices  46.4 us (34%)
  Pallas kernels  25.3 us (19%)
  other arithmetic  6.2 us (5%)
  matrix products  3.78 us (3%)
  blocking collectives  2.39 us (2%)
  local copies, waits for them, and re-layouts  2.19 us (2%)
    ppermute x12, starting transfers between devices, outer_swap(): lax.ppermute(block, 'sp', [(i, i ^ mask) for i in range(self.sp_count)])  25.7 us
    ppermute x9, waiting for transfers between devices, inner_swap(): lax.ppermute(block, 'sp', [(i, i ^ mask) for i in range(self.sp_count)])  25.2 us
    ppermute x12, waiting for transfers between devices, outer_swap(): lax.ppermute(block, 'sp', [(i, i ^ mask) for i in range(self.sp_count)])  18.9 us
    ppermute x9, starting transfers between devices, inner_swap(): lax.ppermute(block, 'sp', [(i, i ^ mask) for i in range(self.sp_count)])  14.4 us
    pallas_call x1, Pallas kernels, local(): pl.pallas_call(functools.partial(attention_kernel, place, score_scale, ra...  9.32 us
    pallas_call x1, Pallas kernels, local(): pl.pallas_call(functools.partial(latent_kernel, place, rank, split_rows),...  5.72 us
    pallas_call x1, Pallas kernels, local(): pl.pallas_call(functools.partial(query_kernel, rank), out_shape=jax.Shape...  5.53 us
    pallas_call x1, Pallas kernels, local(): pl.pallas_call(functools.partial(gated_kernel, place), out_shape=[jax.Sha...  4.72 us
  transfers between devices with their start and end apart: 36, of which 14 were waited for; matrix products, arithmetic and copies ran while one was open for 4% of the time, Pallas kernels for 8%

commit v1 on v0

--- a/solution.py
+++ b/solution.py
@@ -76,10 +76,6 @@
     for c in copies:
         c.start()
     return copies
-
-
-def any_specs(n):
-    return [pl.BlockSpec(memory_space=pl.ANY)] * n
 
 
 def whole_vmem():
@@ -132,29 +128,19 @@
     tables = tp if share else 1
     n_rows, n_w = outer, tables * inner
     row_refs, w_refs = refs[:n_rows], refs[n_rows : n_rows + n_w]
-    gain_ref, cos_ref, sin_ref, out_ref, rows, weight, sem_r, sem_w = refs[n_rows + n_w :]
+    gain_ref, cos_ref, sin_ref, out_ref, rows, weight = refs[n_rows + n_w :]
     zi, xi, ti = place.indices()
     piece = w_refs[0].shape[1]
     block = piece * tables
     count = row_refs[0].shape[0]
-    pairs = []
     for t in range(tables):
         owner = behind(ti, t, tp) if share else 0
         for k in range(inner):
             for j in range(outer):
                 start = ((zi ^ j) * inner + (xi ^ k)) * block + owner * piece
-                pairs.append(
-                    (
-                        w_refs[t * inner + k].at[j],
-                        weight.at[pl.ds(pl.multiple_of(start, piece), piece)],
-                    )
-                )
-    w_copies = copy_all(pairs, sem_w)
-    r_copies = copy_all(
-        [(row_refs[j], rows.at[pl.ds(j * count, count)]) for j in range(outer)], sem_r
-    )
-    for c in w_copies + r_copies:
-        c.wait()
+                weight[pl.ds(pl.multiple_of(start, piece), piece)] = w_refs[t * inner + k][j]
+    for j in range(outer):
+        rows[j * count : (j + 1) * count] = row_refs[j][...]
     pre = jnp.dot(rows[...], weight[...], preferred_element_type=jnp.float32)
     plain = pre[:, :rank]
     scale = lax.rsqrt(jnp.mean(plain * plain, axis=-1, keepdims=True) + epsilon)
@@ -171,39 +157,25 @@
     n_rows = tp * outer
     row_refs, w_refs = refs[:n_rows], refs[n_rows : n_rows + inner]
     outs = refs[n_rows + inner : n_rows + inner + outer]
-    rows, weight, sem_r, sem_w = refs[n_rows + inner + outer :]
+    rows, weight = refs[n_rows + inner + outer :]
     zi, xi, ti = place.indices()
     block = w_refs[0].shape[1]
     count = row_refs[0].shape[0]
-    pairs = []
     for k in range(inner):
         for j in range(outer):
             start = ((zi ^ j) * inner + (xi ^ k)) * block
-            pairs.append(
-                (w_refs[k].at[j], weight.at[pl.ds(pl.multiple_of(start, block), block)])
-            )
-    w_copies = copy_all(pairs, sem_w)
-    pairs = []
+            weight[pl.ds(pl.multiple_of(start, block), block)] = w_refs[k][j]
     for t in range(tp):
         owner = behind(ti, t, tp)
         for j in range(outer):
             start = j * tp * count + owner * count
-            pairs.append(
-                (
-                    row_refs[t * outer + j],
-                    rows.at[pl.ds(pl.multiple_of(start, count), count)],
-                )
-            )
-    r_copies = copy_all(pairs, sem_r)
-    for c in w_copies + r_copies:
-        c.wait()
+            rows[pl.ds(pl.multiple_of(start, count), count)] = row_refs[t * outer + j][...]
     chunk = tp * count
     width = outs[0].shape[1]
+    pre = jnp.dot(rows[...], weight[...], preferred_element_type=jnp.float32)
     for j in range(outer):
-        pre = jnp.dot(
-            rows[pl.ds(j * chunk, chunk)], weight[...], preferred_element_type=jnp.float32
-        )
-        value, gate = pre[:, :width], pre[:, width:]
+        part = pre[j * chunk : (j + 1) * chunk]
+        value, gate = part[:, :width], part[:, width:]
         outs[j][...] = (value * jax.nn.sigmoid(gate)).astype(jnp.bfloat16)
 
 
@@ -211,14 +183,13 @@
     outer, inner, tp = place.outer, place.inner, place.tp_count
     n_k = tp * inner
     key_refs = refs[:n_k]
-    out_ref, lse_ref, keys, sem = refs[n_k:]
+    out_ref, lse_ref, keys = refs[n_k:]
     zi, xi, ti = place.indices()
     heads, count, depth = q_ref.shape
     piece = key_refs[0].shape[0]
     share = piece // outer
-    copies = copy_all(
-        [(key_refs[n], keys.at[pl.ds(n * piece, piece)]) for n in range(n_k)], sem
-    )
+    for n in range(n_k):
+        keys[n * piece : (n + 1) * piece] = key_refs[n][...]
     lane = lax.broadcasted_iota(jnp.int32, (1, piece), 1)
     back = zi ^ lax.shift_right_logical(lane, share.bit_length() - 1)
     within = jnp.bitwise_and(lane, share - 1)
@@ -235,8 +206,6 @@
     allowed = key_index <= jnp.concatenate([query_index] * together, axis=0)
     width = VALUE_HEAD_WIDTH
     sums = []
-    for c in copies:
-        c.wait()
     for g in range(heads // together):
         queries = q_ref[g * together : (g + 1) * together].reshape(size, depth)
         scores = lax.dot_general(
@@ -368,13 +337,11 @@
     latent = pl.pallas_call(
         functools.partial(latent_kernel, place, rank, split_rows),
         out_shape=jax.ShapeDtypeStruct((outer * share, rank + QK_ROPE), bf16),
-        in_specs=any_specs(outer + len(tables)) + [whole_vmem()] * 3,
+        in_specs=[whole_vmem()] * (outer + len(tables) + 3),
         out_specs=whole_vmem(),
         scratch_shapes=[
             pltpu.VMEM((outer * share, model), bf16),
             pltpu.VMEM((model, rank + QK_ROPE), bf16),
-            pltpu.SemaphoreType.DMA((outer,)),
-            pltpu.SemaphoreType.DMA((len(tables) * outer,)),
         ],
         compiler_params=pltpu.CompilerParams(vmem_limit_bytes=16 << 20),
         cost_estimate=pl.CostEstimate(
@@ -392,13 +359,11 @@
     gated = pl.pallas_call(
         functools.partial(gated_kernel, place),
         out_shape=[jax.ShapeDtypeStruct((row_count, width), bf16)] * outer,
-        in_specs=any_specs(len(all_rows) + inner),
+        in_specs=[whole_vmem()] * (len(all_rows) + inner),
         out_specs=[whole_vmem()] * outer,
         scratch_shapes=[
             pltpu.VMEM((outer * row_count, model), bf16),
             pltpu.VMEM((model, 2 * width), bf16),
-            pltpu.SemaphoreType.DMA((len(all_rows),)),
-            pltpu.SemaphoreType.DMA((inner * outer,)),
         ],
         compiler_params=pltpu.CompilerParams(vmem_limit_bytes=24 << 20),
         cost_estimate=pl.CostEstimate(
@@ -417,6 +382,29 @@
         "sp",
         [(i, i + 1) for i in range(place.sp_count - 1)],
     )
+    score_scale = (PLAIN_QK_WIDTH + QK_ROPE) ** (-0.5)
+    key_total = place.sp_count * row_count
+    attention, log_sums = pl.pallas_call(
+        functools.partial(attention_kernel, place, score_scale, rank),
+        out_shape=[
+            jax.ShapeDtypeStruct((row_count, head_count * VALUE_HEAD_WIDTH), bf16),
+            jax.ShapeDtypeStruct((head_count, row_count), jnp.float32),
+        ],
+        in_specs=[whole_vmem()] * (2 + len(latents)),
+        out_specs=[whole_vmem()] * 2,
+        scratch_shapes=[
+            pltpu.VMEM((key_total, rank + QK_ROPE), bf16),
+        ],
+        compiler_params=pltpu.CompilerParams(vmem_limit_bytes=32 << 20),
+        cost_estimate=pl.CostEstimate(
+            flops=2 * row_count * head_count * key_total * (2 * rank + QK_ROPE),
+            bytes_accessed=2 * key_total * (rank + QK_ROPE),
+            transcendentals=row_count * head_count * key_total,
+        ),
+        name="attention",
+    )(queries, value_up_weight, *latents)
+
+    prior_rows, gated_rows, _ = lax.optimization_barrier((prior_rows, gated_rows, attention))
     padded = jnp.concatenate([prior_rows, gated_rows], axis=0).astype(jnp.float32)
     mixed = jnp.zeros(gated_rows.shape, jnp.float32)
     for tap_index in range(conv_taps.shape[0]):
@@ -434,29 +422,6 @@
     conv_out = jax.nn.silu(
         (mixed - channel_mean[:, None]) * lax.rsqrt(channel_var + epsilon)[:, None] * conv_gain
     ).astype(bf16)
-
-    score_scale = (PLAIN_QK_WIDTH + QK_ROPE) ** (-0.5)
-    key_total = place.sp_count * row_count
-    attention, log_sums = pl.pallas_call(
-        functools.partial(attention_kernel, place, score_scale, rank),
-        out_shape=[
-            jax.ShapeDtypeStruct((row_count, head_count * VALUE_HEAD_WIDTH), bf16),
-            jax.ShapeDtypeStruct((head_count, row_count), jnp.float32),
-        ],
-        in_specs=[whole_vmem()] * 2 + any_specs(len(latents)),
-        out_specs=[whole_vmem()] * 2,
-        scratch_shapes=[
-            pltpu.VMEM((key_total, rank + QK_ROPE), bf16),
-            pltpu.SemaphoreType.DMA((len(latents),)),
-        ],
-        compiler_params=pltpu.CompilerParams(vmem_limit_bytes=40 << 20),
-        cost_estimate=pl.CostEstimate(
-            flops=2 * row_count * head_count * key_total * (2 * rank + QK_ROPE),
-            bytes_accessed=2 * key_total * (rank + QK_ROPE),
-            transcendentals=row_count * head_count * key_total,
-        ),
-        name="attention",
-    )(queries, value_up_weight, *latents)
 
     partial = (
         jnp.dot(conv_out, w_merge_conv, preferred_element_type=jnp.float32)

time: 135 us -> 118 us (0.87)
  waiting for transfers between devices: 47 us -> 36.8 us
  Pallas kernels: 25.3 us -> 17.8 us
  starting transfers between devices: 46.4 us -> 45 us
    ppermute x9, waiting for transfers between devices: 25.2 us -> 16.4 us  [inner_swap(): lax.ppermute(block, 'sp', [(i, i ^ mask) for i in range(self.sp_count)])]
    pallas_call x1, Pallas kernels: 5.72 us -> 1.35 us  [local(): pl.pallas_call(functools.partial(latent_kernel, place, rank, split_rows),...]
    pallas_call x1, Pallas kernels: 4.72 us -> 1.43 us  [local(): pl.pallas_call(functools.partial(gated_kernel, place), out_shape=[jax.Sha...]
    ppermute x1, waiting for transfers between devices: 1.66 us -> 0.01 us  [local(): lax.ppermute(gated_rows[row_count - conv_reach:], 'sp', [(i, i + 1) for i...]
  transfers between devices with their start and end apart: 36 -> 36, of which waited for: 14 -> 11; matrix products, arithmetic and copies ran while one was open for 4% -> 3% of each run, Pallas kernels for 8% -> 15%
where the time goes in v1:
time: 118 us; the launch traced here: 116 us
  starting transfers between devices  45 us (38%)
  waiting for transfers between devices  36.8 us (31%)
  Pallas kernels  17.8 us (15%)
  other arithmetic  6.79 us (6%)
  matrix products  4.06 us (3%)
  blocking collectives  2.39 us (2%)
  local copies, waits for them, and re-layouts  2.26 us (2%)
    ppermute x12, starting transfers between devices, outer_swap(): lax.ppermute(block, 'sp', [(i, i ^ mask) for i in range(self.sp_count)])  25.7 us
    ppermute x12, waiting for transfers between devices, outer_swap(): lax.ppermute(block, 'sp', [(i, i ^ mask) for i in range(self.sp_count)])  18.2 us
    ppermute x9, waiting for transfers between devices, inner_swap(): lax.ppermute(block, 'sp', [(i, i ^ mask) for i in range(self.sp_count)])  16.4 us
    ppermute x9, starting transfers between devices, inner_swap(): lax.ppermute(block, 'sp', [(i, i ^ mask) for i in range(self.sp_count)])  13.1 us
    pallas_call x1, Pallas kernels, local(): pl.pallas_call(functools.partial(attention_kernel, place, score_scale, ra...  9.44 us
    pallas_call x1, Pallas kernels, local(): pl.pallas_call(functools.partial(query_kernel, rank), out_shape=jax.Shape...  5.55 us
    ppermute x14, starting transfers between devices, tp_shift(): return lax.ppermute(block, 'tp', route)  3.71 us
    dot_general x1, matrix products, local(): jnp.dot(conv_out, w_merge_conv, preferred_element_type=jnp.float32)  3.32 us
  transfers between devices with their start and end apart: 36, of which 11 were waited for; matrix products, arithmetic and copies ran while one was open for 3% of the time, Pallas kernels for 15%

profile of v1, /device:TPU:0, one launch (start us, length us, event | category | flops | bytes accessed | tf_op | source)
XLA Modules:
  0.0 116.3 jit_solution(8891926151749487303)
XLA Ops:
  2.4 3.1 %collective-permute-start = (bf16[64,576]{1,0:T(8,128)(2,1)S(1)}, bf16[64,576]{1,0:T(8,128)(2,1)S(1)}, u32[]{:S(2)}, u32[]{:S(2)}) collective-permute-start(bf16[64,576]{1,0:T(8,128)(2,1)S(1)} %fusion.39), channel_id=1, source_target_pairs={{0,8},{2,10},{4,12},{6,14},{8,0},{10,2},{12,4},{14,6},{16,24},{18,... | collective-permute-start | bytes 221192 | tf_op jit(solution)/shard_map/ppermute | solution.py:40
  5.5 2.6 %collective-permute-start.1 = (bf16[64,576]{1,0:T(8,128)(2,1)S(1)}, bf16[64,576]{1,0:T(8,128)(2,1)S(1)}, u32[]{:S(2)}, u32[]{:S(2)}) collective-permute-start(bf16[64,576]{1,0:T(8,128)(2,1)S(1)} %fusion.39), channel_id=1, source_target_pairs={{0,16},{2,18},{4,20},{6,22},{8,24},{10,26},{12,28},{14,30},{16,0},... | collective-permute-start | bytes 221192 | tf_op jit(solution)/shard_map/ppermute | solution.py:40
  10.2 3.6 %collective-permute-start.10 = (bf16[128,512]{1,0:T(8,128)(2,1)S(1)}, bf16[128,512]{1,0:T(8,128)(2,1)S(1)}, u32[]{:S(2)}, u32[]{:S(2)}) collective-permute-start(bf16[128,512]{1,0:T(8,128)(2,1)S(1)} %pad_maximum_fusion.4), channel_id=1, source_target_pairs={{0,16},{2,18},{4,20},{6,22},{8,24},{10,26},{12,28},{14,30},{16,0},... | collective-permute-start | bytes 393224 | tf_op jit(solution)/shard_map/ppermute | solution.py:40
  15.3 2.4 %all_gather.3 = bf16[128,2048]{1,0:T(8,128)(2,1)S(1)} all-gather(bf16[128,1024]{1,0:T(8,128)(2,1)} %param.14), channel_id=1, replica_groups=mesh['sp'=16,'tp'=2] {'tp'}, dimensions={1}, use_global_device_ids=true | all-gather | bytes 786432 | tf_op jit(solution)/shard_map/all_gather | solution.py:285
  18.1 6.7 %collective-permute-start.3 = (bf16[64,2048]{1,0:T(8,128)(2,1)S(1)}, bf16[64,2048]{1,0:T(8,128)(2,1)S(1)}, u32[]{:S(2)}, u32[]{:S(2)}) collective-permute-start(bf16[64,2048]{1,0:T(8,128)(2,1)S(1)} %constant_dynamic-slice_fusion.9.refs_0_), channel_id=1, source_target_pairs={{0,8},{2,10},{4,12},{6,14},{8,0},{10,2},{12,4},{14,6},{16,24},{18,... | collective-permute-start | bytes 786440 | tf_op jit(solution)/shard_map/ppermute | solution.py:40
  24.8 2.1 %collective-permute-start.4 = (bf16[64,2048]{1,0:T(8,128)(2,1)S(1)}, bf16[64,2048]{1,0:T(8,128)(2,1)S(1)}, u32[]{:S(2)}, u32[]{:S(2)}) collective-permute-start(bf16[64,2048]{1,0:T(8,128)(2,1)S(1)} %constant_dynamic-slice_fusion.9.refs_0_), channel_id=1, source_target_pairs={{0,16},{2,18},{4,20},{6,22},{8,24},{10,26},{12,28},{14,30},{16,0},... | collective-permute-start | bytes 786440 | tf_op jit(solution)/shard_map/ppermute | solution.py:40
  28.4 1.6 %collective-permute-start.20 = (bf16[4,128,512]{2,1,0:T(8,128)(2,1)S(1)}, bf16[4,128,512]{2,1,0:T(8,128)(2,1)S(1)}, u32[]{:S(2)}, u32[]{:S(2)}) collective-permute-start(bf16[4,128,512]{2,1,0:T(8,128)(2,1)S(1)} %pad_maximum_fusion.refs_8_), channel_id=1, source_target_pairs={{0,2},{2,0},{4,6},{6,4},{8,10},{10,8},{12,14},{14,12},{16,18},{18,... | collective-permute-start | bytes 1572872 | tf_op jit(solution)/shard_map/ppermute | solution.py:43
  29.9 1.5 %collective-permute-start.21 = (bf16[4,128,512]{2,1,0:T(8,128)(2,1)S(1)}, bf16[4,128,512]{2,1,0:T(8,128)(2,1)S(1)}, u32[]{:S(2)}, u32[]{:S(2)}) collective-permute-start(bf16[4,128,512]{2,1,0:T(8,128)(2,1)S(1)} %pad_maximum_fusion.refs_8_), channel_id=1, source_target_pairs={{0,4},{2,6},{4,0},{6,2},{8,12},{10,14},{12,8},{14,10},{16,20},{18,... | collective-permute-start | bytes 1572872 | tf_op jit(solution)/shard_map/ppermute | solution.py:43
  31.5 5.5 %collective-permute-done.3.refs_1_ = bf16[64,2048]{1,0:T(8,128)(2,1)S(1)} collective-permute-done((bf16[64,2048]{1,0:T(8,128)(2,1)S(1)}, bf16[64,2048]{1,0:T(8,128)(2,1)S(1)}, u32[]{:S(2)}, u32[]{:S(2)}) %collective-permute-start.3) | collective-permute-done | bytes 262176 | tf_op jit(solution)/shard_map/ppermute | solution.py:40
  36.9 1.5 %collective-permute-start.6 = (bf16[4,64,576]{2,1,0:T(8,128)(2,1)S(1)}, bf16[4,64,576]{2,1,0:T(8,128)(2,1)S(1)}, u32[]{:S(2)}, u32[]{:S(2)}) collective-permute-start(bf16[4,64,576]{2,1,0:T(8,128)(2,1)S(1)} %pad_maximum_fusion.1.refs_4_), channel_id=1, source_target_pairs={{0,2},{2,0},{4,6},{6,4},{8,10},{10,8},{12,14},{14,12},{16,18},{18,... | collective-permute-start | bytes 884744 | tf_op jit(solution)/shard_map/ppermute | solution.py:43
  38.4 7.7 %collective-permute-done.4.refs_2_ = bf16[64,2048]{1,0:T(8,128)(2,1)S(1)} collective-permute-done((bf16[64,2048]{1,0:T(8,128)(2,1)S(1)}, bf16[64,2048]{1,0:T(8,128)(2,1)S(1)}, u32[]{:S(2)}, u32[]{:S(2)}) %collective-permute-start.4) | collective-permute-done | bytes 262176 | tf_op jit(solution)/shard_map/ppermute | solution.py:40
  46.1 1.5 %collective-permute-start.7 = (bf16[4,64,576]{2,1,0:T(8,128)(2,1)S(1)}, bf16[4,64,576]{2,1,0:T(8,128)(2,1)S(1)}, u32[]{:S(2)}, u32[]{:S(2)}) collective-permute-start(bf16[4,64,576]{2,1,0:T(8,128)(2,1)S(1)} %pad_maximum_fusion.1.refs_4_), channel_id=1, source_target_pairs={{0,4},{2,6},{4,0},{6,2},{8,12},{10,14},{12,8},{14,10},{16,20},{18,... | collective-permute-start | bytes 884744 | tf_op jit(solution)/shard_map/ppermute | solution.py:43
  49.8 5.6 %queries.1.q_ref = bf16[8,128,576]{2,1,0:T(8,128)(2,1)} custom-call(bf16[128,2048]{1,0:T(8,128)(2,1)S(1)} %fusion.3.normed_ref, bf16[2048,1536]{1,0:T(8,128)(2,1)} %w_ref.1, bf16[512,1024]{1,0:T(8,128)(2,1)S(1)} %copy-done.1, f32[384,32]{1,0:T(8,128)S(1)} %get-tuple-element.103.cos_ref.refs_13_, f32[384,32]{1,0:T(8,128)S(1)} %get-tuple-element.102.sin_ref.refs_14_), custom_call_target="tpu_custom_call" | custom-call | flops 805306368 | bytes 6291456 | tf_op jit(solution)/shard_map/queries/pallas_call | solution.py:314
  55.4 4.3 %collective-permute-done.7.refs_6_ = bf16[4,64,576]{2,1,0:T(8,128)(2,1)S(1)} collective-permute-done((bf16[4,64,576]{2,1,0:T(8,128)(2,1)S(1)}, bf16[4,64,576]{2,1,0:T(8,128)(2,1)S(1)}, u32[]{:S(2)}, u32[]{:S(2)}) %collective-permute-start.7) | collective-permute-done | bytes 294944 | tf_op jit(solution)/shard_map/ppermute | solution.py:43
  60.7 2.1 %collective-permute-start.22 = (bf16[4,128,512]{2,1,0:T(8,128)(2,1)S(1)}, bf16[4,128,512]{2,1,0:T(8,128)(2,1)S(1)}, u32[]{:S(2)}, u32[]{:S(2)}) collective-permute-start(bf16[4,128,512]{2,1,0:T(8,128)(2,1)S(1)} %pad_maximum_fusion.refs_8_), channel_id=1, source_target_pairs={{0,6},{2,4},{4,2},{6,0},{8,14},{10,12},{12,10},{14,8},{16,22},{18,... | collective-permute-start | bytes 1572872 | tf_op jit(solution)/shard_map/ppermute | solution.py:43
  65.2 10.3 %collective-permute-done.22.refs_11_ = bf16[4,128,512]{2,1,0:T(8,128)(2,1)S(1)} collective-permute-done((bf16[4,128,512]{2,1,0:T(8,128)(2,1)S(1)}, bf16[4,128,512]{2,1,0:T(8,128)(2,1)S(1)}, u32[]{:S(2)}, u32[]{:S(2)}) %collective-permute-start.22) | collective-permute-done | bytes 524320 | tf_op jit(solution)/shard_map/ppermute | solution.py:43
  80.4 4.6 %collective-permute-start.23 = (bf16[128,256]{1,0:T(8,128)(2,1)S(1)}, bf16[128,256]{1,0:T(8,128)(2,1)S(1)}, u32[]{:S(2)}, u32[]{:S(2)}) collective-permute-start(bf16[128,256]{1,0:T(8,128)(2,1)S(1)} %get-tuple-element.48), channel_id=1, source_target_pairs={{0,24},{2,26},{4,28},{6,30},{8,16},{10,18},{12,20},{14,22},{16,8},... | collective-permute-start | bytes 196616 | tf_op jit(solution)/shard_map/ppermute | solution.py:40
  85.2 2.1 %collective-permute-done.23 = bf16[128,256]{1,0:T(8,128)(2,1)S(1)} collective-permute-done((bf16[128,256]{1,0:T(8,128)(2,1)S(1)}, bf16[128,256]{1,0:T(8,128)(2,1)S(1)}, u32[]{:S(2)}, u32[]{:S(2)}) %collective-permute-start.23) | collective-permute-done | bytes 65568 | tf_op jit(solution)/shard_map/ppermute | solution.py:40
  88.6 1.8 %collective-permute-done.24 = bf16[128,256]{1,0:T(8,128)(2,1)S(1)} collective-permute-done((bf16[128,256]{1,0:T(8,128)(2,1)S(1)}, bf16[128,256]{1,0:T(8,128)(2,1)S(1)}, u32[]{:S(2)}, u32[]{:S(2)}) %collective-permute-start.24) | collective-permute-done | bytes 65568 | tf_op jit(solution)/shard_map/ppermute | solution.py:40
  90.8 1.8 %collective-permute-done.28.refs_2_ = bf16[256,576]{1,0:T(8,128)(2,1)} collective-permute-done((bf16[256,576]{1,0:T(8,128)(2,1)S(1)}, bf16[256,576]{1,0:T(8,128)(2,1)}, u32[]{:S(2)}, u32[]{:S(2)}) %collective-permute-start.28) | collective-permute-done | bytes 294944 | tf_op jit(solution)/shard_map/ppermute | solution.py:43
  93.4 2.5 %collective-permute-start.26 = (bf16[30,1024]{1,0:T(8,128)(2,1)S(1)}, bf16[30,1024]{1,0:T(8,128)(2,1)S(1)}, u32[]{:S(2)}, u32[]{:S(2)}) collective-permute-start(bf16[30,1024]{1,0:T(8,128)(2,1)S(1)} %slice.252), channel_id=1, source_target_pairs={{0,2},{2,4},{4,6},{6,8},{8,10},{10,12},{12,14},{14,16},{16,18},{18... | collective-permute-start | bytes 184328 | tf_op jit(solution)/shard_map/ppermute | solution.py:380
  95.9 9.4 %attention.1 = (bf16[128,1024]{1,0:T(8,128)(2,1)S(1)}, f32[8,128]{1,0:T(8,128)}) custom-call(bf16[8,128,576]{2,1,0:T(8,128)(2,1)S(1)} %copy-done, bf16[512,1024]{1,0:T(8,128)(2,1)S(1)} %copy-done.3, bf16[256,576]{1,0:T(8,128)(2,1)S(1)} %latents.1.refs_0_, bf16[256,576]{1,0:T(8,128)(2,1)S(1)} %collective-permute-done.27.refs_1_, ...), custom_call_target="tpu_custom_call" | custom-call | flops 4563402752 | bytes 2359296 | tf_op jit(solution)/shard_map/attention/pallas_call | solution.py:387
  105.6 2.9 %fusion.44 = (f32[128]{0:T(128)S(1)}, f32[128]{0:T(128)S(1)}, f32[128,1024]{1,0:T(8,128)S(1)}) fusion(f32[158,1024]{1,0:T(8,128)S(1)} %maximum_convert_fusion, f32[1024]{0:T(1024)S(1)} %bitcast.94, f32[1024]{0:T(1024)S(1)} %bitcast.95, f32[1024]{0:T(1024)S(1)} %bitcast.66, f32[1024]{0:T(1024)S(1)} %bitcast.67, f32[1024]{0:T(1024)S(1)} %bitcast.68, ...), kind=kLoop, calls=%fused_computation.151 | loop fusion | flops 8388352 | bytes 16905216 | tf_op jit(solution)/shard_map/reduce_sum | solution.py:416
  109.8 3.3 %fusion.34 = f32[128,2048]{1,0:T(8,128)S(1)} fusion(bf16[1024,2048]{1,0:T(8,128)(2,1)} %param.26, f32[128,1024]{1,0:T(8,128)S(1)} %get-tuple-element.58, f32[1024]{0:T(1024)S(1)} %copy-done.18, f32[128]{0:T(128)S(1)} %fusion.41, f32[128]{0:T(128)S(1)} %multiply_bitcast_fusion), kind=kOutput, calls=%fused_computation.76 | convolution fusion | flops 537919488 | bytes 5772288 | tf_op jit(solution)/shard_map/dot_general | solution.py:427
  (126 shorter events, 24.8 us)
Async XLA Ops:
  2.4 11.5 %collective-permute-start = (bf16[64,576]{1,0:T(8,128)(2,1)S(1)}, bf16[64,576]{1,0:T(8,128)(2,1)S(1)}, u32[]{:S(2)}, u32[]{:S(2)}) collective-permute-start(bf16[64,576]{1,0:T(8,128)(2,1)S(1)} %fusion.39), channel_id=1, source_target_pairs={{0,8},{2,10},{4,12},{6,14},{8,0},{10,2},{12,4},{14,6},{16,24},{18,... | collective-permute-start | bytes 221192 | tf_op jit(solution)/shard_map/ppermute | solution.py:40
  5.5 8.8 %collective-permute-start.1 = (bf16[64,576]{1,0:T(8,128)(2,1)S(1)}, bf16[64,576]{1,0:T(8,128)(2,1)S(1)}, u32[]{:S(2)}, u32[]{:S(2)}) collective-permute-start(bf16[64,576]{1,0:T(8,128)(2,1)S(1)} %fusion.39), channel_id=1, source_target_pairs={{0,16},{2,18},{4,20},{6,22},{8,24},{10,26},{12,28},{14,30},{16,0},... | collective-permute-start | bytes 221192 | tf_op jit(solution)/shard_map/ppermute | solution.py:40
  8.1 7.1 %collective-permute-start.2 = (bf16[64,576]{1,0:T(8,128)(2,1)S(1)}, bf16[64,576]{1,0:T(8,128)(2,1)S(1)}, u32[]{:S(2)}, u32[]{:S(2)}) collective-permute-start(bf16[64,576]{1,0:T(8,128)(2,1)S(1)} %fusion.39), channel_id=1, source_target_pairs={{0,24},{2,26},{4,28},{6,30},{8,16},{10,18},{12,20},{14,22},{16,8},... | collective-permute-start | bytes 221192 | tf_op jit(solution)/shard_map/ppermute | solution.py:40
  9.2 17.7 %collective-permute-start.9 = (bf16[128,512]{1,0:T(8,128)(2,1)S(1)}, bf16[128,512]{1,0:T(8,128)(2,1)S(1)}, u32[]{:S(2)}, u32[]{:S(2)}) collective-permute-start(bf16[128,512]{1,0:T(8,128)(2,1)S(1)} %pad_maximum_fusion.3), channel_id=1, source_target_pairs={{0,8},{2,10},{4,12},{6,14},{8,0},{10,2},{12,4},{14,6},{16,24},{18,... | collective-permute-start | bytes 393224 | tf_op jit(solution)/shard_map/ppermute | solution.py:40
  10.2 18.1 %collective-permute-start.10 = (bf16[128,512]{1,0:T(8,128)(2,1)S(1)}, bf16[128,512]{1,0:T(8,128)(2,1)S(1)}, u32[]{:S(2)}, u32[]{:S(2)}) collective-permute-start(bf16[128,512]{1,0:T(8,128)(2,1)S(1)} %pad_maximum_fusion.4), channel_id=1, source_target_pairs={{0,16},{2,18},{4,20},{6,22},{8,24},{10,26},{12,28},{14,30},{16,0},... | collective-permute-start | bytes 393224 | tf_op jit(solution)/shard_map/ppermute | solution.py:40
  14.0 14.3 %collective-permute-start.11 = (bf16[128,512]{1,0:T(8,128)(2,1)S(1)}, bf16[128,512]{1,0:T(8,128)(2,1)S(1)}, u32[]{:S(2)}, u32[]{:S(2)}) collective-permute-start(bf16[128,512]{1,0:T(8,128)(2,1)S(1)} %pad_maximum_fusion.5), channel_id=1, source_target_pairs={{0,24},{2,26},{4,28},{6,30},{8,16},{10,18},{12,20},{14,22},{16,8},... | collective-permute-start | bytes 393224 | tf_op jit(solution)/shard_map/ppermute | solution.py:40
  18.1 18.8 %collective-permute-start.3 = (bf16[64,2048]{1,0:T(8,128)(2,1)S(1)}, bf16[64,2048]{1,0:T(8,128)(2,1)S(1)}, u32[]{:S(2)}, u32[]{:S(2)}) collective-permute-start(bf16[64,2048]{1,0:T(8,128)(2,1)S(1)} %constant_dynamic-slice_fusion.9.refs_0_), channel_id=1, source_target_pairs={{0,8},{2,10},{4,12},{6,14},{8,0},{10,2},{12,4},{14,6},{16,24},{18,... | collective-permute-start | bytes 786440 | tf_op jit(solution)/shard_map/ppermute | solution.py:40
  24.8 21.3 %collective-permute-start.4 = (bf16[64,2048]{1,0:T(8,128)(2,1)S(1)}, bf16[64,2048]{1,0:T(8,128)(2,1)S(1)}, u32[]{:S(2)}, u32[]{:S(2)}) collective-permute-start(bf16[64,2048]{1,0:T(8,128)(2,1)S(1)} %constant_dynamic-slice_fusion.9.refs_0_), channel_id=1, source_target_pairs={{0,16},{2,18},{4,20},{6,22},{8,24},{10,26},{12,28},{14,30},{16,0},... | collective-permute-start | bytes 786440 | tf_op jit(solution)/shard_map/ppermute | solution.py:40
  26.9 20.7 %collective-permute-start.5 = (bf16[64,2048]{1,0:T(8,128)(2,1)S(1)}, bf16[64,2048]{1,0:T(8,128)(2,1)S(1)}, u32[]{:S(2)}, u32[]{:S(2)}) collective-permute-start(bf16[64,2048]{1,0:T(8,128)(2,1)S(1)} %constant_dynamic-slice_fusion.9.refs_0_), channel_id=1, source_target_pairs={{0,24},{2,26},{4,28},{6,30},{8,16},{10,18},{12,20},{14,22},{16,8},... | collective-permute-start | bytes 786440 | tf_op jit(solution)/shard_map/ppermute | solution.py:40
  28.4 31.8 %collective-permute-start.20 = (bf16[4,128,512]{2,1,0:T(8,128)(2,1)S(1)}, bf16[4,128,512]{2,1,0:T(8,128)(2,1)S(1)}, u32[]{:S(2)}, u32[]{:S(2)}) collective-permute-start(bf16[4,128,512]{2,1,0:T(8,128)(2,1)S(1)} %pad_maximum_fusion.refs_8_), channel_id=1, source_target_pairs={{0,2},{2,0},{4,6},{6,4},{8,10},{10,8},{12,14},{14,12},{16,18},{18,... | collective-permute-start | bytes 1572872 | tf_op jit(solution)/shard_map/ppermute | solution.py:43
  29.9 30.8 %collective-permute-start.21 = (bf16[4,128,512]{2,1,0:T(8,128)(2,1)S(1)}, bf16[4,128,512]{2,1,0:T(8,128)(2,1)S(1)}, u32[]{:S(2)}, u32[]{:S(2)}) collective-permute-start(bf16[4,128,512]{2,1,0:T(8,128)(2,1)S(1)} %pad_maximum_fusion.refs_8_), channel_id=1, source_target_pairs={{0,4},{2,6},{4,0},{6,2},{8,12},{10,14},{12,8},{14,10},{16,20},{18,... | collective-permute-start | bytes 1572872 | tf_op jit(solution)/shard_map/ppermute | solution.py:43
  36.9 18.5 %collective-permute-start.6 = (bf16[4,64,576]{2,1,0:T(8,128)(2,1)S(1)}, bf16[4,64,576]{2,1,0:T(8,128)(2,1)S(1)}, u32[]{:S(2)}, u32[]{:S(2)}) collective-permute-start(bf16[4,64,576]{2,1,0:T(8,128)(2,1)S(1)} %pad_maximum_fusion.1.refs_4_), channel_id=1, source_target_pairs={{0,2},{2,0},{4,6},{6,4},{8,10},{10,8},{12,14},{14,12},{16,18},{18,... | collective-permute-start | bytes 884744 | tf_op jit(solution)/shard_map/ppermute | solution.py:43
  46.1 13.6 %collective-permute-start.7 = (bf16[4,64,576]{2,1,0:T(8,128)(2,1)S(1)}, bf16[4,64,576]{2,1,0:T(8,128)(2,1)S(1)}, u32[]{:S(2)}, u32[]{:S(2)}) collective-permute-start(bf16[4,64,576]{2,1,0:T(8,128)(2,1)S(1)} %pad_maximum_fusion.1.refs_4_), channel_id=1, source_target_pairs={{0,4},{2,6},{4,0},{6,2},{8,12},{10,14},{12,8},{14,10},{16,20},{18,... | collective-permute-start | bytes 884744 | tf_op jit(solution)/shard_map/ppermute | solution.py:43
  47.6 12.1 %collective-permute-start.8 = (bf16[4,64,576]{2,1,0:T(8,128)(2,1)S(1)}, bf16[4,64,576]{2,1,0:T(8,128)(2,1)S(1)}, u32[]{:S(2)}, u32[]{:S(2)}) collective-permute-start(bf16[4,64,576]{2,1,0:T(8,128)(2,1)S(1)} %pad_maximum_fusion.1.refs_4_), channel_id=1, source_target_pairs={{0,6},{2,4},{4,2},{6,0},{8,14},{10,12},{12,10},{14,8},{16,22},{18,... | collective-permute-start | bytes 884744 | tf_op jit(solution)/shard_map/ppermute | solution.py:43
  60.7 14.8 %collective-permute-start.22 = (bf16[4,128,512]{2,1,0:T(8,128)(2,1)S(1)}, bf16[4,128,512]{2,1,0:T(8,128)(2,1)S(1)}, u32[]{:S(2)}, u32[]{:S(2)}) collective-permute-start(bf16[4,128,512]{2,1,0:T(8,128)(2,1)S(1)} %pad_maximum_fusion.refs_8_), channel_id=1, source_target_pairs={{0,6},{2,4},{4,2},{6,0},{8,14},{10,12},{12,10},{14,8},{16,22},{18,... | collective-permute-start | bytes 1572872 | tf_op jit(solution)/shard_map/ppermute | solution.py:43
  62.8 14.2 %collective-permute-start.12 = (bf16[64,2048]{1,0:T(8,128)(2,1)S(1)}, bf16[64,2048]{1,0:T(8,128)(2,1)S(1)}, u32[]{:S(2)}, u32[]{:S(2)}) collective-permute-start(bf16[64,2048]{1,0:T(8,128)(2,1)S(1)} %constant_dynamic-slice_fusion.9.refs_0_), channel_id=1, source_target_pairs={{0,1},{1,0},{2,3},{3,2},{4,5},{5,4},{6,7},{7,6},{8,9},{9,8},{10,11... | collective-permute-start | bytes 786440 | tf_op jit(solution)/shard_map/ppermute | solution.py:47
  62.8 15.4 %collective-permute-start.13 = (bf16[64,2048]{1,0:T(8,128)(2,1)S(1)}, bf16[64,2048]{1,0:T(8,128)(2,1)S(1)}, u32[]{:S(2)}, u32[]{:S(2)}) collective-permute-start(bf16[64,2048]{1,0:T(8,128)(2,1)S(1)} %collective-permute-done.3.refs_1_), channel_id=1, source_target_pairs={{0,1},{1,0},{2,3},{3,2},{4,5},{5,4},{6,7},{7,6},{8,9},{9,8},{10,11... | collective-permute-start | bytes 786440 | tf_op jit(solution)/shard_map/ppermute | solution.py:47
  63.3 15.7 %collective-permute-start.14 = (bf16[64,2048]{1,0:T(8,128)(2,1)S(1)}, bf16[64,2048]{1,0:T(8,128)(2,1)S(1)}, u32[]{:S(2)}, u32[]{:S(2)}) collective-permute-start(bf16[64,2048]{1,0:T(8,128)(2,1)S(1)} %collective-permute-done.4.refs_2_), channel_id=1, source_target_pairs={{0,1},{1,0},{2,3},{3,2},{4,5},{5,4},{6,7},{7,6},{8,9},{9,8},{10,11... | collective-permute-start | bytes 786440 | tf_op jit(solution)/shard_map/ppermute | solution.py:47
  63.4 15.6 %collective-permute-start.15 = (bf16[64,2048]{1,0:T(8,128)(2,1)S(1)}, bf16[64,2048]{1,0:T(8,128)(2,1)S(1)}, u32[]{:S(2)}, u32[]{:S(2)}) collective-permute-start(bf16[64,2048]{1,0:T(8,128)(2,1)S(1)} %collective-permute-done.5.refs_3_), channel_id=1, source_target_pairs={{0,1},{1,0},{2,3},{3,2},{4,5},{5,4},{6,7},{7,6},{8,9},{9,8},{10,11... | collective-permute-start | bytes 786440 | tf_op jit(solution)/shard_map/ppermute | solution.py:47
  75.5 14.8 %collective-permute-start.27 = (bf16[256,576]{1,0:T(8,128)(2,1)S(1)}, bf16[256,576]{1,0:T(8,128)(2,1)S(1)}, u32[]{:S(2)}, u32[]{:S(2)}) collective-permute-start(bf16[256,576]{1,0:T(8,128)(2,1)S(1)} %latents.1.refs_0_), channel_id=1, source_target_pairs={{0,2},{2,0},{4,6},{6,4},{8,10},{10,8},{12,14},{14,12},{16,18},{18,... | collective-permute-start | bytes 884744 | tf_op jit(solution)/shard_map/ppermute | solution.py:43
  77.0 15.7 %collective-permute-start.28 = (bf16[256,576]{1,0:T(8,128)(2,1)S(1)}, bf16[256,576]{1,0:T(8,128)(2,1)}, u32[]{:S(2)}, u32[]{:S(2)}) collective-permute-start(bf16[256,576]{1,0:T(8,128)(2,1)S(1)} %latents.1.refs_0_), channel_id=1, source_target_pairs={{0,4},{2,6},{4,0},{6,2},{8,12},{10,14},{12,8},{14,10},{16,20},{18,... | collective-permute-start | bytes 884744 | tf_op jit(solution)/shard_map/ppermute | solution.py:43
  78.2 14.5 %collective-permute-start.29 = (bf16[256,576]{1,0:T(8,128)(2,1)S(1)}, bf16[256,576]{1,0:T(8,128)(2,1)}, u32[]{:S(2)}, u32[]{:S(2)}) collective-permute-start(bf16[256,576]{1,0:T(8,128)(2,1)S(1)} %latents.1.refs_0_), channel_id=1, source_target_pairs={{0,6},{2,4},{4,2},{6,0},{8,14},{10,12},{12,10},{14,8},{16,22},{18,... | collective-permute-start | bytes 884744 | tf_op jit(solution)/shard_map/ppermute | solution.py:43
  80.4 6.8 %collective-permute-start.23 = (bf16[128,256]{1,0:T(8,128)(2,1)S(1)}, bf16[128,256]{1,0:T(8,128)(2,1)S(1)}, u32[]{:S(2)}, u32[]{:S(2)}) collective-permute-start(bf16[128,256]{1,0:T(8,128)(2,1)S(1)} %get-tuple-element.48), channel_id=1, source_target_pairs={{0,24},{2,26},{4,28},{6,30},{8,16},{10,18},{12,20},{14,22},{16,8},... | collective-permute-start | bytes 196616 | tf_op jit(solution)/shard_map/ppermute | solution.py:40
  93.4 12.0 %collective-permute-start.26 = (bf16[30,1024]{1,0:T(8,128)(2,1)S(1)}, bf16[30,1024]{1,0:T(8,128)(2,1)S(1)}, u32[]{:S(2)}, u32[]{:S(2)}) collective-permute-start(bf16[30,1024]{1,0:T(8,128)(2,1)S(1)} %slice.252), channel_id=1, source_target_pairs={{0,2},{2,4},{4,6},{6,8},{8,10},{10,12},{12,14},{14,16},{16,18},{18... | collective-permute-start | bytes 184328 | tf_op jit(solution)/shard_map/ppermute | solution.py:380
  (31 other events, 352.2 us)

commit v2 on v1

--- a/solution.py
+++ b/solution.py
@@ -179,11 +179,12 @@
         outs[j][...] = (value * jax.nn.sigmoid(gate)).astype(jnp.bfloat16)
 
 
-def attention_kernel(place, scale, rank, q_ref, up_ref, *refs):
+def attention_kernel(place, scale, rank, q_ref, up_ref, conv_ref, wc_ref, wa_ref, *refs):
     outer, inner, tp = place.outer, place.inner, place.tp_count
     n_k = tp * inner
     key_refs = refs[:n_k]
-    out_ref, lse_ref, keys = refs[n_k:]
+    out_ref, lse_ref, keys, attended, conv_weight, attn_weight, sem = refs[n_k:]
+    copies = copy_all([(wc_ref, conv_weight), (wa_ref, attn_weight)], sem)
     zi, xi, ti = place.indices()
     heads, count, depth = q_ref.shape
     piece = key_refs[0].shape[0]
@@ -224,13 +225,19 @@
             h = g * together + i
             part = slice(i * count, (i + 1) * count)
             sums.append(group_sums[part])
-            out_ref[:, h * width : (h + 1) * width] = jnp.dot(
+            attended[:, h * width : (h + 1) * width] = jnp.dot(
                 latent_out[part],
                 up_ref[:, h * width : (h + 1) * width],
                 preferred_element_type=jnp.float32,
             ).astype(jnp.bfloat16)
     spare = [jnp.zeros((count, 128 - heads), jnp.float32)]
     lse_ref[...] = jnp.concatenate(sums + spare, axis=1).T[:heads]
+    for c in copies:
+        c.wait()
+    out_ref[...] = (
+        jnp.dot(conv_ref[...], conv_weight[...], preferred_element_type=jnp.float32)
+        + jnp.dot(attended[...], attn_weight[...], preferred_element_type=jnp.float32)
+    ).astype(jnp.bfloat16)
 
 
 def local(
@@ -382,29 +389,6 @@
         "sp",
         [(i, i + 1) for i in range(place.sp_count - 1)],
     )
-    score_scale = (PLAIN_QK_WIDTH + QK_ROPE) ** (-0.5)
-    key_total = place.sp_count * row_count
-    attention, log_sums = pl.pallas_call(
-        functools.partial(attention_kernel, place, score_scale, rank),
-        out_shape=[
-            jax.ShapeDtypeStruct((row_count, head_count * VALUE_HEAD_WIDTH), bf16),
-            jax.ShapeDtypeStruct((head_count, row_count), jnp.float32),
-        ],
-        in_specs=[whole_vmem()] * (2 + len(latents)),
-        out_specs=[whole_vmem()] * 2,
-        scratch_shapes=[
-            pltpu.VMEM((key_total, rank + QK_ROPE), bf16),
-        ],
-        compiler_params=pltpu.CompilerParams(vmem_limit_bytes=32 << 20),
-        cost_estimate=pl.CostEstimate(
-            flops=2 * row_count * head_count * key_total * (2 * rank + QK_ROPE),
-            bytes_accessed=2 * key_total * (rank + QK_ROPE),
-            transcendentals=row_count * head_count * key_total,
-        ),
-        name="attention",
-    )(queries, value_up_weight, *latents)
-
-    prior_rows, gated_rows, _ = lax.optimization_barrier((prior_rows, gated_rows, attention))
     padded = jnp.concatenate([prior_rows, gated_rows], axis=0).astype(jnp.float32)
     mixed = jnp.zeros(gated_rows.shape, jnp.float32)
     for tap_index in range(conv_taps.shape[0]):
@@ -423,10 +407,35 @@
         (mixed - channel_mean[:, None]) * lax.rsqrt(channel_var + epsilon)[:, None] * conv_gain
     ).astype(bf16)
 
-    partial = (
-        jnp.dot(conv_out, w_merge_conv, preferred_element_type=jnp.float32)
-        + jnp.dot(attention, w_merge_attn, preferred_element_type=jnp.float32)
-    ).astype(bf16)
+    score_scale = (PLAIN_QK_WIDTH + QK_ROPE) ** (-0.5)
+    key_total = place.sp_count * row_count
+    out_width = w_merge_conv.shape[1]
+    partial, log_sums = pl.pallas_call(
+        functools.partial(attention_kernel, place, score_scale, rank),
+        out_shape=[
+            jax.ShapeDtypeStruct((row_count, out_width), bf16),
+            jax.ShapeDtypeStruct((head_count, row_count), jnp.float32),
+        ],
+        in_specs=[whole_vmem()] * 3
+        + [pl.BlockSpec(memory_space=pltpu.HBM)] * 2
+        + [whole_vmem()] * len(latents),
+        out_specs=[whole_vmem()] * 2,
+        scratch_shapes=[
+            pltpu.VMEM((key_total, rank + QK_ROPE), bf16),
+            pltpu.VMEM((row_count, w_merge_attn.shape[0]), bf16),
+            pltpu.VMEM(w_merge_conv.shape, bf16),
+            pltpu.VMEM(w_merge_attn.shape, bf16),
+            pltpu.SemaphoreType.DMA((2,)),
+        ],
+        compiler_params=pltpu.CompilerParams(vmem_limit_bytes=52 << 20),
+        cost_estimate=pl.CostEstimate(
+            flops=2 * row_count * head_count * key_total * (2 * rank + QK_ROPE),
+            bytes_accessed=2 * key_total * (rank + QK_ROPE),
+            transcendentals=row_count * head_count * key_total,
+        ),
+        name="attention",
+    )(queries, value_up_weight, conv_out, w_merge_conv, w_merge_attn, *latents)
+
     merged = lax.dynamic_slice_in_dim(partial, ti * share, share, 0).astype(jnp.float32)
     for t in range(1, tp_count):
         away = lax.dynamic_slice_in_dim(partial, lax.rem(ti + t, tp_count) * share, share, 0)

time: 118 us -> 135 us (1.14); the launches traced: 116 us -> 135 us
  waiting for transfers between devices: 36.8 us -> 51.5 us
  matrix products: 4.06 us -> 0 us
  starting transfers between devices: 45 us -> 48.4 us
  Pallas kernels: 17.8 us -> 20.1 us
  local copies, waits for them, and re-layouts: 2.26 us -> 4.14 us
    ppermute x9, waiting for transfers between devices: 16.4 us -> 28.2 us  [inner_swap(): lax.ppermute(block, 'sp', [(i, i ^ mask) for i in range(self.sp_count)])]
    dot_general x2 -> x0, matrix products: 4.06 us -> none  [the longest x1 3.32 us: local(): jnp.dot(conv_out, w_merge_conv, preferred_element_type=jnp.float32)]
    pallas_call x1, Pallas kernels: 9.44 us -> 11.8 us  [local(): pl.pallas_call(functools.partial(attention_kernel, place, score_scale, ra...]
    ppermute x12, starting transfers between devices: 25.7 us -> 28 us  [outer_swap(): lax.ppermute(block, 'sp', [(i, i ^ mask) for i in range(self.sp_count)])]
    ppermute x1, waiting for transfers between devices: 0.01 us -> 1.66 us  [local(): lax.ppermute(gated_rows[row_count - conv_reach:], 'sp', [(i, i + 1) for i...]
  transfers between devices with their start and end apart: 36 -> 36, of which waited for: 11 -> 16; matrix products, arithmetic and copies ran while one was open for 3% -> 2% of each run, Pallas kernels for 15% -> 5%
where the time goes in v2:
time: 135 us
  waiting for transfers between devices  51.5 us (38%)
  starting transfers between devices  48.4 us (36%)
  Pallas kernels  20.1 us (15%)
  other arithmetic  7.39 us (5%)
  local copies, waits for them, and re-layouts  4.14 us (3%)
  blocking collectives  2.39 us (2%)
    ppermute x9, waiting for transfers between devices, inner_swap(): lax.ppermute(block, 'sp', [(i, i ^ mask) for i in range(self.sp_count)])  28.2 us
    ppermute x12, starting transfers between devices, outer_swap(): lax.ppermute(block, 'sp', [(i, i ^ mask) for i in range(self.sp_count)])  28 us
    ppermute x12, waiting for transfers between devices, outer_swap(): lax.ppermute(block, 'sp', [(i, i ^ mask) for i in range(self.sp_count)])  18.9 us
    ppermute x9, starting transfers between devices, inner_swap(): lax.ppermute(block, 'sp', [(i, i ^ mask) for i in range(self.sp_count)])  14 us
    pallas_call x1, Pallas kernels, local(): pl.pallas_call(functools.partial(attention_kernel, place, score_scale, ra...  11.8 us
    pallas_call x1, Pallas kernels, local(): pl.pallas_call(functools.partial(query_kernel, rank), out_shape=jax.Shape...  5.5 us
    ppermute x1, starting transfers between devices, local(): lax.ppermute(gated_rows[row_count - conv_reach:], 'sp', [(i, i + 1) for i...  3.58 us
    reduce_sum x1, other arithmetic, local(): stats = jnp.stack([jnp.sum(mixed, axis=1), jnp.sum(mixed * mixed, axis=1)])  2.91 us
  transfers between devices with their start and end apart: 36, of which 16 were waited for; matrix products, arithmetic and copies ran while one was open for 2% of the time, Pallas kernels for 5%

profile of v2, /device:TPU:0, one launch (start us, length us, event | category | flops | bytes accessed | tf_op | source)
XLA Modules:
  0.0 134.8 jit_solution(3857288392645480267)
XLA Ops:
  2.4 3.1 %collective-permute-start.3 = (bf16[64,576]{1,0:T(8,128)(2,1)S(1)}, bf16[64,576]{1,0:T(8,128)(2,1)S(1)}, u32[]{:S(2)}, u32[]{:S(2)}) collective-permute-start(bf16[64,576]{1,0:T(8,128)(2,1)S(1)} %fusion.33), channel_id=1, source_target_pairs={{0,8},{2,10},{4,12},{6,14},{8,0},{10,2},{12,4},{14,6},{16,24},{18,... | collective-permute-start | bytes 221192 | tf_op jit(solution)/shard_map/ppermute | solution.py:40
  5.5 2.6 %collective-permute-start.4 = (bf16[64,576]{1,0:T(8,128)(2,1)S(1)}, bf16[64,576]{1,0:T(8,128)(2,1)S(1)}, u32[]{:S(2)}, u32[]{:S(2)}) collective-permute-start(bf16[64,576]{1,0:T(8,128)(2,1)S(1)} %fusion.33), channel_id=1, source_target_pairs={{0,16},{2,18},{4,20},{6,22},{8,24},{10,26},{12,28},{14,30},{16,0},... | collective-permute-start | bytes 221192 | tf_op jit(solution)/shard_map/ppermute | solution.py:40
  10.2 3.6 %collective-permute-start.1 = (bf16[128,512]{1,0:T(8,128)(2,1)S(1)}, bf16[128,512]{1,0:T(8,128)(2,1)S(1)}, u32[]{:S(2)}, u32[]{:S(2)}) collective-permute-start(bf16[128,512]{1,0:T(8,128)(2,1)S(1)} %pad_maximum_fusion.3), channel_id=1, source_target_pairs={{0,16},{2,18},{4,20},{6,22},{8,24},{10,26},{12,28},{14,30},{16,0},... | collective-permute-start | bytes 393224 | tf_op jit(solution)/shard_map/ppermute | solution.py:40
  15.3 2.4 %all_gather.3 = bf16[128,2048]{1,0:T(8,128)(2,1)S(1)} all-gather(bf16[128,1024]{1,0:T(8,128)(2,1)} %param.14), channel_id=1, replica_groups=mesh['sp'=16,'tp'=2] {'tp'}, dimensions={1}, use_global_device_ids=true | all-gather | bytes 786432 | tf_op jit(solution)/shard_map/all_gather | solution.py:292
  18.1 6.7 %collective-permute-start.6 = (bf16[64,2048]{1,0:T(8,128)(2,1)S(1)}, bf16[64,2048]{1,0:T(8,128)(2,1)S(1)}, u32[]{:S(2)}, u32[]{:S(2)}) collective-permute-start(bf16[64,2048]{1,0:T(8,128)(2,1)S(1)} %constant_dynamic-slice_fusion.1.refs_0_), channel_id=1, source_target_pairs={{0,8},{2,10},{4,12},{6,14},{8,0},{10,2},{12,4},{14,6},{16,24},{18,... | collective-permute-start | bytes 786440 | tf_op jit(solution)/shard_map/ppermute | solution.py:40
  24.8 2.1 %collective-permute-start.7 = (bf16[64,2048]{1,0:T(8,128)(2,1)S(1)}, bf16[64,2048]{1,0:T(8,128)(2,1)S(1)}, u32[]{:S(2)}, u32[]{:S(2)}) collective-permute-start(bf16[64,2048]{1,0:T(8,128)(2,1)S(1)} %constant_dynamic-slice_fusion.1.refs_0_), channel_id=1, source_target_pairs={{0,16},{2,18},{4,20},{6,22},{8,24},{10,26},{12,28},{14,30},{16,0},... | collective-permute-start | bytes 786440 | tf_op jit(solution)/shard_map/ppermute | solution.py:40
  31.5 5.5 %collective-permute-done.6.refs_1_ = bf16[64,2048]{1,0:T(8,128)(2,1)S(1)} collective-permute-done((bf16[64,2048]{1,0:T(8,128)(2,1)S(1)}, bf16[64,2048]{1,0:T(8,128)(2,1)S(1)}, u32[]{:S(2)}, u32[]{:S(2)}) %collective-permute-start.6) | collective-permute-done | bytes 262176 | tf_op jit(solution)/shard_map/ppermute | solution.py:40
  38.4 7.6 %collective-permute-done.7.refs_2_ = bf16[64,2048]{1,0:T(8,128)(2,1)S(1)} collective-permute-done((bf16[64,2048]{1,0:T(8,128)(2,1)S(1)}, bf16[64,2048]{1,0:T(8,128)(2,1)S(1)}, u32[]{:S(2)}, u32[]{:S(2)}) %collective-permute-start.7) | collective-permute-done | bytes 262176 | tf_op jit(solution)/shard_map/ppermute | solution.py:40
  46.1 2.4 %collective-permute-start.11 = (bf16[4,64,576]{2,1,0:T(8,128)(2,1)S(1)}, bf16[4,64,576]{2,1,0:T(8,128)(2,1)S(1)}, u32[]{:S(2)}, u32[]{:S(2)}) collective-permute-start(bf16[4,64,576]{2,1,0:T(8,128)(2,1)S(1)} %pad_maximum_fusion.1.refs_4_), channel_id=1, source_target_pairs={{0,6},{2,4},{4,2},{6,0},{8,14},{10,12},{12,10},{14,8},{16,22},{18,... | collective-permute-start | bytes 884744 | tf_op jit(solution)/shard_map/ppermute | solution.py:43
  49.8 5.5 %queries.1.q_ref = bf16[8,128,576]{2,1,0:T(8,128)(2,1)} custom-call(bf16[128,2048]{1,0:T(8,128)(2,1)S(1)} %fusion.2.normed_ref, bf16[2048,1536]{1,0:T(8,128)(2,1)} %w_ref.1, bf16[512,1024]{1,0:T(8,128)(2,1)S(1)} %copy-done, f32[384,32]{1,0:T(8,128)S(1)} %get-tuple-element.99.cos_ref.refs_13_, f32[384,32]{1,0:T(8,128)S(1)} %get-tuple-element.98.sin_ref.refs_14_), custom_call_target="tpu_custom_call" | custom-call | flops 805306368 | bytes 6291456 | tf_op jit(solution)/shard_map/queries/pallas_call | solution.py:321
  55.4 1.7 %collective-permute-done.10.refs_6_ = bf16[4,64,576]{2,1,0:T(8,128)(2,1)S(1)} collective-permute-done((bf16[4,64,576]{2,1,0:T(8,128)(2,1)S(1)}, bf16[4,64,576]{2,1,0:T(8,128)(2,1)S(1)}, u32[]{:S(2)}, u32[]{:S(2)}) %collective-permute-start.10) | collective-permute-done | bytes 294944 | tf_op jit(solution)/shard_map/ppermute | solution.py:43
  59.4 2.4 %collective-permute-start.22 = (bf16[4,128,512]{2,1,0:T(8,128)(2,1)S(1)}, bf16[4,128,512]{2,1,0:T(8,128)(2,1)S(1)}, u32[]{:S(2)}, u32[]{:S(2)}) collective-permute-start(bf16[4,128,512]{2,1,0:T(8,128)(2,1)S(1)} %pad_maximum_fusion.refs_8_), channel_id=1, source_target_pairs={{0,6},{2,4},{4,2},{6,0},{8,14},{10,12},{12,10},{14,8},{16,22},{18,... | collective-permute-start | bytes 1572872 | tf_op jit(solution)/shard_map/ppermute | solution.py:43
  64.2 10.0 %collective-permute-done.22.refs_11_ = bf16[4,128,512]{2,1,0:T(8,128)(2,1)S(1)} collective-permute-done((bf16[4,128,512]{2,1,0:T(8,128)(2,1)S(1)}, bf16[4,128,512]{2,1,0:T(8,128)(2,1)S(1)}, u32[]{:S(2)}, u32[]{:S(2)}) %collective-permute-start.22) | collective-permute-done | bytes 524320 | tf_op jit(solution)/shard_map/ppermute | solution.py:43
  75.6 6.9 %collective-permute-start.23 = (bf16[128,256]{1,0:T(8,128)(2,1)S(1)}, bf16[128,256]{1,0:T(8,128)(2,1)S(1)}, u32[]{:S(2)}, u32[]{:S(2)}) collective-permute-start(bf16[128,256]{1,0:T(8,128)(2,1)S(1)} %get-tuple-element.46), channel_id=1, source_target_pairs={{0,24},{2,26},{4,28},{6,30},{8,16},{10,18},{12,20},{14,22},{16,8},... | collective-permute-start | bytes 196616 | tf_op jit(solution)/shard_map/ppermute | solution.py:40
  83.3 1.7 %collective-permute-done.23 = bf16[128,256]{1,0:T(8,128)(2,1)S(1)} collective-permute-done((bf16[128,256]{1,0:T(8,128)(2,1)S(1)}, bf16[128,256]{1,0:T(8,128)(2,1)S(1)}, u32[]{:S(2)}, u32[]{:S(2)}) %collective-permute-start.23) | collective-permute-done | bytes 65568 | tf_op jit(solution)/shard_map/ppermute | solution.py:40
  84.9 2.8 %collective-permute-done.24 = bf16[128,256]{1,0:T(8,128)(2,1)S(1)} collective-permute-done((bf16[128,256]{1,0:T(8,128)(2,1)S(1)}, bf16[128,256]{1,0:T(8,128)(2,1)S(1)}, u32[]{:S(2)}, u32[]{:S(2)}) %collective-permute-start.24) | collective-permute-done | bytes 65568 | tf_op jit(solution)/shard_map/ppermute | solution.py:40
  88.0 3.6 %collective-permute-start.26 = (bf16[30,1024]{1,0:T(8,128)(2,1)S(1)}, bf16[30,1024]{1,0:T(8,128)(2,1)S(1)}, u32[]{:S(2)}, u32[]{:S(2)}) collective-permute-start(bf16[30,1024]{1,0:T(8,128)(2,1)S(1)} %pad_maximum_fusion.5), channel_id=1, source_target_pairs={{0,2},{2,4},{4,6},{6,8},{8,10},{10,12},{12,14},{14,16},{16,18},{18... | collective-permute-start | bytes 184328 | tf_op jit(solution)/shard_map/ppermute | solution.py:387
  91.6 1.7 %collective-permute-done.26 = bf16[30,1024]{1,0:T(8,128)(2,1)S(1)} collective-permute-done((bf16[30,1024]{1,0:T(8,128)(2,1)S(1)}, bf16[30,1024]{1,0:T(8,128)(2,1)S(1)}, u32[]{:S(2)}, u32[]{:S(2)}) %collective-permute-start.26) | collective-permute-done | bytes 61472 | tf_op jit(solution)/shard_map/ppermute | solution.py:387
  93.4 2.9 %fusion.37 = (f32[128]{0:T(128)S(1)}, f32[128]{0:T(128)S(1)}, f32[128,1024]{1,0:T(8,128)S(1)}) fusion(f32[158,1024]{1,0:T(8,128)S(1)} %maximum_convert_fusion, f32[1024]{0:T(1024)S(1)} %bitcast.91, f32[1024]{0:T(1024)S(1)} %bitcast.92, f32[1024]{0:T(1024)S(1)} %bitcast.63, f32[1024]{0:T(1024)S(1)} %bitcast.64, f32[1024]{0:T(1024)S(1)} %bitcast.65, ...), kind=kLoop, calls=%fused_computation.145 | loop fusion | flops 8388352 | bytes 16905216 | tf_op jit(solution)/shard_map/reduce_sum | solution.py:400
  96.4 2.4 %collective-permute-start.28 = (bf16[256,576]{1,0:T(8,128)(2,1)S(1)}, bf16[256,576]{1,0:T(8,128)(2,1)S(1)}, u32[]{:S(2)}, u32[]{:S(2)}) collective-permute-start(bf16[256,576]{1,0:T(8,128)(2,1)S(1)} %latents.1.refs_0_), channel_id=1, source_target_pairs={{0,2},{2,0},{4,6},{6,4},{8,10},{10,8},{12,14},{14,12},{16,18},{18,... | collective-permute-start | bytes 884744 | tf_op jit(solution)/shard_map/ppermute | solution.py:43
  100.4 7.0 %collective-permute-done.28.refs_1_ = bf16[256,576]{1,0:T(8,128)(2,1)S(1)} collective-permute-done((bf16[256,576]{1,0:T(8,128)(2,1)S(1)}, bf16[256,576]{1,0:T(8,128)(2,1)S(1)}, u32[]{:S(2)}, u32[]{:S(2)}) %collective-permute-start.28) | collective-permute-done | bytes 294944 | tf_op jit(solution)/shard_map/ppermute | solution.py:43
  107.4 8.2 %collective-permute-done.29.refs_2_ = bf16[256,576]{1,0:T(8,128)(2,1)S(1)} collective-permute-done((bf16[256,576]{1,0:T(8,128)(2,1)S(1)}, bf16[256,576]{1,0:T(8,128)(2,1)S(1)}, u32[]{:S(2)}, u32[]{:S(2)}) %collective-permute-start.29) | collective-permute-done | bytes 294944 | tf_op jit(solution)/shard_map/ppermute | solution.py:43
  118.7 11.8 %attention.1 = (bf16[128,2048]{1,0:T(8,128)(2,1)}, f32[8,128]{1,0:T(8,128)}) custom-call(bf16[8,128,576]{2,1,0:T(8,128)(2,1)} %queries.1.q_ref, bf16[512,1024]{1,0:T(8,128)(2,1)} %up_ref.3, bf16[128,1024]{1,0:T(8,128)(2,1)S(1)} %multiply_convert_fusion.conv_ref, bf16[1024,2048]{1,0:T(8,128)(2,1)} %wc_ref.1, bf16[1024,2048]{1,0:T(8,128)(2,1)} %wa_ref.1, ...), custom_call_target="tpu_custom_call" | custom-call | flops 4563402752 | bytes 2359296 | tf_op jit(solution)/shard_map/attention/pallas_call | solution.py:413
  133.1 1.7 %add_convert_fusion = bf16[64,2048]{1,0:T(8,128)(2,1)} fusion(bf16[64,2048]{1,0:T(8,128)(2,1)S(1)} %collective-permute-done.35, bf16[128,2048]{1,0:T(8,128)(2,1)} %get-tuple-element.50, s32[]{:T(128)S(6)} %select_n.73), kind=kLoop, calls=%fused_computation.67 | loop fusion | flops 524288 | bytes 786436 | tf_op jit(solution)/shard_map/convert_element_type | solution.py:443
  (102 shorter events, 27.6 us)
Async XLA Ops:
  2.4 11.5 %collective-permute-start.3 = (bf16[64,576]{1,0:T(8,128)(2,1)S(1)}, bf16[64,576]{1,0:T(8,128)(2,1)S(1)}, u32[]{:S(2)}, u32[]{:S(2)}) collective-permute-start(bf16[64,576]{1,0:T(8,128)(2,1)S(1)} %fusion.33), channel_id=1, source_target_pairs={{0,8},{2,10},{4,12},{6,14},{8,0},{10,2},{12,4},{14,6},{16,24},{18,... | collective-permute-start | bytes 221192 | tf_op jit(solution)/shard_map/ppermute | solution.py:40
  5.5 8.8 %collective-permute-start.4 = (bf16[64,576]{1,0:T(8,128)(2,1)S(1)}, bf16[64,576]{1,0:T(8,128)(2,1)S(1)}, u32[]{:S(2)}, u32[]{:S(2)}) collective-permute-start(bf16[64,576]{1,0:T(8,128)(2,1)S(1)} %fusion.33), channel_id=1, source_target_pairs={{0,16},{2,18},{4,20},{6,22},{8,24},{10,26},{12,28},{14,30},{16,0},... | collective-permute-start | bytes 221192 | tf_op jit(solution)/shard_map/ppermute | solution.py:40
  9.2 17.7 %collective-permute-start = (bf16[128,512]{1,0:T(8,128)(2,1)S(1)}, bf16[128,512]{1,0:T(8,128)(2,1)S(1)}, u32[]{:S(2)}, u32[]{:S(2)}) collective-permute-start(bf16[128,512]{1,0:T(8,128)(2,1)S(1)} %pad_maximum_fusion.2), channel_id=1, source_target_pairs={{0,8},{2,10},{4,12},{6,14},{8,0},{10,2},{12,4},{14,6},{16,24},{18,... | collective-permute-start | bytes 393224 | tf_op jit(solution)/shard_map/ppermute | solution.py:40
  10.2 18.1 %collective-permute-start.1 = (bf16[128,512]{1,0:T(8,128)(2,1)S(1)}, bf16[128,512]{1,0:T(8,128)(2,1)S(1)}, u32[]{:S(2)}, u32[]{:S(2)}) collective-permute-start(bf16[128,512]{1,0:T(8,128)(2,1)S(1)} %pad_maximum_fusion.3), channel_id=1, source_target_pairs={{0,16},{2,18},{4,20},{6,22},{8,24},{10,26},{12,28},{14,30},{16,0},... | collective-permute-start | bytes 393224 | tf_op jit(solution)/shard_map/ppermute | solution.py:40
  14.0 14.3 %collective-permute-start.2 = (bf16[128,512]{1,0:T(8,128)(2,1)S(1)}, bf16[128,512]{1,0:T(8,128)(2,1)S(1)}, u32[]{:S(2)}, u32[]{:S(2)}) collective-permute-start(bf16[128,512]{1,0:T(8,128)(2,1)S(1)} %pad_maximum_fusion.4), channel_id=1, source_target_pairs={{0,24},{2,26},{4,28},{6,30},{8,16},{10,18},{12,20},{14,22},{16,8},... | collective-permute-start | bytes 393224 | tf_op jit(solution)/shard_map/ppermute | solution.py:40
  18.1 18.8 %collective-permute-start.6 = (bf16[64,2048]{1,0:T(8,128)(2,1)S(1)}, bf16[64,2048]{1,0:T(8,128)(2,1)S(1)}, u32[]{:S(2)}, u32[]{:S(2)}) collective-permute-start(bf16[64,2048]{1,0:T(8,128)(2,1)S(1)} %constant_dynamic-slice_fusion.1.refs_0_), channel_id=1, source_target_pairs={{0,8},{2,10},{4,12},{6,14},{8,0},{10,2},{12,4},{14,6},{16,24},{18,... | collective-permute-start | bytes 786440 | tf_op jit(solution)/shard_map/ppermute | solution.py:40
  24.8 21.3 %collective-permute-start.7 = (bf16[64,2048]{1,0:T(8,128)(2,1)S(1)}, bf16[64,2048]{1,0:T(8,128)(2,1)S(1)}, u32[]{:S(2)}, u32[]{:S(2)}) collective-permute-start(bf16[64,2048]{1,0:T(8,128)(2,1)S(1)} %constant_dynamic-slice_fusion.1.refs_0_), channel_id=1, source_target_pairs={{0,16},{2,18},{4,20},{6,22},{8,24},{10,26},{12,28},{14,30},{16,0},... | collective-permute-start | bytes 786440 | tf_op jit(solution)/shard_map/ppermute | solution.py:40
  26.9 21.6 %collective-permute-start.8 = (bf16[64,2048]{1,0:T(8,128)(2,1)S(1)}, bf16[64,2048]{1,0:T(8,128)(2,1)S(1)}, u32[]{:S(2)}, u32[]{:S(2)}) collective-permute-start(bf16[64,2048]{1,0:T(8,128)(2,1)S(1)} %constant_dynamic-slice_fusion.1.refs_0_), channel_id=1, source_target_pairs={{0,24},{2,26},{4,28},{6,30},{8,16},{10,18},{12,20},{14,22},{16,8},... | collective-permute-start | bytes 786440 | tf_op jit(solution)/shard_map/ppermute | solution.py:40
  28.4 30.5 %collective-permute-start.20 = (bf16[4,128,512]{2,1,0:T(8,128)(2,1)S(1)}, bf16[4,128,512]{2,1,0:T(8,128)(2,1)S(1)}, u32[]{:S(2)}, u32[]{:S(2)}) collective-permute-start(bf16[4,128,512]{2,1,0:T(8,128)(2,1)S(1)} %pad_maximum_fusion.refs_8_), channel_id=1, source_target_pairs={{0,2},{2,0},{4,6},{6,4},{8,10},{10,8},{12,14},{14,12},{16,18},{18,... | collective-permute-start | bytes 1572872 | tf_op jit(solution)/shard_map/ppermute | solution.py:43
  29.9 29.4 %collective-permute-start.21 = (bf16[4,128,512]{2,1,0:T(8,128)(2,1)S(1)}, bf16[4,128,512]{2,1,0:T(8,128)(2,1)S(1)}, u32[]{:S(2)}, u32[]{:S(2)}) collective-permute-start(bf16[4,128,512]{2,1,0:T(8,128)(2,1)S(1)} %pad_maximum_fusion.refs_8_), channel_id=1, source_target_pairs={{0,4},{2,6},{4,0},{6,2},{8,12},{10,14},{12,8},{14,10},{16,20},{18,... | collective-permute-start | bytes 1572872 | tf_op jit(solution)/shard_map/ppermute | solution.py:43
  36.9 20.2 %collective-permute-start.10 = (bf16[4,64,576]{2,1,0:T(8,128)(2,1)S(1)}, bf16[4,64,576]{2,1,0:T(8,128)(2,1)S(1)}, u32[]{:S(2)}, u32[]{:S(2)}) collective-permute-start(bf16[4,64,576]{2,1,0:T(8,128)(2,1)S(1)} %pad_maximum_fusion.1.refs_4_), channel_id=1, source_target_pairs={{0,4},{2,6},{4,0},{6,2},{8,12},{10,14},{12,8},{14,10},{16,20},{18,... | collective-permute-start | bytes 884744 | tf_op jit(solution)/shard_map/ppermute | solution.py:43
  46.1 11.0 %collective-permute-start.11 = (bf16[4,64,576]{2,1,0:T(8,128)(2,1)S(1)}, bf16[4,64,576]{2,1,0:T(8,128)(2,1)S(1)}, u32[]{:S(2)}, u32[]{:S(2)}) collective-permute-start(bf16[4,64,576]{2,1,0:T(8,128)(2,1)S(1)} %pad_maximum_fusion.1.refs_4_), channel_id=1, source_target_pairs={{0,6},{2,4},{4,2},{6,0},{8,14},{10,12},{12,10},{14,8},{16,22},{18,... | collective-permute-start | bytes 884744 | tf_op jit(solution)/shard_map/ppermute | solution.py:43
  48.5 9.8 %collective-permute-start.9 = (bf16[4,64,576]{2,1,0:T(8,128)(2,1)S(1)}, bf16[4,64,576]{2,1,0:T(8,128)(2,1)S(1)}, u32[]{:S(2)}, u32[]{:S(2)}) collective-permute-start(bf16[4,64,576]{2,1,0:T(8,128)(2,1)S(1)} %pad_maximum_fusion.1.refs_4_), channel_id=1, source_target_pairs={{0,2},{2,0},{4,6},{6,4},{8,10},{10,8},{12,14},{14,12},{16,18},{18,... | collective-permute-start | bytes 884744 | tf_op jit(solution)/shard_map/ppermute | solution.py:43
  59.4 14.8 %collective-permute-start.22 = (bf16[4,128,512]{2,1,0:T(8,128)(2,1)S(1)}, bf16[4,128,512]{2,1,0:T(8,128)(2,1)S(1)}, u32[]{:S(2)}, u32[]{:S(2)}) collective-permute-start(bf16[4,128,512]{2,1,0:T(8,128)(2,1)S(1)} %pad_maximum_fusion.refs_8_), channel_id=1, source_target_pairs={{0,6},{2,4},{4,2},{6,0},{8,14},{10,12},{12,10},{14,8},{16,22},{18,... | collective-permute-start | bytes 1572872 | tf_op jit(solution)/shard_map/ppermute | solution.py:43
  61.8 12.4 %collective-permute-start.12 = (bf16[64,2048]{1,0:T(8,128)(2,1)S(1)}, bf16[64,2048]{1,0:T(8,128)(2,1)S(1)}, u32[]{:S(2)}, u32[]{:S(2)}) collective-permute-start(bf16[64,2048]{1,0:T(8,128)(2,1)S(1)} %constant_dynamic-slice_fusion.1.refs_0_), channel_id=1, source_target_pairs={{0,1},{1,0},{2,3},{3,2},{4,5},{5,4},{6,7},{7,6},{8,9},{9,8},{10,11... | collective-permute-start | bytes 786440 | tf_op jit(solution)/shard_map/ppermute | solution.py:47
  61.8 12.3 %collective-permute-start.13 = (bf16[64,2048]{1,0:T(8,128)(2,1)S(1)}, bf16[64,2048]{1,0:T(8,128)(2,1)S(1)}, u32[]{:S(2)}, u32[]{:S(2)}) collective-permute-start(bf16[64,2048]{1,0:T(8,128)(2,1)S(1)} %collective-permute-done.6.refs_1_), channel_id=1, source_target_pairs={{0,1},{1,0},{2,3},{3,2},{4,5},{5,4},{6,7},{7,6},{8,9},{9,8},{10,11... | collective-permute-start | bytes 786440 | tf_op jit(solution)/shard_map/ppermute | solution.py:47
  62.3 11.8 %collective-permute-start.14 = (bf16[64,2048]{1,0:T(8,128)(2,1)S(1)}, bf16[64,2048]{1,0:T(8,128)(2,1)S(1)}, u32[]{:S(2)}, u32[]{:S(2)}) collective-permute-start(bf16[64,2048]{1,0:T(8,128)(2,1)S(1)} %collective-permute-done.7.refs_2_), channel_id=1, source_target_pairs={{0,1},{1,0},{2,3},{3,2},{4,5},{5,4},{6,7},{7,6},{8,9},{9,8},{10,11... | collective-permute-start | bytes 786440 | tf_op jit(solution)/shard_map/ppermute | solution.py:47
  62.4 11.8 %collective-permute-start.15 = (bf16[64,2048]{1,0:T(8,128)(2,1)S(1)}, bf16[64,2048]{1,0:T(8,128)(2,1)S(1)}, u32[]{:S(2)}, u32[]{:S(2)}) collective-permute-start(bf16[64,2048]{1,0:T(8,128)(2,1)S(1)} %collective-permute-done.8.refs_3_), channel_id=1, source_target_pairs={{0,1},{1,0},{2,3},{3,2},{4,5},{5,4},{6,7},{7,6},{8,9},{9,8},{10,11... | collective-permute-start | bytes 786440 | tf_op jit(solution)/shard_map/ppermute | solution.py:47
  75.6 9.3 %collective-permute-start.23 = (bf16[128,256]{1,0:T(8,128)(2,1)S(1)}, bf16[128,256]{1,0:T(8,128)(2,1)S(1)}, u32[]{:S(2)}, u32[]{:S(2)}) collective-permute-start(bf16[128,256]{1,0:T(8,128)(2,1)S(1)} %get-tuple-element.46), channel_id=1, source_target_pairs={{0,24},{2,26},{4,28},{6,30},{8,16},{10,18},{12,20},{14,22},{16,8},... | collective-permute-start | bytes 196616 | tf_op jit(solution)/shard_map/ppermute | solution.py:40
  96.4 11.0 %collective-permute-start.28 = (bf16[256,576]{1,0:T(8,128)(2,1)S(1)}, bf16[256,576]{1,0:T(8,128)(2,1)S(1)}, u32[]{:S(2)}, u32[]{:S(2)}) collective-permute-start(bf16[256,576]{1,0:T(8,128)(2,1)S(1)} %latents.1.refs_0_), channel_id=1, source_target_pairs={{0,2},{2,0},{4,6},{6,4},{8,10},{10,8},{12,14},{14,12},{16,18},{18,... | collective-permute-start | bytes 884744 | tf_op jit(solution)/shard_map/ppermute | solution.py:43
  98.8 16.8 %collective-permute-start.29 = (bf16[256,576]{1,0:T(8,128)(2,1)S(1)}, bf16[256,576]{1,0:T(8,128)(2,1)S(1)}, u32[]{:S(2)}, u32[]{:S(2)}) collective-permute-start(bf16[256,576]{1,0:T(8,128)(2,1)S(1)} %latents.1.refs_0_), channel_id=1, source_target_pairs={{0,4},{2,6},{4,0},{6,2},{8,12},{10,14},{12,8},{14,10},{16,20},{18,... | collective-permute-start | bytes 884744 | tf_op jit(solution)/shard_map/ppermute | solution.py:43
  99.4 16.3 %collective-permute-start.30 = (bf16[256,576]{1,0:T(8,128)(2,1)S(1)}, bf16[256,576]{1,0:T(8,128)(2,1)S(1)}, u32[]{:S(2)}, u32[]{:S(2)}) collective-permute-start(bf16[256,576]{1,0:T(8,128)(2,1)S(1)} %latents.1.refs_0_), channel_id=1, source_target_pairs={{0,6},{2,4},{4,2},{6,0},{8,14},{10,12},{12,10},{14,8},{16,22},{18,... | collective-permute-start | bytes 884744 | tf_op jit(solution)/shard_map/ppermute | solution.py:43
  100.4 16.0 %collective-permute-start.31 = (bf16[256,576]{1,0:T(8,128)(2,1)S(1)}, bf16[256,576]{1,0:T(8,128)(2,1)S(1)}, u32[]{:S(2)}, u32[]{:S(2)}) collective-permute-start(bf16[256,576]{1,0:T(8,128)(2,1)S(1)} %latents.1.refs_0_), channel_id=1, source_target_pairs={{0,1},{1,0},{2,3},{3,2},{4,5},{5,4},{6,7},{7,6},{8,9},{9,8},{10,11... | collective-permute-start | bytes 884744 | tf_op jit(solution)/shard_map/ppermute | solution.py:47
  107.4 9.0 %collective-permute-start.32 = (bf16[256,576]{1,0:T(8,128)(2,1)S(1)}, bf16[256,576]{1,0:T(8,128)(2,1)S(1)}, u32[]{:S(2)}, u32[]{:S(2)}) collective-permute-start(bf16[256,576]{1,0:T(8,128)(2,1)S(1)} %collective-permute-done.28.refs_1_), channel_id=1, source_target_pairs={{0,1},{1,0},{2,3},{3,2},{4,5},{5,4},{6,7},{7,6},{8,9},{9,8},{10,11... | collective-permute-start | bytes 884744 | tf_op jit(solution)/shard_map/ppermute | solution.py:47
  (20 other events, 171.7 us)

commit v3 on v2

--- a/solution.py
+++ b/solution.py
@@ -48,6 +48,13 @@
 
     def outer_gather(self, block):
         return [block] + [self.outer_swap(block, j) for j in range(1, self.outer)]
+
+    def outer_forward(self, block):
+        blocks = [block]
+        for j in range(1, self.outer):
+            near = j & -j
+            blocks.append(self.outer_swap(blocks[j ^ near], near))
+        return blocks
 
     def inner_gather(self, block):
         return [block] + [self.inner_swap(block, k) for k in range(1, self.inner)]
@@ -179,12 +186,11 @@
         outs[j][...] = (value * jax.nn.sigmoid(gate)).astype(jnp.bfloat16)
 
 
-def attention_kernel(place, scale, rank, q_ref, up_ref, conv_ref, wc_ref, wa_ref, *refs):
+def attention_kernel(place, scale, rank, q_ref, up_ref, *refs):
     outer, inner, tp = place.outer, place.inner, place.tp_count
     n_k = tp * inner
     key_refs = refs[:n_k]
-    out_ref, lse_ref, keys, attended, conv_weight, attn_weight, sem = refs[n_k:]
-    copies = copy_all([(wc_ref, conv_weight), (wa_ref, attn_weight)], sem)
+    out_ref, lse_ref, keys = refs[n_k:]
     zi, xi, ti = place.indices()
     heads, count, depth = q_ref.shape
     piece = key_refs[0].shape[0]
@@ -225,19 +231,13 @@
             h = g * together + i
             part = slice(i * count, (i + 1) * count)
             sums.append(group_sums[part])
-            attended[:, h * width : (h + 1) * width] = jnp.dot(
+            out_ref[:, h * width : (h + 1) * width] = jnp.dot(
                 latent_out[part],
                 up_ref[:, h * width : (h + 1) * width],
                 preferred_element_type=jnp.float32,
             ).astype(jnp.bfloat16)
     spare = [jnp.zeros((count, 128 - heads), jnp.float32)]
     lse_ref[...] = jnp.concatenate(sums + spare, axis=1).T[:heads]
-    for c in copies:
-        c.wait()
-    out_ref[...] = (
-        jnp.dot(conv_ref[...], conv_weight[...], preferred_element_type=jnp.float32)
-        + jnp.dot(attended[...], attn_weight[...], preferred_element_type=jnp.float32)
-    ).astype(jnp.bfloat16)
 
 
 def local(
@@ -264,14 +264,6 @@
     depth = latent_down_weight.shape[0]
     rank = latent_down_weight.shape[1]
 
-    split_rows = depth % (16 * tp_count) == 0
-    own_table = jnp.concatenate([latent_down_weight, w_rope_key], axis=1)
-    if split_rows:
-        piece = depth // tp_count
-        own_table = lax.dynamic_slice_in_dim(own_table, ti * piece, piece, 0)
-    own_table, w_value, w_gate = lax.optimization_barrier((own_table, w_value, w_gate))
-    table_parts = place.outer_gather(own_table)
-
     width = w_value.shape[1] // outer
     columns = []
     for j in range(outer):
@@ -285,9 +277,15 @@
         )
         columns.append(block if j == 0 else place.outer_swap(block, j))
 
-    table = jnp.stack(table_parts)
-    table, tokens = lax.optimization_barrier((table, tokens))
-    tables = place.inner_gather(table)
+    split_rows = depth % (16 * tp_count) == 0
+    own_table = jnp.concatenate([latent_down_weight, w_rope_key], axis=1)
+    if split_rows:
+        piece = depth // tp_count
+        own_table = lax.dynamic_slice_in_dim(own_table, ti * piece, piece, 0)
+    table_parts = place.outer_gather(own_table)
+
+    weight_blocks = place.inner_gather(jnp.stack(columns))
+    tables = place.inner_gather(jnp.stack(table_parts))
 
     gathered = lax.all_gather(tokens, "tp", axis=1, tiled=True)
     features = gathered.astype(jnp.float32)
@@ -298,10 +296,7 @@
     ).astype(jnp.bfloat16)
 
     own_rows = lax.dynamic_slice_in_dim(normed, ti * share, share, 0)
-    rows = place.outer_gather(own_rows)
-    weight_block = jnp.stack(columns)
-    weight_block, query_rows = lax.optimization_barrier((weight_block, normed))
-    weight_blocks = place.inner_gather(weight_block)
+    rows = place.outer_forward(own_rows)
 
     bf16 = jnp.bfloat16
     model = normed.shape[1]
@@ -335,33 +330,9 @@
             transcendentals=0,
         ),
         name="queries",
-    )(query_rows, w_query, key_up_weight, cosine, sine)
-
-    rows, tables, _ = lax.optimization_barrier((rows, tables, queries))
-    if split_rows:
-        tables = sum(place.tp_gather(tables), [])
-
-    latent = pl.pallas_call(
-        functools.partial(latent_kernel, place, rank, split_rows),
-        out_shape=jax.ShapeDtypeStruct((outer * share, rank + QK_ROPE), bf16),
-        in_specs=[whole_vmem()] * (outer + len(tables) + 3),
-        out_specs=whole_vmem(),
-        scratch_shapes=[
-            pltpu.VMEM((outer * share, model), bf16),
-            pltpu.VMEM((model, rank + QK_ROPE), bf16),
-        ],
-        compiler_params=pltpu.CompilerParams(vmem_limit_bytes=16 << 20),
-        cost_estimate=pl.CostEstimate(
-            flops=2 * outer * share * model * (rank + QK_ROPE),
-            bytes_accessed=2 * model * (rank + QK_ROPE + outer * share),
-            transcendentals=0,
-        ),
-        name="latents",
-    )(*rows, *tables, latent_norm_gain[None, :], cosine, sine)
-    _, *weight_blocks = lax.optimization_barrier((latent, *weight_blocks))
-    latents = place.inner_gather(latent)
-    latents = sum(place.tp_gather(latents), [])
-
+    )(normed, w_query, key_up_weight, cosine, sine)
+
+    rows, _ = lax.optimization_barrier((rows, queries))
     all_rows = sum(place.tp_gather(rows), [])
     gated = pl.pallas_call(
         functools.partial(gated_kernel, place),
@@ -381,8 +352,29 @@
         name="gated",
     )(*all_rows, *weight_blocks)
     home = [gated[0]] + [place.outer_swap(gated[j], j) for j in range(1, outer)]
+    if split_rows:
+        tables = sum(place.tp_gather(tables), [])
+
+    latent = pl.pallas_call(
+        functools.partial(latent_kernel, place, rank, split_rows),
+        out_shape=jax.ShapeDtypeStruct((outer * share, rank + QK_ROPE), bf16),
+        in_specs=[whole_vmem()] * (outer + len(tables) + 3),
+        out_specs=whole_vmem(),
+        scratch_shapes=[
+            pltpu.VMEM((outer * share, model), bf16),
+            pltpu.VMEM((model, rank + QK_ROPE), bf16),
+        ],
+        compiler_params=pltpu.CompilerParams(vmem_limit_bytes=16 << 20),
+        cost_estimate=pl.CostEstimate(
+            flops=2 * outer * share * model * (rank + QK_ROPE),
+            bytes_accessed=2 * model * (rank + QK_ROPE + outer * share),
+            transcendentals=0,
+        ),
+        name="latents",
+    )(*rows, *tables, latent_norm_gain[None, :], cosine, sine)
+    latents = place.inner_gather(latent)
+    home, _ = lax.optimization_barrier((home, latent))
     gated_rows = jnp.concatenate(untangled(home, zi), axis=1)
-
     conv_reach = conv_taps.shape[0] - 1
     prior_rows = lax.ppermute(
         gated_rows[row_count - conv_reach :],
@@ -407,35 +399,35 @@
         (mixed - channel_mean[:, None]) * lax.rsqrt(channel_var + epsilon)[:, None] * conv_gain
     ).astype(bf16)
 
+    conv_part = jnp.dot(conv_out, w_merge_conv, preferred_element_type=jnp.float32)
+    latents, queries, _ = lax.optimization_barrier((latents, queries, conv_part))
+    latents = sum(place.tp_gather(latents), [])
+
     score_scale = (PLAIN_QK_WIDTH + QK_ROPE) ** (-0.5)
     key_total = place.sp_count * row_count
-    out_width = w_merge_conv.shape[1]
-    partial, log_sums = pl.pallas_call(
+    attention, log_sums = pl.pallas_call(
         functools.partial(attention_kernel, place, score_scale, rank),
         out_shape=[
-            jax.ShapeDtypeStruct((row_count, out_width), bf16),
+            jax.ShapeDtypeStruct((row_count, head_count * VALUE_HEAD_WIDTH), bf16),
             jax.ShapeDtypeStruct((head_count, row_count), jnp.float32),
         ],
-        in_specs=[whole_vmem()] * 3
-        + [pl.BlockSpec(memory_space=pltpu.HBM)] * 2
-        + [whole_vmem()] * len(latents),
+        in_specs=[whole_vmem()] * (2 + len(latents)),
         out_specs=[whole_vmem()] * 2,
         scratch_shapes=[
             pltpu.VMEM((key_total, rank + QK_ROPE), bf16),
-            pltpu.VMEM((row_count, w_merge_attn.shape[0]), bf16),
-            pltpu.VMEM(w_merge_conv.shape, bf16),
-            pltpu.VMEM(w_merge_attn.shape, bf16),
-            pltpu.SemaphoreType.DMA((2,)),
         ],
-        compiler_params=pltpu.CompilerParams(vmem_limit_bytes=52 << 20),
+        compiler_params=pltpu.CompilerParams(vmem_limit_bytes=32 << 20),
         cost_estimate=pl.CostEstimate(
             flops=2 * row_count * head_count * key_total * (2 * rank + QK_ROPE),
             bytes_accessed=2 * key_total * (rank + QK_ROPE),
             transcendentals=row_count * head_count * key_total,
         ),
         name="attention",
-    )(queries, value_up_weight, conv_out, w_merge_conv, w_merge_attn, *latents)
-
+    )(queries, value_up_weight, *latents)
+
+    partial = (
+        conv_part + jnp.dot(attention, w_merge_attn, preferred_element_type=jnp.float32)
+    ).astype(bf16)
     merged = lax.dynamic_slice_in_dim(partial, ti * share, share, 0).astype(jnp.float32)
     for t in range(1, tp_count):
         away = lax.dynamic_slice_in_dim(partial, lax.rem(ti + t, tp_count) * share, share, 0)

time: 135 us -> 137 us (1.015)
  starting transfers between devices: 48.4 us -> 40.4 us
  waiting for transfers between devices: 51.5 us -> 57.5 us
  matrix products: 0 us -> 2.6 us
  other arithmetic: 7.39 us -> 9.33 us
    ppermute x9, waiting for transfers between devices: 28.2 us -> 38.6 us  [inner_swap(): lax.ppermute(block, 'sp', [(i, i ^ mask) for i in range(self.sp_count)])]
    ppermute x12, starting transfers between devices: 28 us -> 20.1 us  [outer_swap(): lax.ppermute(block, 'sp', [(i, i ^ mask) for i in range(self.sp_count)])]
    ppermute x12, waiting for transfers between devices: 18.9 us -> 12.6 us  [outer_swap(): lax.ppermute(block, 'sp', [(i, i ^ mask) for i in range(self.sp_count)])]
    dot_general x0 -> x2, matrix products: none -> 2.6 us  [the longest x1 1.87 us: local(): jnp.dot(conv_out, w_merge_conv, preferred_element_type=jnp.float32)]
    pallas_call x1, Pallas kernels: 11.8 us -> 9.7 us  [local(): pl.pallas_call(functools.partial(attention_kernel, place, score_scale, ra...]
    ppermute x14, waiting for transfers between devices: 2.73 us -> 4.67 us  [tp_shift(): return lax.ppermute(block, 'tp', route)]
  transfers between devices with their start and end apart: 36 -> 36, of which waited for: 16 -> 19; matrix products, arithmetic and copies ran while one was open for 2% -> 5% of each run, Pallas kernels for 5% -> 7%
where the time goes in v3:
time: 137 us; the launch traced here: 136 us
  waiting for transfers between devices  57.5 us (42%)
  starting transfers between devices  40.4 us (29%)
  Pallas kernels  19.1 us (14%)
  other arithmetic  9.33 us (7%)
  local copies, waits for them, and re-layouts  3.9 us (3%)
  matrix products  2.6 us (2%)
  blocking collectives  2.38 us (2%)
    ppermute x9, waiting for transfers between devices, inner_swap(): lax.ppermute(block, 'sp', [(i, i ^ mask) for i in range(self.sp_count)])  38.6 us
    ppermute x12, starting transfers between devices, outer_swap(): lax.ppermute(block, 'sp', [(i, i ^ mask) for i in range(self.sp_count)])  20.1 us
    ppermute x9, starting transfers between devices, inner_swap(): lax.ppermute(block, 'sp', [(i, i ^ mask) for i in range(self.sp_count)])  14.6 us
    ppermute x12, waiting for transfers between devices, outer_swap(): lax.ppermute(block, 'sp', [(i, i ^ mask) for i in range(self.sp_count)])  12.6 us
    pallas_call x1, Pallas kernels, local(): pl.pallas_call(functools.partial(attention_kernel, place, score_scale, ra...  9.7 us
    pallas_call x1, Pallas kernels, local(): pl.pallas_call(functools.partial(query_kernel, rank), out_shape=jax.Shape...  5.5 us
    ppermute x14, waiting for transfers between devices, tp_shift(): return lax.ppermute(block, 'tp', route)  4.67 us
    ppermute x1, starting transfers between devices, local(): lax.ppermute(gated_rows[row_count - conv_reach:], 'sp', [(i, i + 1) for i...  2.96 us
  transfers between devices with their start and end apart: 36, of which 19 were waited for; matrix products, arithmetic and copies ran while one was open for 5% of the time, Pallas kernels for 7%

profile of v3, /device:TPU:0, one launch (start us, length us, event | category | flops | bytes accessed | tf_op | source)
XLA Modules:
  0.0 136.3 jit_solution(10776203152090793357)
XLA Ops:
  2.4 3.1 %collective-permute-start.16 = (bf16[64,576]{1,0:T(8,128)(2,1)S(1)}, bf16[64,576]{1,0:T(8,128)(2,1)S(1)}, u32[]{:S(2)}, u32[]{:S(2)}) collective-permute-start(bf16[64,576]{1,0:T(8,128)(2,1)S(1)} %fusion.39), channel_id=1, source_target_pairs={{0,8},{2,10},{4,12},{6,14},{8,0},{10,2},{12,4},{14,6},{16,24},{18,... | collective-permute-start | bytes 221192 | tf_op jit(solution)/shard_map/ppermute | solution.py:40
  5.5 2.6 %collective-permute-start.17 = (bf16[64,576]{1,0:T(8,128)(2,1)S(1)}, bf16[64,576]{1,0:T(8,128)(2,1)S(1)}, u32[]{:S(2)}, u32[]{:S(2)}) collective-permute-start(bf16[64,576]{1,0:T(8,128)(2,1)S(1)} %fusion.39), channel_id=1, source_target_pairs={{0,16},{2,18},{4,20},{6,22},{8,24},{10,26},{12,28},{14,30},{16,0},... | collective-permute-start | bytes 221192 | tf_op jit(solution)/shard_map/ppermute | solution.py:40
  8.1 2.4 %all_gather.3 = bf16[128,2048]{1,0:T(8,128)(2,1)S(1)} all-gather(bf16[128,1024]{1,0:T(8,128)(2,1)} %param.14), channel_id=1, replica_groups=mesh['sp'=16,'tp'=2] {'tp'}, dimensions={1}, use_global_device_ids=true | all-gather | bytes 786432 | tf_op jit(solution)/shard_map/all_gather | solution.py:290
  11.6 2.0 %collective-permute-start.1 = (bf16[64,2048]{1,0:T(8,128)(2,1)S(1)}, bf16[64,2048]{1,0:T(8,128)(2,1)S(1)}, u32[]{:S(2)}, u32[]{:S(2)}) collective-permute-start(bf16[64,2048]{1,0:T(8,128)(2,1)S(1)} %constant_dynamic-slice_fusion.9.refs_0_), channel_id=1, source_target_pairs={{0,16},{2,18},{4,20},{6,22},{8,24},{10,26},{12,28},{14,30},{16,0},... | collective-permute-start | bytes 786440 | tf_op jit(solution)/shard_map/ppermute | solution.py:40
  14.7 2.5 %collective-permute-start.7 = (bf16[128,512]{1,0:T(8,128)(2,1)S(1)}, bf16[128,512]{1,0:T(8,128)(2,1)S(1)}, u32[]{:S(2)}, u32[]{:S(2)}) collective-permute-start(bf16[128,512]{1,0:T(8,128)(2,1)S(1)} %pad_maximum_fusion.2), channel_id=1, source_target_pairs={{0,8},{2,10},{4,12},{6,14},{8,0},{10,2},{12,4},{14,6},{16,24},{18,... | collective-permute-start | bytes 393224 | tf_op jit(solution)/shard_map/ppermute | solution.py:40
  18.7 3.8 %collective-permute-start.9 = (bf16[128,512]{1,0:T(8,128)(2,1)S(1)}, bf16[128,512]{1,0:T(8,128)(2,1)S(1)}, u32[]{:S(2)}, u32[]{:S(2)}) collective-permute-start(bf16[128,512]{1,0:T(8,128)(2,1)S(1)} %pad_maximum_fusion.4), channel_id=1, source_target_pairs={{0,24},{2,26},{4,28},{6,30},{8,16},{10,18},{12,20},{14,22},{16,8},... | collective-permute-start | bytes 393224 | tf_op jit(solution)/shard_map/ppermute | solution.py:40
  25.1 2.4 %collective-permute-done.1.refs_2_ = bf16[64,2048]{1,0:T(8,128)(2,1)S(1)} collective-permute-done((bf16[64,2048]{1,0:T(8,128)(2,1)S(1)}, bf16[64,2048]{1,0:T(8,128)(2,1)S(1)}, u32[]{:S(2)}, u32[]{:S(2)}) %collective-permute-start.1) | collective-permute-done | bytes 262176 | tf_op jit(solution)/shard_map/ppermute | solution.py:40
  27.4 4.2 %collective-permute-done.8 = bf16[128,512]{1,0:T(8,128)(2,1)S(1)} collective-permute-done((bf16[128,512]{1,0:T(8,128)(2,1)}, bf16[128,512]{1,0:T(8,128)(2,1)S(1)}, u32[]{:S(2)}, u32[]{:S(2)}) %collective-permute-start.8) | collective-permute-done | bytes 131104 | tf_op jit(solution)/shard_map/ppermute | solution.py:40
  31.7 5.1 %collective-permute-done.9 = bf16[128,512]{1,0:T(8,128)(2,1)S(1)} collective-permute-done((bf16[128,512]{1,0:T(8,128)(2,1)S(1)}, bf16[128,512]{1,0:T(8,128)(2,1)S(1)}, u32[]{:S(2)}, u32[]{:S(2)}) %collective-permute-start.9) | collective-permute-done | bytes 131104 | tf_op jit(solution)/shard_map/ppermute | solution.py:40
  42.2 2.4 %collective-permute-start.12 = (bf16[4,128,512]{2,1,0:T(8,128)(2,1)S(1)}, bf16[4,128,512]{2,1,0:T(8,128)(2,1)S(1)}, u32[]{:S(2)}, u32[]{:S(2)}) collective-permute-start(bf16[4,128,512]{2,1,0:T(8,128)(2,1)S(1)} %pad_maximum_fusion.refs_8_), channel_id=1, source_target_pairs={{0,6},{2,4},{4,2},{6,0},{8,14},{10,12},{12,10},{14,8},{16,22},{18,... | collective-permute-start | bytes 1572872 | tf_op jit(solution)/shard_map/ppermute | solution.py:43
  45.4 5.5 %queries.1.q_ref = bf16[8,128,576]{2,1,0:T(8,128)(2,1)} custom-call(bf16[128,2048]{1,0:T(8,128)(2,1)S(1)} %fusion.3.normed_ref, bf16[2048,1536]{1,0:T(8,128)(2,1)} %w_ref.1, bf16[512,1024]{1,0:T(8,128)(2,1)S(1)} %copy-done.1, f32[384,32]{1,0:T(8,128)S(1)} %get-tuple-element.87.cos_ref.refs_13_, f32[384,32]{1,0:T(8,128)S(1)} %get-tuple-element.86.sin_ref.refs_14_), custom_call_target="tpu_custom_call" | custom-call | flops 805306368 | bytes 6291456 | tf_op jit(solution)/shard_map/queries/pallas_call | solution.py:316
  50.9 25.4 %collective-permute-done.20.refs_6_ = bf16[4,64,576]{2,1,0:T(8,128)(2,1)} collective-permute-done((bf16[4,64,576]{2,1,0:T(8,128)(2,1)S(1)}, bf16[4,64,576]{2,1,0:T(8,128)(2,1)}, u32[]{:S(2)}, u32[]{:S(2)}) %collective-permute-start.20) | collective-permute-done | bytes 294944 | tf_op jit(solution)/shard_map/ppermute | solution.py:43
  80.4 2.3 %collective-permute-start.13 = (bf16[128,256]{1,0:T(8,128)(2,1)S(1)}, bf16[128,256]{1,0:T(8,128)(2,1)S(1)}, u32[]{:S(2)}, u32[]{:S(2)}) collective-permute-start(bf16[128,256]{1,0:T(8,128)(2,1)S(1)} %get-tuple-element.26), channel_id=1, source_target_pairs={{0,8},{2,10},{4,12},{6,14},{8,0},{10,2},{12,4},{14,6},{16,24},{18,... | collective-permute-start | bytes 196616 | tf_op jit(solution)/shard_map/ppermute | solution.py:40
  82.7 1.8 %collective-permute-start.14 = (bf16[128,256]{1,0:T(8,128)(2,1)S(1)}, bf16[128,256]{1,0:T(8,128)(2,1)}, u32[]{:S(2)}, u32[]{:S(2)}) collective-permute-start(bf16[128,256]{1,0:T(8,128)(2,1)S(1)} %get-tuple-element.27), channel_id=1, source_target_pairs={{0,16},{2,18},{4,20},{6,22},{8,24},{10,26},{12,28},{14,30},{16,0},... | collective-permute-start | bytes 196616 | tf_op jit(solution)/shard_map/ppermute | solution.py:40
  87.8 2.5 %latents.1.refs_0_ = bf16[256,576]{1,0:T(8,128)(2,1)S(1)} custom-call(bf16[64,2048]{1,0:T(8,128)(2,1)S(1)} %constant_dynamic-slice_fusion.9.refs_0_, bf16[64,2048]{1,0:T(8,128)(2,1)S(1)} %collective-permute-done.refs_1_, bf16[64,2048]{1,0:T(8,128)(2,1)S(1)} %collective-permute-done.1.refs_2_, bf16[64,2048]{1,0:T(8,128)(2,1)S(1)} %collective-permute-done.2.refs_3_, ...), custom_call_target="tpu_custom_call" | custom-call | flops 603979776 | bytes 3407872 | tf_op jit(solution)/shard_map/latents/pallas_call | solution.py:358
  91.9 3.0 %collective-permute-start.26 = (bf16[30,1024]{1,0:T(8,128)(2,1)S(1)}, bf16[30,1024]{1,0:T(8,128)(2,1)S(1)}, u32[]{:S(2)}, u32[]{:S(2)}) collective-permute-start(bf16[30,1024]{1,0:T(8,128)(2,1)S(1)} %pad_maximum_fusion.5), channel_id=1, source_target_pairs={{0,2},{2,4},{4,6},{6,8},{8,10},{10,12},{12,14},{14,16},{16,18},{18... | collective-permute-start | bytes 184328 | tf_op jit(solution)/shard_map/ppermute | solution.py:379
  94.9 1.7 %collective-permute-done.26 = bf16[30,1024]{1,0:T(8,128)(2,1)S(1)} collective-permute-done((bf16[30,1024]{1,0:T(8,128)(2,1)S(1)}, bf16[30,1024]{1,0:T(8,128)(2,1)S(1)}, u32[]{:S(2)}, u32[]{:S(2)}) %collective-permute-start.26) | collective-permute-done | bytes 61472 | tf_op jit(solution)/shard_map/ppermute | solution.py:379
  96.7 2.9 %fusion.44 = (f32[128]{0:T(128)S(1)}, f32[128]{0:T(128)S(1)}, f32[128,1024]{1,0:T(8,128)S(1)}) fusion(f32[158,1024]{1,0:T(8,128)S(1)} %maximum_convert_fusion, f32[1024]{0:T(1024)S(1)} %bitcast.93, f32[1024]{0:T(1024)S(1)} %bitcast.94, f32[1024]{0:T(1024)S(1)} %bitcast.65, f32[1024]{0:T(1024)S(1)} %bitcast.66, f32[1024]{0:T(1024)S(1)} %bitcast.67, ...), kind=kLoop, calls=%fused_computation.153 | loop fusion | flops 8388352 | bytes 16905216 | tf_op jit(solution)/shard_map/reduce_sum | solution.py:392
  99.7 2.4 %collective-permute-start.28 = (bf16[256,576]{1,0:T(8,128)(2,1)S(1)}, bf16[256,576]{1,0:T(8,128)(2,1)S(1)}, u32[]{:S(2)}, u32[]{:S(2)}) collective-permute-start(bf16[256,576]{1,0:T(8,128)(2,1)S(1)} %latents.1.refs_0_), channel_id=1, source_target_pairs={{0,2},{2,0},{4,6},{6,4},{8,10},{10,8},{12,14},{14,12},{16,18},{18,... | collective-permute-start | bytes 884744 | tf_op jit(solution)/shard_map/ppermute | solution.py:43
  105.2 1.9 %fusion.34 = f32[128,2048]{1,0:T(8,128)} fusion(bf16[1024,2048]{1,0:T(8,128)(2,1)S(1)} %copy-done.12, f32[128,1024]{1,0:T(8,128)S(1)} %get-tuple-element.42, f32[1024]{0:T(1024)S(1)} %copy-done.13, f32[128]{0:T(128)S(1)} %fusion.41, f32[128]{0:T(128)S(1)} %multiply_bitcast_fusion), kind=kOutput, calls=%fused_computation.76 | convolution fusion | flops 537919488 | bytes 5772288 | tf_op jit(solution)/shard_map/dot_general | solution.py:402
  107.1 3.6 %collective-permute-done.28.refs_1_ = bf16[256,576]{1,0:T(8,128)(2,1)S(1)} collective-permute-done((bf16[256,576]{1,0:T(8,128)(2,1)S(1)}, bf16[256,576]{1,0:T(8,128)(2,1)S(1)}, u32[]{:S(2)}, u32[]{:S(2)}) %collective-permute-start.28) | collective-permute-done | bytes 294944 | tf_op jit(solution)/shard_map/ppermute | solution.py:43
  110.7 7.6 %collective-permute-done.29.refs_2_ = bf16[256,576]{1,0:T(8,128)(2,1)S(1)} collective-permute-done((bf16[256,576]{1,0:T(8,128)(2,1)S(1)}, bf16[256,576]{1,0:T(8,128)(2,1)S(1)}, u32[]{:S(2)}, u32[]{:S(2)}) %collective-permute-start.29) | collective-permute-done | bytes 294944 | tf_op jit(solution)/shard_map/ppermute | solution.py:43
  118.3 2.0 %collective-permute-done.30.refs_3_ = bf16[256,576]{1,0:T(8,128)(2,1)} collective-permute-done((bf16[256,576]{1,0:T(8,128)(2,1)S(1)}, bf16[256,576]{1,0:T(8,128)(2,1)}, u32[]{:S(2)}, u32[]{:S(2)}) %collective-permute-start.30) | collective-permute-done | bytes 294944 | tf_op jit(solution)/shard_map/ppermute | solution.py:43
  123.5 9.7 %attention.1 = (bf16[128,1024]{1,0:T(8,128)(2,1)S(1)}, f32[8,128]{1,0:T(8,128)}) custom-call(bf16[8,128,576]{2,1,0:T(8,128)(2,1)S(1)} %copy-done, bf16[512,1024]{1,0:T(8,128)(2,1)S(1)} %copy-done.7, bf16[256,576]{1,0:T(8,128)(2,1)S(1)} %latents.1.refs_0_, bf16[256,576]{1,0:T(8,128)(2,1)S(1)} %collective-permute-done.28.refs_1_, ...), custom_call_target="tpu_custom_call" | custom-call | flops 4563402752 | bytes 2359296 | tf_op jit(solution)/shard_map/attention/pallas_call | solution.py:408
  (115 shorter events, 32.6 us)
Async XLA Ops:
  2.4 15.7 %collective-permute-start.16 = (bf16[64,576]{1,0:T(8,128)(2,1)S(1)}, bf16[64,576]{1,0:T(8,128)(2,1)S(1)}, u32[]{:S(2)}, u32[]{:S(2)}) collective-permute-start(bf16[64,576]{1,0:T(8,128)(2,1)S(1)} %fusion.39), channel_id=1, source_target_pairs={{0,8},{2,10},{4,12},{6,14},{8,0},{10,2},{12,4},{14,6},{16,24},{18,... | collective-permute-start | bytes 221192 | tf_op jit(solution)/shard_map/ppermute | solution.py:40
  5.5 12.7 %collective-permute-start.17 = (bf16[64,576]{1,0:T(8,128)(2,1)S(1)}, bf16[64,576]{1,0:T(8,128)(2,1)S(1)}, u32[]{:S(2)}, u32[]{:S(2)}) collective-permute-start(bf16[64,576]{1,0:T(8,128)(2,1)S(1)} %fusion.39), channel_id=1, source_target_pairs={{0,16},{2,18},{4,20},{6,22},{8,24},{10,26},{12,28},{14,30},{16,0},... | collective-permute-start | bytes 221192 | tf_op jit(solution)/shard_map/ppermute | solution.py:40
  8.1 10.6 %collective-permute-start.18 = (bf16[64,576]{1,0:T(8,128)(2,1)S(1)}, bf16[64,576]{1,0:T(8,128)(2,1)}, u32[]{:S(2)}, u32[]{:S(2)}) collective-permute-start(bf16[64,576]{1,0:T(8,128)(2,1)S(1)} %fusion.39), channel_id=1, source_target_pairs={{0,24},{2,26},{4,28},{6,30},{8,16},{10,18},{12,20},{14,22},{16,8},... | collective-permute-start | bytes 221192 | tf_op jit(solution)/shard_map/ppermute | solution.py:40
  11.6 15.9 %collective-permute-start.1 = (bf16[64,2048]{1,0:T(8,128)(2,1)S(1)}, bf16[64,2048]{1,0:T(8,128)(2,1)S(1)}, u32[]{:S(2)}, u32[]{:S(2)}) collective-permute-start(bf16[64,2048]{1,0:T(8,128)(2,1)S(1)} %constant_dynamic-slice_fusion.9.refs_0_), channel_id=1, source_target_pairs={{0,16},{2,18},{4,20},{6,22},{8,24},{10,26},{12,28},{14,30},{16,0},... | collective-permute-start | bytes 786440 | tf_op jit(solution)/shard_map/ppermute | solution.py:40
  14.7 8.8 %collective-permute-start.7 = (bf16[128,512]{1,0:T(8,128)(2,1)S(1)}, bf16[128,512]{1,0:T(8,128)(2,1)S(1)}, u32[]{:S(2)}, u32[]{:S(2)}) collective-permute-start(bf16[128,512]{1,0:T(8,128)(2,1)S(1)} %pad_maximum_fusion.2), channel_id=1, source_target_pairs={{0,8},{2,10},{4,12},{6,14},{8,0},{10,2},{12,4},{14,6},{16,24},{18,... | collective-permute-start | bytes 393224 | tf_op jit(solution)/shard_map/ppermute | solution.py:40
  18.1 21.8 %collective-permute-start = (bf16[64,2048]{1,0:T(8,128)(2,1)S(1)}, bf16[64,2048]{1,0:T(8,128)(2,1)S(1)}, u32[]{:S(2)}, u32[]{:S(2)}) collective-permute-start(bf16[64,2048]{1,0:T(8,128)(2,1)S(1)} %constant_dynamic-slice_fusion.9.refs_0_), channel_id=1, source_target_pairs={{0,8},{2,10},{4,12},{6,14},{8,0},{10,2},{12,4},{14,6},{16,24},{18,... | collective-permute-start | bytes 786440 | tf_op jit(solution)/shard_map/ppermute | solution.py:40
  18.1 13.5 %collective-permute-start.8 = (bf16[128,512]{1,0:T(8,128)(2,1)}, bf16[128,512]{1,0:T(8,128)(2,1)S(1)}, u32[]{:S(2)}, u32[]{:S(2)}) collective-permute-start(bf16[128,512]{1,0:T(8,128)(2,1)} %pad_maximum_fusion.3), channel_id=1, source_target_pairs={{0,16},{2,18},{4,20},{6,22},{8,24},{10,26},{12,28},{14,30},{16,0},... | collective-permute-start | bytes 393224 | tf_op jit(solution)/shard_map/ppermute | solution.py:40
  18.7 18.1 %collective-permute-start.9 = (bf16[128,512]{1,0:T(8,128)(2,1)S(1)}, bf16[128,512]{1,0:T(8,128)(2,1)S(1)}, u32[]{:S(2)}, u32[]{:S(2)}) collective-permute-start(bf16[128,512]{1,0:T(8,128)(2,1)S(1)} %pad_maximum_fusion.4), channel_id=1, source_target_pairs={{0,24},{2,26},{4,28},{6,30},{8,16},{10,18},{12,20},{14,22},{16,8},... | collective-permute-start | bytes 393224 | tf_op jit(solution)/shard_map/ppermute | solution.py:40
  23.5 17.0 %collective-permute-start.19 = (bf16[4,64,576]{2,1,0:T(8,128)(2,1)S(1)}, bf16[4,64,576]{2,1,0:T(8,128)(2,1)S(1)}, u32[]{:S(2)}, u32[]{:S(2)}) collective-permute-start(bf16[4,64,576]{2,1,0:T(8,128)(2,1)S(1)} %pad_maximum_fusion.1.refs_4_), channel_id=1, source_target_pairs={{0,2},{2,0},{4,6},{6,4},{8,10},{10,8},{12,14},{14,12},{16,18},{18,... | collective-permute-start | bytes 884744 | tf_op jit(solution)/shard_map/ppermute | solution.py:43
  27.4 14.8 %collective-permute-start.2 = (bf16[64,2048]{1,0:T(8,128)(2,1)S(1)}, bf16[64,2048]{1,0:T(8,128)(2,1)S(1)}, u32[]{:S(2)}, u32[]{:S(2)}) collective-permute-start(bf16[64,2048]{1,0:T(8,128)(2,1)S(1)} %collective-permute-done.1.refs_2_), channel_id=1, source_target_pairs={{0,8},{2,10},{4,12},{6,14},{8,0},{10,2},{12,4},{14,6},{16,24},{18,... | collective-permute-start | bytes 786440 | tf_op jit(solution)/shard_map/ppermute | solution.py:40
  36.8 40.0 %collective-permute-start.10 = (bf16[4,128,512]{2,1,0:T(8,128)(2,1)S(1)}, bf16[4,128,512]{2,1,0:T(8,128)(2,1)S(1)}, u32[]{:S(2)}, u32[]{:S(2)}) collective-permute-start(bf16[4,128,512]{2,1,0:T(8,128)(2,1)S(1)} %pad_maximum_fusion.refs_8_), channel_id=1, source_target_pairs={{0,2},{2,0},{4,6},{6,4},{8,10},{10,8},{12,14},{14,12},{16,18},{18,... | collective-permute-start | bytes 1572872 | tf_op jit(solution)/shard_map/ppermute | solution.py:43
  38.4 38.5 %collective-permute-start.11 = (bf16[4,128,512]{2,1,0:T(8,128)(2,1)S(1)}, bf16[4,128,512]{2,1,0:T(8,128)(2,1)S(1)}, u32[]{:S(2)}, u32[]{:S(2)}) collective-permute-start(bf16[4,128,512]{2,1,0:T(8,128)(2,1)S(1)} %pad_maximum_fusion.refs_8_), channel_id=1, source_target_pairs={{0,4},{2,6},{4,0},{6,2},{8,12},{10,14},{12,8},{14,10},{16,20},{18,... | collective-permute-start | bytes 1572872 | tf_op jit(solution)/shard_map/ppermute | solution.py:43
  39.9 36.4 %collective-permute-start.20 = (bf16[4,64,576]{2,1,0:T(8,128)(2,1)S(1)}, bf16[4,64,576]{2,1,0:T(8,128)(2,1)}, u32[]{:S(2)}, u32[]{:S(2)}) collective-permute-start(bf16[4,64,576]{2,1,0:T(8,128)(2,1)S(1)} %pad_maximum_fusion.1.refs_4_), channel_id=1, source_target_pairs={{0,4},{2,6},{4,0},{6,2},{8,12},{10,14},{12,8},{14,10},{16,20},{18,... | collective-permute-start | bytes 884744 | tf_op jit(solution)/shard_map/ppermute | solution.py:43
  40.5 35.8 %collective-permute-start.21 = (bf16[4,64,576]{2,1,0:T(8,128)(2,1)S(1)}, bf16[4,64,576]{2,1,0:T(8,128)(2,1)}, u32[]{:S(2)}, u32[]{:S(2)}) collective-permute-start(bf16[4,64,576]{2,1,0:T(8,128)(2,1)S(1)} %pad_maximum_fusion.1.refs_4_), channel_id=1, source_target_pairs={{0,6},{2,4},{4,2},{6,0},{8,14},{10,12},{12,10},{14,8},{16,22},{18,... | collective-permute-start | bytes 884744 | tf_op jit(solution)/shard_map/ppermute | solution.py:43
  42.2 35.2 %collective-permute-start.12 = (bf16[4,128,512]{2,1,0:T(8,128)(2,1)S(1)}, bf16[4,128,512]{2,1,0:T(8,128)(2,1)S(1)}, u32[]{:S(2)}, u32[]{:S(2)}) collective-permute-start(bf16[4,128,512]{2,1,0:T(8,128)(2,1)S(1)} %pad_maximum_fusion.refs_8_), channel_id=1, source_target_pairs={{0,6},{2,4},{4,2},{6,0},{8,14},{10,12},{12,10},{14,8},{16,22},{18,... | collective-permute-start | bytes 1572872 | tf_op jit(solution)/shard_map/ppermute | solution.py:43
  77.9 6.7 %collective-permute-start.23 = (bf16[4,64,576]{2,1,0:T(8,128)(2,1)S(1)}, bf16[4,64,576]{2,1,0:T(8,128)(2,1)S(1)}, u32[]{:S(2)}, u32[]{:S(2)}) collective-permute-start(bf16[4,64,576]{2,1,0:T(8,128)(2,1)S(1)} %collective-permute-done.19.refs_5_), channel_id=1, source_target_pairs={{0,1},{1,0},{2,3},{3,2},{4,5},{5,4},{6,7},{7,6},{8,9},{9,8},{10,11... | collective-permute-start | bytes 884744 | tf_op jit(solution)/shard_map/ppermute | solution.py:47
  78.2 7.8 %collective-permute-start.24 = (bf16[4,64,576]{2,1,0:T(8,128)(2,1)}, bf16[4,64,576]{2,1,0:T(8,128)(2,1)S(1)}, u32[]{:S(2)}, u32[]{:S(2)}) collective-permute-start(bf16[4,64,576]{2,1,0:T(8,128)(2,1)} %collective-permute-done.20.refs_6_), channel_id=1, source_target_pairs={{0,1},{1,0},{2,3},{3,2},{4,5},{5,4},{6,7},{7,6},{8,9},{9,8},{10,11... | collective-permute-start | bytes 884744 | tf_op jit(solution)/shard_map/ppermute | solution.py:47
  78.6 8.2 %collective-permute-start.25 = (bf16[4,64,576]{2,1,0:T(8,128)(2,1)}, bf16[4,64,576]{2,1,0:T(8,128)(2,1)}, u32[]{:S(2)}, u32[]{:S(2)}) collective-permute-start(bf16[4,64,576]{2,1,0:T(8,128)(2,1)} %collective-permute-done.21.refs_7_), channel_id=1, source_target_pairs={{0,1},{1,0},{2,3},{3,2},{4,5},{5,4},{6,7},{7,6},{8,9},{9,8},{10,11... | collective-permute-start | bytes 884744 | tf_op jit(solution)/shard_map/ppermute | solution.py:47
  80.4 9.9 %collective-permute-start.13 = (bf16[128,256]{1,0:T(8,128)(2,1)S(1)}, bf16[128,256]{1,0:T(8,128)(2,1)S(1)}, u32[]{:S(2)}, u32[]{:S(2)}) collective-permute-start(bf16[128,256]{1,0:T(8,128)(2,1)S(1)} %get-tuple-element.26), channel_id=1, source_target_pairs={{0,8},{2,10},{4,12},{6,14},{8,0},{10,2},{12,4},{14,6},{16,24},{18,... | collective-permute-start | bytes 196616 | tf_op jit(solution)/shard_map/ppermute | solution.py:40
  82.7 8.3 %collective-permute-start.14 = (bf16[128,256]{1,0:T(8,128)(2,1)S(1)}, bf16[128,256]{1,0:T(8,128)(2,1)}, u32[]{:S(2)}, u32[]{:S(2)}) collective-permute-start(bf16[128,256]{1,0:T(8,128)(2,1)S(1)} %get-tuple-element.27), channel_id=1, source_target_pairs={{0,16},{2,18},{4,20},{6,22},{8,24},{10,26},{12,28},{14,30},{16,0},... | collective-permute-start | bytes 196616 | tf_op jit(solution)/shard_map/ppermute | solution.py:40
  84.5 6.4 %collective-permute-start.15 = (bf16[128,256]{1,0:T(8,128)(2,1)S(1)}, bf16[128,256]{1,0:T(8,128)(2,1)}, u32[]{:S(2)}, u32[]{:S(2)}) collective-permute-start(bf16[128,256]{1,0:T(8,128)(2,1)S(1)} %get-tuple-element.28), channel_id=1, source_target_pairs={{0,24},{2,26},{4,28},{6,30},{8,16},{10,18},{12,20},{14,22},{16,8},... | collective-permute-start | bytes 196616 | tf_op jit(solution)/shard_map/ppermute | solution.py:40
  99.7 11.0 %collective-permute-start.28 = (bf16[256,576]{1,0:T(8,128)(2,1)S(1)}, bf16[256,576]{1,0:T(8,128)(2,1)S(1)}, u32[]{:S(2)}, u32[]{:S(2)}) collective-permute-start(bf16[256,576]{1,0:T(8,128)(2,1)S(1)} %latents.1.refs_0_), channel_id=1, source_target_pairs={{0,2},{2,0},{4,6},{6,4},{8,10},{10,8},{12,14},{14,12},{16,18},{18,... | collective-permute-start | bytes 884744 | tf_op jit(solution)/shard_map/ppermute | solution.py:43
  102.1 16.1 %collective-permute-start.29 = (bf16[256,576]{1,0:T(8,128)(2,1)S(1)}, bf16[256,576]{1,0:T(8,128)(2,1)S(1)}, u32[]{:S(2)}, u32[]{:S(2)}) collective-permute-start(bf16[256,576]{1,0:T(8,128)(2,1)S(1)} %latents.1.refs_0_), channel_id=1, source_target_pairs={{0,4},{2,6},{4,0},{6,2},{8,12},{10,14},{12,8},{14,10},{16,20},{18,... | collective-permute-start | bytes 884744 | tf_op jit(solution)/shard_map/ppermute | solution.py:43
  103.7 16.5 %collective-permute-start.30 = (bf16[256,576]{1,0:T(8,128)(2,1)S(1)}, bf16[256,576]{1,0:T(8,128)(2,1)}, u32[]{:S(2)}, u32[]{:S(2)}) collective-permute-start(bf16[256,576]{1,0:T(8,128)(2,1)S(1)} %latents.1.refs_0_), channel_id=1, source_target_pairs={{0,6},{2,4},{4,2},{6,0},{8,14},{10,12},{12,10},{14,8},{16,22},{18,... | collective-permute-start | bytes 884744 | tf_op jit(solution)/shard_map/ppermute | solution.py:43
  (26 other events, 289.6 us)

commit v4 on v1

--- a/solution.py
+++ b/solution.py
@@ -48,6 +48,13 @@
 
     def outer_gather(self, block):
         return [block] + [self.outer_swap(block, j) for j in range(1, self.outer)]
+
+    def outer_forward(self, block):
+        blocks = [block]
+        for j in range(1, self.outer):
+            near = j & -j
+            blocks.append(self.outer_swap(blocks[j ^ near], near))
+        return blocks
 
     def inner_gather(self, block):
         return [block] + [self.inner_swap(block, k) for k in range(1, self.inner)]
@@ -291,7 +298,7 @@
     ).astype(jnp.bfloat16)
 
     own_rows = lax.dynamic_slice_in_dim(normed, ti * share, share, 0)
-    rows = place.outer_gather(own_rows)
+    rows = place.outer_forward(own_rows)
     weight_block = jnp.stack(columns)
     weight_block, query_rows = lax.optimization_barrier((weight_block, normed))
     weight_blocks = place.inner_gather(weight_block)
@@ -404,7 +411,8 @@
         name="attention",
     )(queries, value_up_weight, *latents)
 
-    prior_rows, gated_rows, _ = lax.optimization_barrier((prior_rows, gated_rows, attention))
+    attn_part = jnp.dot(attention, w_merge_attn, preferred_element_type=jnp.float32)
+    prior_rows, gated_rows, _ = lax.optimization_barrier((prior_rows, gated_rows, attn_part))
     padded = jnp.concatenate([prior_rows, gated_rows], axis=0).astype(jnp.float32)
     mixed = jnp.zeros(gated_rows.shape, jnp.float32)
     for tap_index in range(conv_taps.shape[0]):
@@ -424,8 +432,7 @@
     ).astype(bf16)
 
     partial = (
-        jnp.dot(conv_out, w_merge_conv, preferred_element_type=jnp.float32)
-        + jnp.dot(attention, w_merge_attn, preferred_element_type=jnp.float32)
+        attn_part + jnp.dot(conv_out, w_merge_conv, preferred_element_type=jnp.float32)
     ).astype(bf16)
     merged = lax.dynamic_slice_in_dim(partial, ti * share, share, 0).astype(jnp.float32)
     for t in range(1, tp_count):

time: 118 us -> 115 us (0.975); the launches traced: 116 us -> 114 us
  starting transfers between devices: 45 us -> 39.4 us
  waiting for transfers between devices: 36.8 us -> 38.5 us
  other arithmetic: 6.79 us -> 8.35 us
    ppermute x9, waiting for transfers between devices: 16.4 us -> 22.8 us  [inner_swap(): lax.ppermute(block, 'sp', [(i, i ^ mask) for i in range(self.sp_count)])]
    ppermute x12, waiting for transfers between devices: 18.2 us -> 13.2 us  [outer_swap(): lax.ppermute(block, 'sp', [(i, i ^ mask) for i in range(self.sp_count)])]
    ppermute x12, starting transfers between devices: 25.7 us -> 21.7 us  [outer_swap(): lax.ppermute(block, 'sp', [(i, i ^ mask) for i in range(self.sp_count)])]
    ppermute x9, starting transfers between devices: 13.1 us -> 11.5 us  [inner_swap(): lax.ppermute(block, 'sp', [(i, i ^ mask) for i in range(self.sp_count)])]
  transfers between devices with their start and end apart: 36 -> 36, of which waited for: 11 -> 11; matrix products, arithmetic and copies ran while one was open for 3% -> 5% of each run, Pallas kernels for 15% -> 15%
where the time goes in v4:
time: 115 us; the launch traced here: 114 us
  starting transfers between devices  39.4 us (34%)
  waiting for transfers between devices  38.5 us (33%)
  Pallas kernels  17.6 us (15%)
  other arithmetic  8.35 us (7%)
  matrix products  3.78 us (3%)
  local copies, waits for them, and re-layouts  2.95 us (3%)
  blocking collectives  2.39 us (2%)
  between operations  1.42 us (1%)
    ppermute x9, waiting for transfers between devices, inner_swap(): lax.ppermute(block, 'sp', [(i, i ^ mask) for i in range(self.sp_count)])  22.8 us
    ppermute x12, starting transfers between devices, outer_swap(): lax.ppermute(block, 'sp', [(i, i ^ mask) for i in range(self.sp_count)])  21.7 us
    ppermute x12, waiting for transfers between devices, outer_swap(): lax.ppermute(block, 'sp', [(i, i ^ mask) for i in range(self.sp_count)])  13.2 us
    ppermute x9, starting transfers between devices, inner_swap(): lax.ppermute(block, 'sp', [(i, i ^ mask) for i in range(self.sp_count)])  11.5 us
    pallas_call x1, Pallas kernels, local(): pl.pallas_call(functools.partial(attention_kernel, place, score_scale, ra...  9.33 us
    pallas_call x1, Pallas kernels, local(): pl.pallas_call(functools.partial(query_kernel, rank), out_shape=jax.Shape...  5.52 us
    ppermute x14, starting transfers between devices, tp_shift(): return lax.ppermute(block, 'tp', route)  3.36 us
    dot_general x1, matrix products, local(): jnp.dot(conv_out, w_merge_conv, preferred_element_type=jnp.float32)  3.07 us
  transfers between devices with their start and end apart: 36, of which 11 were waited for; matrix products, arithmetic and copies ran while one was open for 5% of the time, Pallas kernels for 15%

profile of v4, /device:TPU:0, one launch (start us, length us, event | category | flops | bytes accessed | tf_op | source)
XLA Modules:
  0.0 114.5 jit_solution(17832011079086883533)
XLA Ops:
  2.4 3.1 %collective-permute-start.3 = (bf16[64,576]{1,0:T(8,128)(2,1)S(1)}, bf16[64,576]{1,0:T(8,128)(2,1)S(1)}, u32[]{:S(2)}, u32[]{:S(2)}) collective-permute-start(bf16[64,576]{1,0:T(8,128)(2,1)S(1)} %fusion.38), channel_id=1, source_target_pairs={{0,8},{2,10},{4,12},{6,14},{8,0},{10,2},{12,4},{14,6},{16,24},{18,... | collective-permute-start | bytes 221192 | tf_op jit(solution)/shard_map/ppermute | solution.py:40
  5.5 2.6 %collective-permute-start.4 = (bf16[64,576]{1,0:T(8,128)(2,1)S(1)}, bf16[64,576]{1,0:T(8,128)(2,1)S(1)}, u32[]{:S(2)}, u32[]{:S(2)}) collective-permute-start(bf16[64,576]{1,0:T(8,128)(2,1)S(1)} %fusion.38), channel_id=1, source_target_pairs={{0,16},{2,18},{4,20},{6,22},{8,24},{10,26},{12,28},{14,30},{16,0},... | collective-permute-start | bytes 221192 | tf_op jit(solution)/shard_map/ppermute | solution.py:40
  10.2 3.6 %collective-permute-start.1 = (bf16[128,512]{1,0:T(8,128)(2,1)S(1)}, bf16[128,512]{1,0:T(8,128)(2,1)S(1)}, u32[]{:S(2)}, u32[]{:S(2)}) collective-permute-start(bf16[128,512]{1,0:T(8,128)(2,1)S(1)} %pad_maximum_fusion.4), channel_id=1, source_target_pairs={{0,16},{2,18},{4,20},{6,22},{8,24},{10,26},{12,28},{14,30},{16,0},... | collective-permute-start | bytes 393224 | tf_op jit(solution)/shard_map/ppermute | solution.py:40
  15.3 2.4 %all_gather.3 = bf16[128,2048]{1,0:T(8,128)(2,1)S(1)} all-gather(bf16[128,1024]{1,0:T(8,128)(2,1)} %param.14), channel_id=1, replica_groups=mesh['sp'=16,'tp'=2] {'tp'}, dimensions={1}, use_global_device_ids=true | all-gather | bytes 786432 | tf_op jit(solution)/shard_map/all_gather | solution.py:292
  18.1 8.7 %collective-permute-start.7 = (bf16[64,2048]{1,0:T(8,128)(2,1)S(1)}, bf16[64,2048]{1,0:T(8,128)(2,1)S(1)}, u32[]{:S(2)}, u32[]{:S(2)}) collective-permute-start(bf16[64,2048]{1,0:T(8,128)(2,1)S(1)} %constant_dynamic-slice_fusion.1.refs_0_), channel_id=1, source_target_pairs={{0,16},{2,18},{4,20},{6,22},{8,24},{10,26},{12,28},{14,30},{16,0},... | collective-permute-start | bytes 786440 | tf_op jit(solution)/shard_map/ppermute | solution.py:40
  26.8 1.5 %collective-permute-start.10 = (bf16[4,64,576]{2,1,0:T(8,128)(2,1)S(1)}, bf16[4,64,576]{2,1,0:T(8,128)(2,1)S(1)}, u32[]{:S(2)}, u32[]{:S(2)}) collective-permute-start(bf16[4,64,576]{2,1,0:T(8,128)(2,1)S(1)} %pad_maximum_fusion.1.refs_4_), channel_id=1, source_target_pairs={{0,4},{2,6},{4,0},{6,2},{8,12},{10,14},{12,8},{14,10},{16,20},{18,... | collective-permute-start | bytes 884744 | tf_op jit(solution)/shard_map/ppermute | solution.py:43
  28.4 1.6 %collective-permute-start.27 = (bf16[4,128,512]{2,1,0:T(8,128)(2,1)S(1)}, bf16[4,128,512]{2,1,0:T(8,128)(2,1)S(1)}, u32[]{:S(2)}, u32[]{:S(2)}) collective-permute-start(bf16[4,128,512]{2,1,0:T(8,128)(2,1)S(1)} %pad_maximum_fusion.refs_8_), channel_id=1, source_target_pairs={{0,2},{2,0},{4,6},{6,4},{8,10},{10,8},{12,14},{14,12},{16,18},{18,... | collective-permute-start | bytes 1572872 | tf_op jit(solution)/shard_map/ppermute | solution.py:43
  30.5 8.6 %collective-permute-done.7.refs_2_ = bf16[64,2048]{1,0:T(8,128)(2,1)S(1)} collective-permute-done((bf16[64,2048]{1,0:T(8,128)(2,1)S(1)}, bf16[64,2048]{1,0:T(8,128)(2,1)S(1)}, u32[]{:S(2)}, u32[]{:S(2)}) %collective-permute-start.7) | collective-permute-done | bytes 262176 | tf_op jit(solution)/shard_map/ppermute | solution.py:40
  39.1 2.4 %collective-permute-start.11 = (bf16[4,64,576]{2,1,0:T(8,128)(2,1)S(1)}, bf16[4,64,576]{2,1,0:T(8,128)(2,1)S(1)}, u32[]{:S(2)}, u32[]{:S(2)}) collective-permute-start(bf16[4,64,576]{2,1,0:T(8,128)(2,1)S(1)} %pad_maximum_fusion.1.refs_4_), channel_id=1, source_target_pairs={{0,6},{2,4},{4,2},{6,0},{8,14},{10,12},{12,10},{14,8},{16,22},{18,... | collective-permute-start | bytes 884744 | tf_op jit(solution)/shard_map/ppermute | solution.py:43
  43.1 5.5 %queries.1.q_ref = bf16[8,128,576]{2,1,0:T(8,128)(2,1)} custom-call(bf16[128,2048]{1,0:T(8,128)(2,1)S(1)} %fusion.3.normed_ref, bf16[2048,1536]{1,0:T(8,128)(2,1)} %w_ref.1, bf16[512,1024]{1,0:T(8,128)(2,1)S(1)} %copy-done.1, f32[384,32]{1,0:T(8,128)S(1)} %get-tuple-element.103.cos_ref.refs_13_, f32[384,32]{1,0:T(8,128)S(1)} %get-tuple-element.102.sin_ref.refs_14_), custom_call_target="tpu_custom_call" | custom-call | flops 805306368 | bytes 6291456 | tf_op jit(solution)/shard_map/queries/pallas_call | solution.py:321
  48.6 2.0 %collective-permute-done.11.refs_7_ = bf16[4,64,576]{2,1,0:T(8,128)(2,1)S(1)} collective-permute-done((bf16[4,64,576]{2,1,0:T(8,128)(2,1)S(1)}, bf16[4,64,576]{2,1,0:T(8,128)(2,1)S(1)}, u32[]{:S(2)}, u32[]{:S(2)}) %collective-permute-start.11) | collective-permute-done | bytes 294944 | tf_op jit(solution)/shard_map/ppermute | solution.py:43
  50.6 6.1 %collective-permute-done.9.refs_5_ = bf16[4,64,576]{2,1,0:T(8,128)(2,1)S(1)} collective-permute-done((bf16[4,64,576]{2,1,0:T(8,128)(2,1)S(1)}, bf16[4,64,576]{2,1,0:T(8,128)(2,1)S(1)}, u32[]{:S(2)}, u32[]{:S(2)}) %collective-permute-start.9) | collective-permute-done | bytes 294944 | tf_op jit(solution)/shard_map/ppermute | solution.py:43
  57.8 1.4 %collective-permute-start.29 = (bf16[4,128,512]{2,1,0:T(8,128)(2,1)S(1)}, bf16[4,128,512]{2,1,0:T(8,128)(2,1)S(1)}, u32[]{:S(2)}, u32[]{:S(2)}) collective-permute-start(bf16[4,128,512]{2,1,0:T(8,128)(2,1)S(1)} %pad_maximum_fusion.refs_8_), channel_id=1, source_target_pairs={{0,6},{2,4},{4,2},{6,0},{8,14},{10,12},{12,10},{14,8},{16,22},{18,... | collective-permute-start | bytes 1572872 | tf_op jit(solution)/shard_map/ppermute | solution.py:43
  61.6 11.0 %collective-permute-done.29.refs_11_ = bf16[4,128,512]{2,1,0:T(8,128)(2,1)S(1)} collective-permute-done((bf16[4,128,512]{2,1,0:T(8,128)(2,1)S(1)}, bf16[4,128,512]{2,1,0:T(8,128)(2,1)S(1)}, u32[]{:S(2)}, u32[]{:S(2)}) %collective-permute-start.29) | collective-permute-done | bytes 524320 | tf_op jit(solution)/shard_map/ppermute | solution.py:43
  72.6 1.5 %collective-permute-start.16 = (bf16[256,576]{1,0:T(8,128)(2,1)S(1)}, bf16[256,576]{1,0:T(8,128)(2,1)S(1)}, u32[]{:S(2)}, u32[]{:S(2)}) collective-permute-start(bf16[256,576]{1,0:T(8,128)(2,1)S(1)} %latents.1.refs_0_), channel_id=1, source_target_pairs={{0,2},{2,0},{4,6},{6,4},{8,10},{10,8},{12,14},{14,12},{16,18},{18,... | collective-permute-start | bytes 884744 | tf_op jit(solution)/shard_map/ppermute | solution.py:43
  74.6 1.5 %collective-permute-start.18 = (bf16[256,576]{1,0:T(8,128)(2,1)S(1)}, bf16[256,576]{1,0:T(8,128)(2,1)}, u32[]{:S(2)}, u32[]{:S(2)}) collective-permute-start(bf16[256,576]{1,0:T(8,128)(2,1)S(1)} %latents.1.refs_0_), channel_id=1, source_target_pairs={{0,6},{2,4},{4,2},{6,0},{8,14},{10,12},{12,10},{14,8},{16,22},{18,... | collective-permute-start | bytes 884744 | tf_op jit(solution)/shard_map/ppermute | solution.py:43
  76.1 1.4 %gated.1 = (bf16[128,256]{1,0:T(8,128)(2,1)S(1)}, bf16[128,256]{1,0:T(8,128)(2,1)S(1)}, bf16[128,256]{1,0:T(8,128)(2,1)S(1)}, bf16[128,256]{1,0:T(8,128)(2,1)S(1)}) custom-call(bf16[64,2048]{1,0:T(8,128)(2,1)S(1)} %constant_dynamic-slice_fusion.1.refs_0_, bf16[64,2048]{1,0:T(8,128)(2,1)S(1)} %collective-permute-done.6.refs_1_, ...), custom_call_target="tpu_custom_call" | custom-call | flops 1073741824 | bytes 4194304 | tf_op jit(solution)/shard_map/gated/pallas_call | solution.py:366
  79.0 1.7 %collective-permute-start.31 = (bf16[128,256]{1,0:T(8,128)(2,1)S(1)}, bf16[128,256]{1,0:T(8,128)(2,1)}, u32[]{:S(2)}, u32[]{:S(2)}) collective-permute-start(bf16[128,256]{1,0:T(8,128)(2,1)S(1)} %get-tuple-element.50), channel_id=1, source_target_pairs={{0,16},{2,18},{4,20},{6,22},{8,24},{10,26},{12,28},{14,30},{16,0},... | collective-permute-start | bytes 196616 | tf_op jit(solution)/shard_map/ppermute | solution.py:40
  80.7 3.2 %collective-permute-done.30 = bf16[128,256]{1,0:T(8,128)(2,1)S(1)} collective-permute-done((bf16[128,256]{1,0:T(8,128)(2,1)S(1)}, bf16[128,256]{1,0:T(8,128)(2,1)S(1)}, u32[]{:S(2)}, u32[]{:S(2)}) %collective-permute-start.30) | collective-permute-done | bytes 65568 | tf_op jit(solution)/shard_map/ppermute | solution.py:40
  85.9 3.7 %collective-permute-done.17.refs_2_ = bf16[256,576]{1,0:T(8,128)(2,1)S(1)} collective-permute-done((bf16[256,576]{1,0:T(8,128)(2,1)S(1)}, bf16[256,576]{1,0:T(8,128)(2,1)S(1)}, u32[]{:S(2)}, u32[]{:S(2)}) %collective-permute-start.17) | collective-permute-done | bytes 294944 | tf_op jit(solution)/shard_map/ppermute | solution.py:43
  91.1 2.9 %collective-permute-start.33 = (bf16[30,1024]{1,0:T(8,128)(2,1)S(1)}, bf16[30,1024]{1,0:T(8,128)(2,1)S(1)}, u32[]{:S(2)}, u32[]{:S(2)}) collective-permute-start(bf16[30,1024]{1,0:T(8,128)(2,1)S(1)} %slice.252), channel_id=1, source_target_pairs={{0,2},{2,4},{4,6},{6,8},{8,10},{10,12},{12,14},{14,16},{16,18},{18... | collective-permute-start | bytes 184328 | tf_op jit(solution)/shard_map/ppermute | solution.py:387
  94.1 9.3 %attention.1 = (bf16[128,1024]{1,0:T(8,128)(2,1)S(1)}, f32[8,128]{1,0:T(8,128)}) custom-call(bf16[8,128,576]{2,1,0:T(8,128)(2,1)S(1)} %copy-done, bf16[512,1024]{1,0:T(8,128)(2,1)S(1)} %copy-done.3, bf16[256,576]{1,0:T(8,128)(2,1)S(1)} %latents.1.refs_0_, bf16[256,576]{1,0:T(8,128)(2,1)S(1)} %collective-permute-done.16.refs_1_, ...), custom_call_target="tpu_custom_call" | custom-call | flops 4563402752 | bytes 2359296 | tf_op jit(solution)/shard_map/attention/pallas_call | solution.py:394
  104.8 2.9 %fusion.43 = (f32[128]{0:T(128)S(1)}, f32[128]{0:T(128)S(1)}, f32[128,1024]{1,0:T(8,128)S(1)}) fusion(f32[158,1024]{1,0:T(8,128)S(1)} %maximum_convert_fusion, f32[1024]{0:T(1024)S(1)} %bitcast.94, f32[1024]{0:T(1024)S(1)} %bitcast.95, f32[1024]{0:T(1024)S(1)} %bitcast.66, f32[1024]{0:T(1024)S(1)} %bitcast.67, f32[1024]{0:T(1024)S(1)} %bitcast.68, ...), kind=kLoop, calls=%fused_computation.150 | loop fusion | flops 8388352 | bytes 16905216 | tf_op jit(solution)/shard_map/reduce_sum | solution.py:424
  109.0 3.1 %fusion = bf16[128,2048]{1,0:T(8,128)(2,1)S(1)} fusion(f32[128,2048]{1,0:T(8,128)S(1)} %fusion.45, bf16[1024,2048]{1,0:T(8,128)(2,1)} %param.26, f32[128,1024]{1,0:T(8,128)S(1)} %get-tuple-element.58, f32[1024]{0:T(1024)S(1)} %copy-done.35, f32[128]{0:T(128)S(1)} %fusion.40, f32[128]{0:T(128)S(1)} %multiply_bitcast_fusion), kind=kOutput, calls=%fused_computation.1 | convolution fusion | flops 538443776 | bytes 6296576 | tf_op jit(solution)/shard_map/dot_general | solution.py:435
  (160 shorter events, 21.3 us)
Async XLA Ops:
  2.4 11.5 %collective-permute-start.3 = (bf16[64,576]{1,0:T(8,128)(2,1)S(1)}, bf16[64,576]{1,0:T(8,128)(2,1)S(1)}, u32[]{:S(2)}, u32[]{:S(2)}) collective-permute-start(bf16[64,576]{1,0:T(8,128)(2,1)S(1)} %fusion.38), channel_id=1, source_target_pairs={{0,8},{2,10},{4,12},{6,14},{8,0},{10,2},{12,4},{14,6},{16,24},{18,... | collective-permute-start | bytes 221192 | tf_op jit(solution)/shard_map/ppermute | solution.py:40
  5.5 8.8 %collective-permute-start.4 = (bf16[64,576]{1,0:T(8,128)(2,1)S(1)}, bf16[64,576]{1,0:T(8,128)(2,1)S(1)}, u32[]{:S(2)}, u32[]{:S(2)}) collective-permute-start(bf16[64,576]{1,0:T(8,128)(2,1)S(1)} %fusion.38), channel_id=1, source_target_pairs={{0,16},{2,18},{4,20},{6,22},{8,24},{10,26},{12,28},{14,30},{16,0},... | collective-permute-start | bytes 221192 | tf_op jit(solution)/shard_map/ppermute | solution.py:40
  9.2 17.6 %collective-permute-start = (bf16[128,512]{1,0:T(8,128)(2,1)S(1)}, bf16[128,512]{1,0:T(8,128)(2,1)S(1)}, u32[]{:S(2)}, u32[]{:S(2)}) collective-permute-start(bf16[128,512]{1,0:T(8,128)(2,1)S(1)} %pad_maximum_fusion.3), channel_id=1, source_target_pairs={{0,8},{2,10},{4,12},{6,14},{8,0},{10,2},{12,4},{14,6},{16,24},{18,... | collective-permute-start | bytes 393224 | tf_op jit(solution)/shard_map/ppermute | solution.py:40
  10.2 18.2 %collective-permute-start.1 = (bf16[128,512]{1,0:T(8,128)(2,1)S(1)}, bf16[128,512]{1,0:T(8,128)(2,1)S(1)}, u32[]{:S(2)}, u32[]{:S(2)}) collective-permute-start(bf16[128,512]{1,0:T(8,128)(2,1)S(1)} %pad_maximum_fusion.4), channel_id=1, source_target_pairs={{0,16},{2,18},{4,20},{6,22},{8,24},{10,26},{12,28},{14,30},{16,0},... | collective-permute-start | bytes 393224 | tf_op jit(solution)/shard_map/ppermute | solution.py:40
  14.0 14.4 %collective-permute-start.2 = (bf16[128,512]{1,0:T(8,128)(2,1)S(1)}, bf16[128,512]{1,0:T(8,128)(2,1)S(1)}, u32[]{:S(2)}, u32[]{:S(2)}) collective-permute-start(bf16[128,512]{1,0:T(8,128)(2,1)S(1)} %pad_maximum_fusion.5), channel_id=1, source_target_pairs={{0,24},{2,26},{4,28},{6,30},{8,16},{10,18},{12,20},{14,22},{16,8},... | collective-permute-start | bytes 393224 | tf_op jit(solution)/shard_map/ppermute | solution.py:40
  18.1 21.1 %collective-permute-start.7 = (bf16[64,2048]{1,0:T(8,128)(2,1)S(1)}, bf16[64,2048]{1,0:T(8,128)(2,1)S(1)}, u32[]{:S(2)}, u32[]{:S(2)}) collective-permute-start(bf16[64,2048]{1,0:T(8,128)(2,1)S(1)} %constant_dynamic-slice_fusion.1.refs_0_), channel_id=1, source_target_pairs={{0,16},{2,18},{4,20},{6,22},{8,24},{10,26},{12,28},{14,30},{16,0},... | collective-permute-start | bytes 786440 | tf_op jit(solution)/shard_map/ppermute | solution.py:40
  26.8 14.8 %collective-permute-start.6 = (bf16[64,2048]{1,0:T(8,128)(2,1)S(1)}, bf16[64,2048]{1,0:T(8,128)(2,1)S(1)}, u32[]{:S(2)}, u32[]{:S(2)}) collective-permute-start(bf16[64,2048]{1,0:T(8,128)(2,1)S(1)} %constant_dynamic-slice_fusion.1.refs_0_), channel_id=1, source_target_pairs={{0,8},{2,10},{4,12},{6,14},{8,0},{10,2},{12,4},{14,6},{16,24},{18,... | collective-permute-start | bytes 786440 | tf_op jit(solution)/shard_map/ppermute | solution.py:40
  26.8 15.3 %collective-permute-start.10 = (bf16[4,64,576]{2,1,0:T(8,128)(2,1)S(1)}, bf16[4,64,576]{2,1,0:T(8,128)(2,1)S(1)}, u32[]{:S(2)}, u32[]{:S(2)}) collective-permute-start(bf16[4,64,576]{2,1,0:T(8,128)(2,1)S(1)} %pad_maximum_fusion.1.refs_4_), channel_id=1, source_target_pairs={{0,4},{2,6},{4,0},{6,2},{8,12},{10,14},{12,8},{14,10},{16,20},{18,... | collective-permute-start | bytes 884744 | tf_op jit(solution)/shard_map/ppermute | solution.py:43
  28.4 28.8 %collective-permute-start.27 = (bf16[4,128,512]{2,1,0:T(8,128)(2,1)S(1)}, bf16[4,128,512]{2,1,0:T(8,128)(2,1)S(1)}, u32[]{:S(2)}, u32[]{:S(2)}) collective-permute-start(bf16[4,128,512]{2,1,0:T(8,128)(2,1)S(1)} %pad_maximum_fusion.refs_8_), channel_id=1, source_target_pairs={{0,2},{2,0},{4,6},{6,4},{8,10},{10,8},{12,14},{14,12},{16,18},{18,... | collective-permute-start | bytes 1572872 | tf_op jit(solution)/shard_map/ppermute | solution.py:43
  30.0 27.8 %collective-permute-start.28 = (bf16[4,128,512]{2,1,0:T(8,128)(2,1)S(1)}, bf16[4,128,512]{2,1,0:T(8,128)(2,1)S(1)}, u32[]{:S(2)}, u32[]{:S(2)}) collective-permute-start(bf16[4,128,512]{2,1,0:T(8,128)(2,1)S(1)} %pad_maximum_fusion.refs_8_), channel_id=1, source_target_pairs={{0,4},{2,6},{4,0},{6,2},{8,12},{10,14},{12,8},{14,10},{16,20},{18,... | collective-permute-start | bytes 1572872 | tf_op jit(solution)/shard_map/ppermute | solution.py:43
  39.1 11.5 %collective-permute-start.11 = (bf16[4,64,576]{2,1,0:T(8,128)(2,1)S(1)}, bf16[4,64,576]{2,1,0:T(8,128)(2,1)S(1)}, u32[]{:S(2)}, u32[]{:S(2)}) collective-permute-start(bf16[4,64,576]{2,1,0:T(8,128)(2,1)S(1)} %pad_maximum_fusion.1.refs_4_), channel_id=1, source_target_pairs={{0,6},{2,4},{4,2},{6,0},{8,14},{10,12},{12,10},{14,8},{16,22},{18,... | collective-permute-start | bytes 884744 | tf_op jit(solution)/shard_map/ppermute | solution.py:43
  41.6 15.1 %collective-permute-start.9 = (bf16[4,64,576]{2,1,0:T(8,128)(2,1)S(1)}, bf16[4,64,576]{2,1,0:T(8,128)(2,1)S(1)}, u32[]{:S(2)}, u32[]{:S(2)}) collective-permute-start(bf16[4,64,576]{2,1,0:T(8,128)(2,1)S(1)} %pad_maximum_fusion.1.refs_4_), channel_id=1, source_target_pairs={{0,2},{2,0},{4,6},{6,4},{8,10},{10,8},{12,14},{14,12},{16,18},{18,... | collective-permute-start | bytes 884744 | tf_op jit(solution)/shard_map/ppermute | solution.py:43
  42.1 14.6 %collective-permute-start.8 = (bf16[64,2048]{1,0:T(8,128)(2,1)S(1)}, bf16[64,2048]{1,0:T(8,128)(2,1)S(1)}, u32[]{:S(2)}, u32[]{:S(2)}) collective-permute-start(bf16[64,2048]{1,0:T(8,128)(2,1)S(1)} %collective-permute-done.7.refs_2_), channel_id=1, source_target_pairs={{0,8},{2,10},{4,12},{6,14},{8,0},{10,2},{12,4},{14,6},{16,24},{18,... | collective-permute-start | bytes 786440 | tf_op jit(solution)/shard_map/ppermute | solution.py:40
  57.8 14.8 %collective-permute-start.29 = (bf16[4,128,512]{2,1,0:T(8,128)(2,1)S(1)}, bf16[4,128,512]{2,1,0:T(8,128)(2,1)S(1)}, u32[]{:S(2)}, u32[]{:S(2)}) collective-permute-start(bf16[4,128,512]{2,1,0:T(8,128)(2,1)S(1)} %pad_maximum_fusion.refs_8_), channel_id=1, source_target_pairs={{0,6},{2,4},{4,2},{6,0},{8,14},{10,12},{12,10},{14,8},{16,22},{18,... | collective-permute-start | bytes 1572872 | tf_op jit(solution)/shard_map/ppermute | solution.py:43
  59.2 14.9 %collective-permute-start.23 = (bf16[64,2048]{1,0:T(8,128)(2,1)S(1)}, bf16[64,2048]{1,0:T(8,128)(2,1)S(1)}, u32[]{:S(2)}, u32[]{:S(2)}) collective-permute-start(bf16[64,2048]{1,0:T(8,128)(2,1)S(1)} %constant_dynamic-slice_fusion.1.refs_0_), channel_id=1, source_target_pairs={{0,1},{1,0},{2,3},{3,2},{4,5},{5,4},{6,7},{7,6},{8,9},{9,8},{10,11... | collective-permute-start | bytes 786440 | tf_op jit(solution)/shard_map/ppermute | solution.py:47
  59.2 15.4 %collective-permute-start.24 = (bf16[64,2048]{1,0:T(8,128)(2,1)S(1)}, bf16[64,2048]{1,0:T(8,128)(2,1)S(1)}, u32[]{:S(2)}, u32[]{:S(2)}) collective-permute-start(bf16[64,2048]{1,0:T(8,128)(2,1)S(1)} %collective-permute-done.6.refs_1_), channel_id=1, source_target_pairs={{0,1},{1,0},{2,3},{3,2},{4,5},{5,4},{6,7},{7,6},{8,9},{9,8},{10,11... | collective-permute-start | bytes 786440 | tf_op jit(solution)/shard_map/ppermute | solution.py:47
  59.7 16.3 %collective-permute-start.25 = (bf16[64,2048]{1,0:T(8,128)(2,1)S(1)}, bf16[64,2048]{1,0:T(8,128)(2,1)S(1)}, u32[]{:S(2)}, u32[]{:S(2)}) collective-permute-start(bf16[64,2048]{1,0:T(8,128)(2,1)S(1)} %collective-permute-done.7.refs_2_), channel_id=1, source_target_pairs={{0,1},{1,0},{2,3},{3,2},{4,5},{5,4},{6,7},{7,6},{8,9},{9,8},{10,11... | collective-permute-start | bytes 786440 | tf_op jit(solution)/shard_map/ppermute | solution.py:47
  59.8 16.3 %collective-permute-start.26 = (bf16[64,2048]{1,0:T(8,128)(2,1)S(1)}, bf16[64,2048]{1,0:T(8,128)(2,1)S(1)}, u32[]{:S(2)}, u32[]{:S(2)}) collective-permute-start(bf16[64,2048]{1,0:T(8,128)(2,1)S(1)} %collective-permute-done.8.refs_3_), channel_id=1, source_target_pairs={{0,1},{1,0},{2,3},{3,2},{4,5},{5,4},{6,7},{7,6},{8,9},{9,8},{10,11... | collective-permute-start | bytes 786440 | tf_op jit(solution)/shard_map/ppermute | solution.py:47
  72.6 12.8 %collective-permute-start.16 = (bf16[256,576]{1,0:T(8,128)(2,1)S(1)}, bf16[256,576]{1,0:T(8,128)(2,1)S(1)}, u32[]{:S(2)}, u32[]{:S(2)}) collective-permute-start(bf16[256,576]{1,0:T(8,128)(2,1)S(1)} %latents.1.refs_0_), channel_id=1, source_target_pairs={{0,2},{2,0},{4,6},{6,4},{8,10},{10,8},{12,14},{14,12},{16,18},{18,... | collective-permute-start | bytes 884744 | tf_op jit(solution)/shard_map/ppermute | solution.py:43
  74.1 15.6 %collective-permute-start.17 = (bf16[256,576]{1,0:T(8,128)(2,1)S(1)}, bf16[256,576]{1,0:T(8,128)(2,1)S(1)}, u32[]{:S(2)}, u32[]{:S(2)}) collective-permute-start(bf16[256,576]{1,0:T(8,128)(2,1)S(1)} %latents.1.refs_0_), channel_id=1, source_target_pairs={{0,4},{2,6},{4,0},{6,2},{8,12},{10,14},{12,8},{14,10},{16,20},{18,... | collective-permute-start | bytes 884744 | tf_op jit(solution)/shard_map/ppermute | solution.py:43
  74.6 15.1 %collective-permute-start.18 = (bf16[256,576]{1,0:T(8,128)(2,1)S(1)}, bf16[256,576]{1,0:T(8,128)(2,1)}, u32[]{:S(2)}, u32[]{:S(2)}) collective-permute-start(bf16[256,576]{1,0:T(8,128)(2,1)S(1)} %latents.1.refs_0_), channel_id=1, source_target_pairs={{0,6},{2,4},{4,2},{6,0},{8,14},{10,12},{12,10},{14,8},{16,22},{18,... | collective-permute-start | bytes 884744 | tf_op jit(solution)/shard_map/ppermute | solution.py:43
  85.4 8.6 %collective-permute-start.19 = (bf16[256,576]{1,0:T(8,128)(2,1)S(1)}, bf16[256,576]{1,0:T(8,128)(2,1)S(1)}, u32[]{:S(2)}, u32[]{:S(2)}) collective-permute-start(bf16[256,576]{1,0:T(8,128)(2,1)S(1)} %latents.1.refs_0_), channel_id=1, source_target_pairs={{0,1},{1,0},{2,3},{3,2},{4,5},{5,4},{6,7},{7,6},{8,9},{9,8},{10,11... | collective-permute-start | bytes 884744 | tf_op jit(solution)/shard_map/ppermute | solution.py:47
  85.4 8.6 %collective-permute-start.20 = (bf16[256,576]{1,0:T(8,128)(2,1)S(1)}, bf16[256,576]{1,0:T(8,128)(2,1)S(1)}, u32[]{:S(2)}, u32[]{:S(2)}) collective-permute-start(bf16[256,576]{1,0:T(8,128)(2,1)S(1)} %collective-permute-done.16.refs_1_), channel_id=1, source_target_pairs={{0,1},{1,0},{2,3},{3,2},{4,5},{5,4},{6,7},{7,6},{8,9},{9,8},{10,11... | collective-permute-start | bytes 884744 | tf_op jit(solution)/shard_map/ppermute | solution.py:47
  91.1 13.3 %collective-permute-start.33 = (bf16[30,1024]{1,0:T(8,128)(2,1)S(1)}, bf16[30,1024]{1,0:T(8,128)(2,1)S(1)}, u32[]{:S(2)}, u32[]{:S(2)}) collective-permute-start(bf16[30,1024]{1,0:T(8,128)(2,1)S(1)} %slice.252), channel_id=1, source_target_pairs={{0,2},{2,4},{4,6},{6,8},{8,10},{10,12},{12,14},{14,16},{16,18},{18... | collective-permute-start | bytes 184328 | tf_op jit(solution)/shard_map/ppermute | solution.py:387
  (48 other events, 257.3 us)

commit v5 on v4

--- a/solution.py
+++ b/solution.py
@@ -286,7 +286,6 @@
         columns.append(block if j == 0 else place.outer_swap(block, j))
 
     table = jnp.stack(table_parts)
-    table, tokens = lax.optimization_barrier((table, tokens))
     tables = place.inner_gather(table)
 
     gathered = lax.all_gather(tokens, "tp", axis=1, tiled=True)
@@ -300,7 +299,8 @@
     own_rows = lax.dynamic_slice_in_dim(normed, ti * share, share, 0)
     rows = place.outer_forward(own_rows)
     weight_block = jnp.stack(columns)
-    weight_block, query_rows = lax.optimization_barrier((weight_block, normed))
+    taps = conv_taps.astype(jnp.float32)
+    weight_block, query_rows, taps = lax.optimization_barrier((weight_block, normed, taps))
     weight_blocks = place.inner_gather(weight_block)
 
     bf16 = jnp.bfloat16
@@ -337,7 +337,8 @@
         name="queries",
     )(query_rows, w_query, key_up_weight, cosine, sine)
 
-    rows, tables, _ = lax.optimization_barrier((rows, tables, queries))
+    tables, _ = lax.optimization_barrier((tables, queries))
+    rows, _ = lax.optimization_barrier((rows, queries))
     if split_rows:
         tables = sum(place.tp_gather(tables), [])
 
@@ -418,7 +419,7 @@
     for tap_index in range(conv_taps.shape[0]):
         mixed = (
             mixed
-            + conv_taps[tap_index].astype(jnp.float32) * padded[tap_index : tap_index + row_count]
+            + taps[tap_index] * padded[tap_index : tap_index + row_count]
         )
     channel_total = mixed.shape[1] * tp_count
     stats = jnp.stack([jnp.sum(mixed, axis=1), jnp.sum(mixed * mixed, axis=1)])
@@ -431,9 +432,9 @@
         (mixed - channel_mean[:, None]) * lax.rsqrt(channel_var + epsilon)[:, None] * conv_gain
     ).astype(bf16)
 
-    partial = (
-        attn_part + jnp.dot(conv_out, w_merge_conv, preferred_element_type=jnp.float32)
-    ).astype(bf16)
+    conv_part = jnp.dot(conv_out, w_merge_conv, preferred_element_type=jnp.float32)
+    conv_part = lax.optimization_barrier(conv_part)
+    partial = (conv_part + attn_part).astype(bf16)
     merged = lax.dynamic_slice_in_dim(partial, ti * share, share, 0).astype(jnp.float32)
     for t in range(1, tp_count):
         away = lax.dynamic_slice_in_dim(partial, lax.rem(ti + t, tp_count) * share, share, 0)

time: 115 us -> 112 us (0.974); the launches traced: 114 us -> 110 us
  waiting for transfers between devices: 38.5 us -> 15.7 us
  local copies, waits for them, and re-layouts: 2.95 us -> 14.4 us
  starting transfers between devices: 39.4 us -> 43.2 us
  other arithmetic: 8.35 us -> 10.6 us
  Pallas kernels: 17.6 us -> 19.1 us
    ppermute x9, waiting for transfers between devices: 22.8 us -> 1.32 us  [inner_swap(): lax.ppermute(block, 'sp', [(i, i ^ mask) for i in range(self.sp_count)])]
    unnamed x73 -> x51, local copies, waits for them, and re-layouts: 1.69 us -> 13 us
    ppermute x9, starting transfers between devices: 11.5 us -> 14.6 us  [inner_swap(): lax.ppermute(block, 'sp', [(i, i ^ mask) for i in range(self.sp_count)])]
    ppermute x12, waiting for transfers between devices: 13.2 us -> 11.8 us  [outer_swap(): lax.ppermute(block, 'sp', [(i, i ^ mask) for i in range(self.sp_count)])]
    pallas_call x1, Pallas kernels: 1.42 us -> 2.78 us  [local(): pl.pallas_call(functools.partial(gated_kernel, place), out_shape=[jax.Sha...]
    mul x2 -> x0, other arithmetic: 1.32 us -> none  [local(): conv_taps[tap_index].astype(jnp.float32)]
    pallas_call x1, Pallas kernels: 1.35 us -> 2.52 us  [local(): pl.pallas_call(functools.partial(latent_kernel, place, rank, split_rows),...]
  transfers between devices with their start and end apart: 36 -> 36, of which waited for: 11 -> 9; matrix products, arithmetic and copies ran while one was open for 5% -> 7% of each run, Pallas kernels for 15% -> 17%
where the time goes in v5:
time: 112 us; the launch traced here: 110 us
  starting transfers between devices  43.2 us (39%)
  Pallas kernels  19.1 us (17%)
  waiting for transfers between devices  15.7 us (14%)
  local copies, waits for them, and re-layouts  14.4 us (13%)
  other arithmetic  10.6 us (9%)
  matrix products  3.77 us (3%)
  blocking collectives  2.38 us (2%)
    ppermute x12, starting transfers between devices, outer_swap(): lax.ppermute(block, 'sp', [(i, i ^ mask) for i in range(self.sp_count)])  21.4 us
    ppermute x9, starting transfers between devices, inner_swap(): lax.ppermute(block, 'sp', [(i, i ^ mask) for i in range(self.sp_count)])  14.6 us
    unnamed x51, local copies, waits for them, and re-layouts  13 us
    ppermute x12, waiting for transfers between devices, outer_swap(): lax.ppermute(block, 'sp', [(i, i ^ mask) for i in range(self.sp_count)])  11.8 us
    pallas_call x1, Pallas kernels, local(): pl.pallas_call(functools.partial(attention_kernel, place, score_scale, ra...  8.34 us
    pallas_call x1, Pallas kernels, local(): pl.pallas_call(functools.partial(query_kernel, rank), out_shape=jax.Shape...  5.5 us
    ppermute x1, starting transfers between devices, local(): lax.ppermute(gated_rows[row_count - conv_reach:], 'sp', [(i, i + 1) for i...  3.84 us
    ppermute x14, starting transfers between devices, tp_shift(): return lax.ppermute(block, 'tp', route)  3.35 us
  transfers between devices with their start and end apart: 36, of which 9 were waited for; matrix products, arithmetic and copies ran while one was open for 7% of the time, Pallas kernels for 17%

profile of v5, /device:TPU:0, one launch (start us, length us, event | category | flops | bytes accessed | tf_op | source)
XLA Modules:
  0.0 110.2 jit_solution(10285144754424786279)
XLA Ops:
  2.4 3.1 %collective-permute-start.10 = (bf16[64,576]{1,0:T(8,128)(2,1)S(1)}, bf16[64,576]{1,0:T(8,128)(2,1)S(1)}, u32[]{:S(2)}, u32[]{:S(2)}) collective-permute-start(bf16[64,576]{1,0:T(8,128)(2,1)S(1)} %fusion.38), channel_id=1, source_target_pairs={{0,8},{2,10},{4,12},{6,14},{8,0},{10,2},{12,4},{14,6},{16,24},{18,... | collective-permute-start | bytes 221192 | tf_op jit(solution)/shard_map/ppermute | solution.py:40
  5.5 2.6 %collective-permute-start.11 = (bf16[64,576]{1,0:T(8,128)(2,1)S(1)}, bf16[64,576]{1,0:T(8,128)(2,1)}, u32[]{:S(2)}, u32[]{:S(2)}) collective-permute-start(bf16[64,576]{1,0:T(8,128)(2,1)S(1)} %fusion.38), channel_id=1, source_target_pairs={{0,16},{2,18},{4,20},{6,22},{8,24},{10,26},{12,28},{14,30},{16,0},... | collective-permute-start | bytes 221192 | tf_op jit(solution)/shard_map/ppermute | solution.py:40
  10.8 3.6 %collective-permute-start.1 = (bf16[128,512]{1,0:T(8,128)(2,1)S(1)}, bf16[128,512]{1,0:T(8,128)(2,1)}, u32[]{:S(2)}, u32[]{:S(2)}) collective-permute-start(bf16[128,512]{1,0:T(8,128)(2,1)S(1)} %pad_maximum_fusion.4), channel_id=1, source_target_pairs={{0,16},{2,18},{4,20},{6,22},{8,24},{10,26},{12,28},{14,30},{16,0},... | collective-permute-start | bytes 393224 | tf_op jit(solution)/shard_map/ppermute | solution.py:40
  14.3 2.4 %all_gather.3 = bf16[128,2048]{1,0:T(8,128)(2,1)S(1)} all-gather(bf16[128,1024]{1,0:T(8,128)(2,1)} %param.14), channel_id=1, replica_groups=mesh['sp'=16,'tp'=2] {'tp'}, dimensions={1}, use_global_device_ids=true | all-gather | bytes 786432 | tf_op jit(solution)/shard_map/all_gather | solution.py:291
  21.1 1.6 %collective-permute-start.13 = (bf16[4,64,576]{2,1,0:T(8,128)(2,1)S(1)}, bf16[4,64,576]{2,1,0:T(8,128)(2,1)S(1)}, u32[]{:S(2)}, u32[]{:S(2)}) collective-permute-start(bf16[4,64,576]{2,1,0:T(8,128)(2,1)S(1)} %pad_maximum_fusion.1.refs_4_), channel_id=1, source_target_pairs={{0,2},{2,0},{4,6},{6,4},{8,10},{10,8},{12,14},{14,12},{16,18},{18,... | collective-permute-start | bytes 884744 | tf_op jit(solution)/shard_map/ppermute | solution.py:43
  22.7 1.5 %collective-permute-start.14 = (bf16[4,64,576]{2,1,0:T(8,128)(2,1)S(1)}, bf16[4,64,576]{2,1,0:T(8,128)(2,1)S(1)}, u32[]{:S(2)}, u32[]{:S(2)}) collective-permute-start(bf16[4,64,576]{2,1,0:T(8,128)(2,1)S(1)} %pad_maximum_fusion.1.refs_4_), channel_id=1, source_target_pairs={{0,4},{2,6},{4,0},{6,2},{8,12},{10,14},{12,8},{14,10},{16,20},{18,... | collective-permute-start | bytes 884744 | tf_op jit(solution)/shard_map/ppermute | solution.py:43
  24.2 2.1 %collective-permute-done.2 = bf16[128,512]{1,0:T(8,128)(2,1)S(1)} collective-permute-done((bf16[128,512]{1,0:T(8,128)(2,1)S(1)}, bf16[128,512]{1,0:T(8,128)(2,1)S(1)}, u32[]{:S(2)}, u32[]{:S(2)}) %collective-permute-start.2) | collective-permute-done | bytes 131104 | tf_op jit(solution)/shard_map/ppermute | solution.py:40
  27.3 1.6 %collective-permute-start.20 = (bf16[4,128,512]{2,1,0:T(8,128)(2,1)S(1)}, bf16[4,128,512]{2,1,0:T(8,128)(2,1)S(1)}, u32[]{:S(2)}, u32[]{:S(2)}) collective-permute-start(bf16[4,128,512]{2,1,0:T(8,128)(2,1)S(1)} %pad_maximum_fusion.refs_8_), channel_id=1, source_target_pairs={{0,2},{2,0},{4,6},{6,4},{8,10},{10,8},{12,14},{14,12},{16,18},{18,... | collective-permute-start | bytes 1572872 | tf_op jit(solution)/shard_map/ppermute | solution.py:43
  28.9 1.5 %collective-permute-start.21 = (bf16[4,128,512]{2,1,0:T(8,128)(2,1)S(1)}, bf16[4,128,512]{2,1,0:T(8,128)(2,1)S(1)}, u32[]{:S(2)}, u32[]{:S(2)}) collective-permute-start(bf16[4,128,512]{2,1,0:T(8,128)(2,1)S(1)} %pad_maximum_fusion.refs_8_), channel_id=1, source_target_pairs={{0,4},{2,6},{4,0},{6,2},{8,12},{10,14},{12,8},{14,10},{16,20},{18,... | collective-permute-start | bytes 1572872 | tf_op jit(solution)/shard_map/ppermute | solution.py:43
  30.4 7.6 %collective-permute-done.4.refs_2_ = bf16[64,2048]{1,0:T(8,128)(2,1)S(1)} collective-permute-done((bf16[64,2048]{1,0:T(8,128)(2,1)S(1)}, bf16[64,2048]{1,0:T(8,128)(2,1)S(1)}, u32[]{:S(2)}, u32[]{:S(2)}) %collective-permute-start.4) | collective-permute-done | bytes 262176 | tf_op jit(solution)/shard_map/ppermute | solution.py:40
  38.1 2.4 %collective-permute-start.15 = (bf16[4,64,576]{2,1,0:T(8,128)(2,1)S(1)}, bf16[4,64,576]{2,1,0:T(8,128)(2,1)S(1)}, u32[]{:S(2)}, u32[]{:S(2)}) collective-permute-start(bf16[4,64,576]{2,1,0:T(8,128)(2,1)S(1)} %pad_maximum_fusion.1.refs_4_), channel_id=1, source_target_pairs={{0,6},{2,4},{4,2},{6,0},{8,14},{10,12},{12,10},{14,8},{16,22},{18,... | collective-permute-start | bytes 884744 | tf_op jit(solution)/shard_map/ppermute | solution.py:43
  40.6 2.0 %collective-permute-start.5 = (bf16[64,2048]{1,0:T(8,128)(2,1)S(1)}, bf16[64,2048]{1,0:T(8,128)(2,1)}, u32[]{:S(2)}, u32[]{:S(2)}) collective-permute-start(bf16[64,2048]{1,0:T(8,128)(2,1)S(1)} %collective-permute-done.4.refs_2_), channel_id=1, source_target_pairs={{0,8},{2,10},{4,12},{6,14},{8,0},{10,2},{12,4},{14,6},{16,24},{18,... | collective-permute-start | bytes 786440 | tf_op jit(solution)/shard_map/ppermute | solution.py:40
  43.9 5.5 %queries.1.q_ref = bf16[8,128,576]{2,1,0:T(8,128)(2,1)} custom-call(bf16[128,2048]{1,0:T(8,128)(2,1)S(1)} %fusion.2.normed_ref, bf16[2048,1536]{1,0:T(8,128)(2,1)} %w_ref.1, bf16[512,1024]{1,0:T(8,128)(2,1)S(1)} %copy-done.1, f32[384,32]{1,0:T(8,128)S(1)} %get-tuple-element.101.cos_ref.refs_13_, f32[384,32]{1,0:T(8,128)S(1)} %get-tuple-element.100.sin_ref.refs_14_), custom_call_target="tpu_custom_call" | custom-call | flops 805306368 | bytes 6291456 | tf_op jit(solution)/shard_map/queries/pallas_call | solution.py:321
  54.0 2.4 %collective-permute-start.22 = (bf16[4,128,512]{2,1,0:T(8,128)(2,1)S(1)}, bf16[4,128,512]{2,1,0:T(8,128)(2,1)S(1)}, u32[]{:S(2)}, u32[]{:S(2)}) collective-permute-start(bf16[4,128,512]{2,1,0:T(8,128)(2,1)S(1)} %pad_maximum_fusion.refs_8_), channel_id=1, source_target_pairs={{0,6},{2,4},{4,2},{6,0},{8,14},{10,12},{12,10},{14,8},{16,22},{18,... | collective-permute-start | bytes 1572872 | tf_op jit(solution)/shard_map/ppermute | solution.py:43
  67.2 2.5 %latents.1.refs_0_ = bf16[256,576]{1,0:T(8,128)(2,1)S(1)} custom-call(bf16[64,2048]{1,0:T(8,128)(2,1)S(1)} %constant_dynamic-slice_fusion.1.refs_0_, bf16[64,2048]{1,0:T(8,128)(2,1)} %collective-permute-done.3.refs_1_, bf16[64,2048]{1,0:T(8,128)(2,1)S(1)} %collective-permute-done.4.refs_2_, bf16[64,2048]{1,0:T(8,128)(2,1)} %collective-permute-done.5.refs_3_, ...), custom_call_target="tpu_custom_call" | custom-call | flops 603979776 | bytes 3407872 | tf_op jit(solution)/shard_map/latents/pallas_call | solution.py:345
  71.8 1.6 %collective-permute-start.29 = (bf16[256,576]{1,0:T(8,128)(2,1)S(1)}, bf16[256,576]{1,0:T(8,128)(2,1)S(1)}, u32[]{:S(2)}, u32[]{:S(2)}) collective-permute-start(bf16[256,576]{1,0:T(8,128)(2,1)S(1)} %latents.1.refs_0_), channel_id=1, source_target_pairs={{0,6},{2,4},{4,2},{6,0},{8,14},{10,12},{12,10},{14,8},{16,22},{18,... | collective-permute-start | bytes 884744 | tf_op jit(solution)/shard_map/ppermute | solution.py:43
  73.4 2.8 %gated.1 = (bf16[128,256]{1,0:T(8,128)(2,1)S(1)}, bf16[128,256]{1,0:T(8,128)(2,1)S(1)}, bf16[128,256]{1,0:T(8,128)(2,1)S(1)}, bf16[128,256]{1,0:T(8,128)(2,1)S(1)}) custom-call(bf16[64,2048]{1,0:T(8,128)(2,1)S(1)} %constant_dynamic-slice_fusion.1.refs_0_, bf16[64,2048]{1,0:T(8,128)(2,1)} %collective-permute-done.3.refs_1_, ...), custom_call_target="tpu_custom_call" | custom-call | flops 1073741824 | bytes 4194304 | tf_op jit(solution)/shard_map/gated/pallas_call | solution.py:367
  76.2 2.4 %collective-permute-start.23 = (bf16[128,256]{1,0:T(8,128)(2,1)S(1)}, bf16[128,256]{1,0:T(8,128)(2,1)S(1)}, u32[]{:S(2)}, u32[]{:S(2)}) collective-permute-start(bf16[128,256]{1,0:T(8,128)(2,1)S(1)} %get-tuple-element.46), channel_id=1, source_target_pairs={{0,24},{2,26},{4,28},{6,30},{8,16},{10,18},{12,20},{14,22},{16,8},... | collective-permute-start | bytes 196616 | tf_op jit(solution)/shard_map/ppermute | solution.py:40
  78.6 2.8 %collective-permute-start.24 = (bf16[128,256]{1,0:T(8,128)(2,1)S(1)}, bf16[128,256]{1,0:T(8,128)(2,1)S(1)}, u32[]{:S(2)}, u32[]{:S(2)}) collective-permute-start(bf16[128,256]{1,0:T(8,128)(2,1)S(1)} %get-tuple-element.47), channel_id=1, source_target_pairs={{0,16},{2,18},{4,20},{6,22},{8,24},{10,26},{12,28},{14,30},{16,0},... | collective-permute-start | bytes 196616 | tf_op jit(solution)/shard_map/ppermute | solution.py:40
  82.4 2.6 %collective-permute-start.25 = (bf16[128,256]{1,0:T(8,128)(2,1)S(1)}, bf16[128,256]{1,0:T(8,128)(2,1)S(1)}, u32[]{:S(2)}, u32[]{:S(2)}) collective-permute-start(bf16[128,256]{1,0:T(8,128)(2,1)S(1)} %get-tuple-element.48), channel_id=1, source_target_pairs={{0,8},{2,10},{4,12},{6,14},{8,0},{10,2},{12,4},{14,6},{16,24},{18,... | collective-permute-start | bytes 196616 | tf_op jit(solution)/shard_map/ppermute | solution.py:40
  87.4 3.8 %collective-permute-start.26 = (bf16[30,1024]{1,0:T(8,128)(2,1)S(1)}, bf16[30,1024]{1,0:T(8,128)(2,1)S(1)}, u32[]{:S(2)}, u32[]{:S(2)}) collective-permute-start(bf16[30,1024]{1,0:T(8,128)(2,1)S(1)} %slice.252), channel_id=1, source_target_pairs={{0,2},{2,4},{4,6},{6,8},{8,10},{10,12},{12,14},{14,16},{16,18},{18... | collective-permute-start | bytes 184328 | tf_op jit(solution)/shard_map/ppermute | solution.py:388
  91.3 8.3 %attention.1 = (bf16[128,1024]{1,0:T(8,128)(2,1)S(1)}, f32[8,128]{1,0:T(8,128)}) custom-call(bf16[8,128,576]{2,1,0:T(8,128)(2,1)S(1)} %copy-done, bf16[512,1024]{1,0:T(8,128)(2,1)S(1)} %copy-done.21, bf16[256,576]{1,0:T(8,128)(2,1)S(1)} %latents.1.refs_0_, bf16[256,576]{1,0:T(8,128)(2,1)S(1)} %collective-permute-done.27.refs_1_, ...), custom_call_target="tpu_custom_call" | custom-call | flops 4563402752 | bytes 2359296 | tf_op jit(solution)/shard_map/attention/pallas_call | solution.py:395
  100.4 2.9 %fusion.43 = (f32[128]{0:T(128)S(1)}, f32[128]{0:T(128)S(1)}, f32[128,1024]{1,0:T(8,128)S(1)}) fusion(f32[158,1024]{1,0:T(8,128)S(1)} %maximum_convert_fusion, f32[1024]{0:T(1024)S(1)} %bitcast.62, f32[1024]{0:T(1024)S(1)} %bitcast.63, f32[1024]{0:T(1024)S(1)} %bitcast.64, f32[1024]{0:T(1024)S(1)} %bitcast.65, f32[1024]{0:T(1024)S(1)} %bitcast.66, ...), kind=kLoop, calls=%fused_computation.119 | loop fusion | flops 8388352 | bytes 16905216 | tf_op jit(solution)/shard_map/reduce_sum | solution.py:425
  104.6 3.1 %fusion.33 = f32[128,2048]{1,0:T(8,128)S(1)} fusion(bf16[1024,2048]{1,0:T(8,128)(2,1)} %param.26, f32[128,1024]{1,0:T(8,128)S(1)} %get-tuple-element.56, f32[1024]{0:T(1024)S(1)} %copy-done.24, f32[128]{0:T(128)S(1)} %fusion.40, f32[128]{0:T(128)S(1)} %multiply_bitcast_fusion), kind=kOutput, calls=%fused_computation.75 | convolution fusion | flops 537919488 | bytes 5772288 | tf_op jit(solution)/shard_map/dot_general | solution.py:435
  (140 shorter events, 36.6 us)
Async XLA Ops:
  2.4 15.5 %collective-permute-start.10 = (bf16[64,576]{1,0:T(8,128)(2,1)S(1)}, bf16[64,576]{1,0:T(8,128)(2,1)S(1)}, u32[]{:S(2)}, u32[]{:S(2)}) collective-permute-start(bf16[64,576]{1,0:T(8,128)(2,1)S(1)} %fusion.38), channel_id=1, source_target_pairs={{0,8},{2,10},{4,12},{6,14},{8,0},{10,2},{12,4},{14,6},{16,24},{18,... | collective-permute-start | bytes 221192 | tf_op jit(solution)/shard_map/ppermute | solution.py:40
  5.5 13.2 %collective-permute-start.11 = (bf16[64,576]{1,0:T(8,128)(2,1)S(1)}, bf16[64,576]{1,0:T(8,128)(2,1)}, u32[]{:S(2)}, u32[]{:S(2)}) collective-permute-start(bf16[64,576]{1,0:T(8,128)(2,1)S(1)} %fusion.38), channel_id=1, source_target_pairs={{0,16},{2,18},{4,20},{6,22},{8,24},{10,26},{12,28},{14,30},{16,0},... | collective-permute-start | bytes 221192 | tf_op jit(solution)/shard_map/ppermute | solution.py:40
  8.1 12.0 %collective-permute-start.12 = (bf16[64,576]{1,0:T(8,128)(2,1)S(1)}, bf16[64,576]{1,0:T(8,128)(2,1)}, u32[]{:S(2)}, u32[]{:S(2)}) collective-permute-start(bf16[64,576]{1,0:T(8,128)(2,1)S(1)} %fusion.38), channel_id=1, source_target_pairs={{0,24},{2,26},{4,28},{6,30},{8,16},{10,18},{12,20},{14,22},{16,8},... | collective-permute-start | bytes 221192 | tf_op jit(solution)/shard_map/ppermute | solution.py:40
  9.8 12.8 %collective-permute-start = (bf16[128,512]{1,0:T(8,128)(2,1)}, bf16[128,512]{1,0:T(8,128)(2,1)}, u32[]{:S(2)}, u32[]{:S(2)}) collective-permute-start(bf16[128,512]{1,0:T(8,128)(2,1)} %pad_maximum_fusion.3), channel_id=1, source_target_pairs={{0,8},{2,10},{4,12},{6,14},{8,0},{10,2},{12,4},{14,6},{16,24},{18,... | collective-permute-start | bytes 393224 | tf_op jit(solution)/shard_map/ppermute | solution.py:40
  10.8 13.4 %collective-permute-start.1 = (bf16[128,512]{1,0:T(8,128)(2,1)S(1)}, bf16[128,512]{1,0:T(8,128)(2,1)}, u32[]{:S(2)}, u32[]{:S(2)}) collective-permute-start(bf16[128,512]{1,0:T(8,128)(2,1)S(1)} %pad_maximum_fusion.4), channel_id=1, source_target_pairs={{0,16},{2,18},{4,20},{6,22},{8,24},{10,26},{12,28},{14,30},{16,0},... | collective-permute-start | bytes 393224 | tf_op jit(solution)/shard_map/ppermute | solution.py:40
  18.0 8.3 %collective-permute-start.2 = (bf16[128,512]{1,0:T(8,128)(2,1)S(1)}, bf16[128,512]{1,0:T(8,128)(2,1)S(1)}, u32[]{:S(2)}, u32[]{:S(2)}) collective-permute-start(bf16[128,512]{1,0:T(8,128)(2,1)S(1)} %pad_maximum_fusion.5), channel_id=1, source_target_pairs={{0,24},{2,26},{4,28},{6,30},{8,16},{10,18},{12,20},{14,22},{16,8},... | collective-permute-start | bytes 393224 | tf_op jit(solution)/shard_map/ppermute | solution.py:40
  18.7 19.4 %collective-permute-start.4 = (bf16[64,2048]{1,0:T(8,128)(2,1)S(1)}, bf16[64,2048]{1,0:T(8,128)(2,1)S(1)}, u32[]{:S(2)}, u32[]{:S(2)}) collective-permute-start(bf16[64,2048]{1,0:T(8,128)(2,1)S(1)} %constant_dynamic-slice_fusion.1.refs_0_), channel_id=1, source_target_pairs={{0,16},{2,18},{4,20},{6,22},{8,24},{10,26},{12,28},{14,30},{16,0},... | collective-permute-start | bytes 786440 | tf_op jit(solution)/shard_map/ppermute | solution.py:40
  21.1 17.0 %collective-permute-start.13 = (bf16[4,64,576]{2,1,0:T(8,128)(2,1)S(1)}, bf16[4,64,576]{2,1,0:T(8,128)(2,1)S(1)}, u32[]{:S(2)}, u32[]{:S(2)}) collective-permute-start(bf16[4,64,576]{2,1,0:T(8,128)(2,1)S(1)} %pad_maximum_fusion.1.refs_4_), channel_id=1, source_target_pairs={{0,2},{2,0},{4,6},{6,4},{8,10},{10,8},{12,14},{14,12},{16,18},{18,... | collective-permute-start | bytes 884744 | tf_op jit(solution)/shard_map/ppermute | solution.py:43
  22.7 17.9 %collective-permute-start.14 = (bf16[4,64,576]{2,1,0:T(8,128)(2,1)S(1)}, bf16[4,64,576]{2,1,0:T(8,128)(2,1)S(1)}, u32[]{:S(2)}, u32[]{:S(2)}) collective-permute-start(bf16[4,64,576]{2,1,0:T(8,128)(2,1)S(1)} %pad_maximum_fusion.1.refs_4_), channel_id=1, source_target_pairs={{0,4},{2,6},{4,0},{6,2},{8,12},{10,14},{12,8},{14,10},{16,20},{18,... | collective-permute-start | bytes 884744 | tf_op jit(solution)/shard_map/ppermute | solution.py:43
  27.3 23.8 %collective-permute-start.20 = (bf16[4,128,512]{2,1,0:T(8,128)(2,1)S(1)}, bf16[4,128,512]{2,1,0:T(8,128)(2,1)S(1)}, u32[]{:S(2)}, u32[]{:S(2)}) collective-permute-start(bf16[4,128,512]{2,1,0:T(8,128)(2,1)S(1)} %pad_maximum_fusion.refs_8_), channel_id=1, source_target_pairs={{0,2},{2,0},{4,6},{6,4},{8,10},{10,8},{12,14},{14,12},{16,18},{18,... | collective-permute-start | bytes 1572872 | tf_op jit(solution)/shard_map/ppermute | solution.py:43
  28.9 24.3 %collective-permute-start.21 = (bf16[4,128,512]{2,1,0:T(8,128)(2,1)S(1)}, bf16[4,128,512]{2,1,0:T(8,128)(2,1)S(1)}, u32[]{:S(2)}, u32[]{:S(2)}) collective-permute-start(bf16[4,128,512]{2,1,0:T(8,128)(2,1)S(1)} %pad_maximum_fusion.refs_8_), channel_id=1, source_target_pairs={{0,4},{2,6},{4,0},{6,2},{8,12},{10,14},{12,8},{14,10},{16,20},{18,... | collective-permute-start | bytes 1572872 | tf_op jit(solution)/shard_map/ppermute | solution.py:43
  38.0 11.7 %collective-permute-start.3 = (bf16[64,2048]{1,0:T(8,128)(2,1)S(1)}, bf16[64,2048]{1,0:T(8,128)(2,1)}, u32[]{:S(2)}, u32[]{:S(2)}) collective-permute-start(bf16[64,2048]{1,0:T(8,128)(2,1)S(1)} %constant_dynamic-slice_fusion.1.refs_0_), channel_id=1, source_target_pairs={{0,8},{2,10},{4,12},{6,14},{8,0},{10,2},{12,4},{14,6},{16,24},{18,... | collective-permute-start | bytes 786440 | tf_op jit(solution)/shard_map/ppermute | solution.py:40
  38.1 11.6 %collective-permute-start.15 = (bf16[4,64,576]{2,1,0:T(8,128)(2,1)S(1)}, bf16[4,64,576]{2,1,0:T(8,128)(2,1)S(1)}, u32[]{:S(2)}, u32[]{:S(2)}) collective-permute-start(bf16[4,64,576]{2,1,0:T(8,128)(2,1)S(1)} %pad_maximum_fusion.1.refs_4_), channel_id=1, source_target_pairs={{0,6},{2,4},{4,2},{6,0},{8,14},{10,12},{12,10},{14,8},{16,22},{18,... | collective-permute-start | bytes 884744 | tf_op jit(solution)/shard_map/ppermute | solution.py:43
  40.6 10.6 %collective-permute-start.5 = (bf16[64,2048]{1,0:T(8,128)(2,1)S(1)}, bf16[64,2048]{1,0:T(8,128)(2,1)}, u32[]{:S(2)}, u32[]{:S(2)}) collective-permute-start(bf16[64,2048]{1,0:T(8,128)(2,1)S(1)} %collective-permute-done.4.refs_2_), channel_id=1, source_target_pairs={{0,8},{2,10},{4,12},{6,14},{8,0},{10,2},{12,4},{14,6},{16,24},{18,... | collective-permute-start | bytes 786440 | tf_op jit(solution)/shard_map/ppermute | solution.py:40
  49.7 7.5 %collective-permute-start.17 = (bf16[4,64,576]{2,1,0:T(8,128)(2,1)S(1)}, bf16[4,64,576]{2,1,0:T(8,128)(2,1)S(1)}, u32[]{:S(2)}, u32[]{:S(2)}) collective-permute-start(bf16[4,64,576]{2,1,0:T(8,128)(2,1)S(1)} %collective-permute-done.13.refs_5_), channel_id=1, source_target_pairs={{0,1},{1,0},{2,3},{3,2},{4,5},{5,4},{6,7},{7,6},{8,9},{9,8},{10,11... | collective-permute-start | bytes 884744 | tf_op jit(solution)/shard_map/ppermute | solution.py:47
  54.0 15.8 %collective-permute-start.22 = (bf16[4,128,512]{2,1,0:T(8,128)(2,1)S(1)}, bf16[4,128,512]{2,1,0:T(8,128)(2,1)S(1)}, u32[]{:S(2)}, u32[]{:S(2)}) collective-permute-start(bf16[4,128,512]{2,1,0:T(8,128)(2,1)S(1)} %pad_maximum_fusion.refs_8_), channel_id=1, source_target_pairs={{0,6},{2,4},{4,2},{6,0},{8,14},{10,12},{12,10},{14,8},{16,22},{18,... | collective-permute-start | bytes 1572872 | tf_op jit(solution)/shard_map/ppermute | solution.py:43
  57.2 13.2 %collective-permute-start.6 = (bf16[64,2048]{1,0:T(8,128)(2,1)S(1)}, bf16[64,2048]{1,0:T(8,128)(2,1)}, u32[]{:S(2)}, u32[]{:S(2)}) collective-permute-start(bf16[64,2048]{1,0:T(8,128)(2,1)S(1)} %constant_dynamic-slice_fusion.1.refs_0_), channel_id=1, source_target_pairs={{0,1},{1,0},{2,3},{3,2},{4,5},{5,4},{6,7},{7,6},{8,9},{9,8},{10,11... | collective-permute-start | bytes 786440 | tf_op jit(solution)/shard_map/ppermute | solution.py:47
  57.9 13.8 %collective-permute-start.7 = (bf16[64,2048]{1,0:T(8,128)(2,1)}, bf16[64,2048]{1,0:T(8,128)(2,1)}, u32[]{:S(2)}, u32[]{:S(2)}) collective-permute-start(bf16[64,2048]{1,0:T(8,128)(2,1)} %collective-permute-done.3.refs_1_), channel_id=1, source_target_pairs={{0,1},{1,0},{2,3},{3,2},{4,5},{5,4},{6,7},{7,6},{8,9},{9,8},{10,11... | collective-permute-start | bytes 786440 | tf_op jit(solution)/shard_map/ppermute | solution.py:47
  59.2 14.2 %collective-permute-start.8 = (bf16[64,2048]{1,0:T(8,128)(2,1)S(1)}, bf16[64,2048]{1,0:T(8,128)(2,1)}, u32[]{:S(2)}, u32[]{:S(2)}) collective-permute-start(bf16[64,2048]{1,0:T(8,128)(2,1)S(1)} %collective-permute-done.4.refs_2_), channel_id=1, source_target_pairs={{0,1},{1,0},{2,3},{3,2},{4,5},{5,4},{6,7},{7,6},{8,9},{9,8},{10,11... | collective-permute-start | bytes 786440 | tf_op jit(solution)/shard_map/ppermute | solution.py:47
  59.9 13.4 %collective-permute-start.9 = (bf16[64,2048]{1,0:T(8,128)(2,1)}, bf16[64,2048]{1,0:T(8,128)(2,1)}, u32[]{:S(2)}, u32[]{:S(2)}) collective-permute-start(bf16[64,2048]{1,0:T(8,128)(2,1)} %collective-permute-done.5.refs_3_), channel_id=1, source_target_pairs={{0,1},{1,0},{2,3},{3,2},{4,5},{5,4},{6,7},{7,6},{8,9},{9,8},{10,11... | collective-permute-start | bytes 786440 | tf_op jit(solution)/shard_map/ppermute | solution.py:47
  69.8 15.4 %collective-permute-start.27 = (bf16[256,576]{1,0:T(8,128)(2,1)S(1)}, bf16[256,576]{1,0:T(8,128)(2,1)S(1)}, u32[]{:S(2)}, u32[]{:S(2)}) collective-permute-start(bf16[256,576]{1,0:T(8,128)(2,1)S(1)} %latents.1.refs_0_), channel_id=1, source_target_pairs={{0,2},{2,0},{4,6},{6,4},{8,10},{10,8},{12,14},{14,12},{16,18},{18,... | collective-permute-start | bytes 884744 | tf_op jit(solution)/shard_map/ppermute | solution.py:43
  70.4 16.4 %collective-permute-start.28 = (bf16[256,576]{1,0:T(8,128)(2,1)S(1)}, bf16[256,576]{1,0:T(8,128)(2,1)S(1)}, u32[]{:S(2)}, u32[]{:S(2)}) collective-permute-start(bf16[256,576]{1,0:T(8,128)(2,1)S(1)} %latents.1.refs_0_), channel_id=1, source_target_pairs={{0,4},{2,6},{4,0},{6,2},{8,12},{10,14},{12,8},{14,10},{16,20},{18,... | collective-permute-start | bytes 884744 | tf_op jit(solution)/shard_map/ppermute | solution.py:43
  71.8 15.0 %collective-permute-start.29 = (bf16[256,576]{1,0:T(8,128)(2,1)S(1)}, bf16[256,576]{1,0:T(8,128)(2,1)S(1)}, u32[]{:S(2)}, u32[]{:S(2)}) collective-permute-start(bf16[256,576]{1,0:T(8,128)(2,1)S(1)} %latents.1.refs_0_), channel_id=1, source_target_pairs={{0,6},{2,4},{4,2},{6,0},{8,14},{10,12},{12,10},{14,8},{16,22},{18,... | collective-permute-start | bytes 884744 | tf_op jit(solution)/shard_map/ppermute | solution.py:43
  87.4 13.0 %collective-permute-start.26 = (bf16[30,1024]{1,0:T(8,128)(2,1)S(1)}, bf16[30,1024]{1,0:T(8,128)(2,1)S(1)}, u32[]{:S(2)}, u32[]{:S(2)}) collective-permute-start(bf16[30,1024]{1,0:T(8,128)(2,1)S(1)} %slice.252), channel_id=1, source_target_pairs={{0,2},{2,4},{4,6},{6,8},{8,10},{10,12},{12,14},{14,16},{16,18},{18... | collective-permute-start | bytes 184328 | tf_op jit(solution)/shard_map/ppermute | solution.py:388
  (37 other events, 276.4 us)

commit v6 on v4

--- a/solution.py
+++ b/solution.py
@@ -41,6 +41,14 @@
 
     def inner_swap(self, block, mask):
         return lax.ppermute(block, "sp", [(i, i ^ mask) for i in range(self.sp_count)])
+
+    def inner_forward(self, block):
+        half = block.shape[0] // 2
+        if self.inner != 4 or half == 0:
+            return [(k, 0) for k in range(self.inner)], self.inner_gather(block)
+        one, two = self.inner_swap(block, 1), self.inner_swap(block, 2)
+        low, high = self.inner_swap(two[:half], 1), self.inner_swap(one[half:], 2)
+        return [(0, 0), (1, 0), (2, 0), (3, 0), (3, half)], [block, one, two, low, high]
 
     def tp_shift(self, block, distance):
         route = [(i, (i + distance) % self.tp_count) for i in range(self.tp_count)]
@@ -130,10 +138,10 @@
             out_ref[h, :, rank:] = turned(rope[:, :half], rope[:, half:], cosine, sine)
 
 
-def latent_kernel(place, rank, share, *refs):
+def latent_kernel(place, rank, share, parts, *refs):
     outer, inner, tp = place.outer, place.inner, place.tp_count
     tables = tp if share else 1
-    n_rows, n_w = outer, tables * inner
+    n_rows, n_w = outer, tables * len(parts)
     row_refs, w_refs = refs[:n_rows], refs[n_rows : n_rows + n_w]
     gain_ref, cos_ref, sin_ref, out_ref, rows, weight = refs[n_rows + n_w :]
     zi, xi, ti = place.indices()
@@ -142,10 +150,10 @@
     count = row_refs[0].shape[0]
     for t in range(tables):
         owner = behind(ti, t, tp) if share else 0
-        for k in range(inner):
-            for j in range(outer):
-                start = ((zi ^ j) * inner + (xi ^ k)) * block + owner * piece
-                weight[pl.ds(pl.multiple_of(start, piece), piece)] = w_refs[t * inner + k][j]
+        for (k, first), ref in zip(parts, w_refs[t * len(parts) :]):
+            for j in range(ref.shape[0]):
+                start = ((zi ^ (first + j)) * inner + (xi ^ k)) * block + owner * piece
+                weight[pl.ds(pl.multiple_of(start, piece), piece)] = ref[j]
     for j in range(outer):
         rows[j * count : (j + 1) * count] = row_refs[j][...]
     pre = jnp.dot(rows[...], weight[...], preferred_element_type=jnp.float32)
@@ -159,19 +167,20 @@
     out_ref[:, rank:] = turned(rope[:, :half], rope[:, half:], cosine, sine)
 
 
-def gated_kernel(place, *refs):
+def gated_kernel(place, parts, *refs):
     outer, inner, tp = place.outer, place.inner, place.tp_count
     n_rows = tp * outer
-    row_refs, w_refs = refs[:n_rows], refs[n_rows : n_rows + inner]
-    outs = refs[n_rows + inner : n_rows + inner + outer]
-    rows, weight = refs[n_rows + inner + outer :]
+    n_w = len(parts)
+    row_refs, w_refs = refs[:n_rows], refs[n_rows : n_rows + n_w]
+    outs = refs[n_rows + n_w : n_rows + n_w + outer]
+    rows, weight = refs[n_rows + n_w + outer :]
     zi, xi, ti = place.indices()
     block = w_refs[0].shape[1]
     count = row_refs[0].shape[0]
-    for k in range(inner):
-        for j in range(outer):
-            start = ((zi ^ j) * inner + (xi ^ k)) * block
-            weight[pl.ds(pl.multiple_of(start, block), block)] = w_refs[k][j]
+    for (k, first), ref in zip(parts, w_refs):
+        for j in range(ref.shape[0]):
+            start = ((zi ^ (first + j)) * inner + (xi ^ k)) * block
+            weight[pl.ds(pl.multiple_of(start, block), block)] = ref[j]
     for t in range(tp):
         owner = behind(ti, t, tp)
         for j in range(outer):
@@ -286,8 +295,7 @@
         columns.append(block if j == 0 else place.outer_swap(block, j))
 
     table = jnp.stack(table_parts)
-    table, tokens = lax.optimization_barrier((table, tokens))
-    tables = place.inner_gather(table)
+    table_map, tables = place.inner_forward(table)
 
     gathered = lax.all_gather(tokens, "tp", axis=1, tiled=True)
     features = gathered.astype(jnp.float32)
@@ -301,7 +309,7 @@
     rows = place.outer_forward(own_rows)
     weight_block = jnp.stack(columns)
     weight_block, query_rows = lax.optimization_barrier((weight_block, normed))
-    weight_blocks = place.inner_gather(weight_block)
+    weight_map, weight_blocks = place.inner_forward(weight_block)
 
     bf16 = jnp.bfloat16
     model = normed.shape[1]
@@ -337,12 +345,14 @@
         name="queries",
     )(query_rows, w_query, key_up_weight, cosine, sine)
 
-    rows, tables, _ = lax.optimization_barrier((rows, tables, queries))
+    tables, _ = lax.optimization_barrier((tables, queries))
+    tap_rows = [conv_taps[n].astype(jnp.float32) for n in range(conv_taps.shape[0])]
+    rows, tap_rows, _ = lax.optimization_barrier((rows, tap_rows, queries))
     if split_rows:
         tables = sum(place.tp_gather(tables), [])
 
     latent = pl.pallas_call(
-        functools.partial(latent_kernel, place, rank, split_rows),
+        functools.partial(latent_kernel, place, rank, split_rows, table_map),
         out_shape=jax.ShapeDtypeStruct((outer * share, rank + QK_ROPE), bf16),
         in_specs=[whole_vmem()] * (outer + len(tables) + 3),
         out_specs=whole_vmem(),
@@ -364,9 +374,9 @@
 
     all_rows = sum(place.tp_gather(rows), [])
     gated = pl.pallas_call(
-        functools.partial(gated_kernel, place),
+        functools.partial(gated_kernel, place, weight_map),
         out_shape=[jax.ShapeDtypeStruct((row_count, width), bf16)] * outer,
-        in_specs=[whole_vmem()] * (len(all_rows) + inner),
+        in_specs=[whole_vmem()] * (len(all_rows) + len(weight_blocks)),
         out_specs=[whole_vmem()] * outer,
         scratch_shapes=[
             pltpu.VMEM((outer * row_count, model), bf16),
@@ -418,7 +428,7 @@
     for tap_index in range(conv_taps.shape[0]):
         mixed = (
             mixed
-            + conv_taps[tap_index].astype(jnp.float32) * padded[tap_index : tap_index + row_count]
+            + tap_rows[tap_index] * padded[tap_index : tap_index + row_count]
         )
     channel_total = mixed.shape[1] * tp_count
     stats = jnp.stack([jnp.sum(mixed, axis=1), jnp.sum(mixed * mixed, axis=1)])

time: 115 us -> 111 us (0.965)
  waiting for transfers between devices: 38.5 us -> 24.3 us
  starting transfers between devices: 39.4 us -> 50.2 us
    ppermute x9 -> x11, waiting for transfers between devices: 22.8 us -> 11.7 us  [inner_swap(): lax.ppermute(block, 'sp', [(i, i ^ mask) for i in range(self.sp_count)])]
    ppermute x12, starting transfers between devices: 21.7 us -> 29 us  [outer_swap(): lax.ppermute(block, 'sp', [(i, i ^ mask) for i in range(self.sp_count)])]
    ppermute x12, waiting for transfers between devices: 13.2 us -> 8.37 us  [outer_swap(): lax.ppermute(block, 'sp', [(i, i ^ mask) for i in range(self.sp_count)])]
    ppermute x9 -> x11, starting transfers between devices: 11.5 us -> 13.7 us  [inner_swap(): lax.ppermute(block, 'sp', [(i, i ^ mask) for i in range(self.sp_count)])]
    ppermute x14 -> x15, waiting for transfers between devices: 2.55 us -> 4.19 us  [tp_shift(): return lax.ppermute(block, 'tp', route)]
    mul x2 -> x0, other arithmetic: 1.32 us -> none  [local(): conv_taps[tap_index].astype(jnp.float32)]
    convert_element_type x0 -> x2, other arithmetic: none -> 1.31 us  [local(): conv_taps[n].astype(jnp.float32)]
    ppermute x14 -> x15, starting transfers between devices: 3.36 us -> 3.6 us  [tp_shift(): return lax.ppermute(block, 'tp', route)]
  transfers between devices with their start and end apart: 36 -> 39, of which waited for: 11 -> 10; matrix products, arithmetic and copies ran while one was open for 5% -> 6% of each run, Pallas kernels for 15% -> 16%
where the time goes in v6:
time: 111 us
  starting transfers between devices  50.2 us (45%)
  waiting for transfers between devices  24.3 us (22%)
  Pallas kernels  17.6 us (16%)
  other arithmetic  9.01 us (8%)
  matrix products  3.78 us (3%)
  local copies, waits for them, and re-layouts  2.38 us (2%)
  blocking collectives  2.38 us (2%)
  between operations  1.48 us (1%)
    ppermute x12, starting transfers between devices, outer_swap(): lax.ppermute(block, 'sp', [(i, i ^ mask) for i in range(self.sp_count)])  29 us
    ppermute x11, starting transfers between devices, inner_swap(): lax.ppermute(block, 'sp', [(i, i ^ mask) for i in range(self.sp_count)])  13.7 us
    ppermute x11, waiting for transfers between devices, inner_swap(): lax.ppermute(block, 'sp', [(i, i ^ mask) for i in range(self.sp_count)])  11.7 us
    pallas_call x1, Pallas kernels, local(): pl.pallas_call(functools.partial(attention_kernel, place, score_scale, ra...  9.32 us
    ppermute x12, waiting for transfers between devices, outer_swap(): lax.ppermute(block, 'sp', [(i, i ^ mask) for i in range(self.sp_count)])  8.37 us
    pallas_call x1, Pallas kernels, local(): pl.pallas_call(functools.partial(query_kernel, rank), out_shape=jax.Shape...  5.5 us
    ppermute x15, waiting for transfers between devices, tp_shift(): return lax.ppermute(block, 'tp', route)  4.19 us
    ppermute x1, starting transfers between devices, local(): lax.ppermute(gated_rows[row_count - conv_reach:], 'sp', [(i, i + 1) for i...  3.84 us
  transfers between devices with their start and end apart: 39, of which 10 were waited for; matrix products, arithmetic and copies ran while one was open for 6% of the time, Pallas kernels for 16%

profile of v6, /device:TPU:0, one launch (start us, length us, event | category | flops | bytes accessed | tf_op | source)
XLA Modules:
  0.0 111.1 jit_solution(6048105129413604761)
XLA Ops:
  2.4 3.1 %collective-permute-start.6 = (bf16[64,576]{1,0:T(8,128)(2,1)S(1)}, bf16[64,576]{1,0:T(8,128)(2,1)S(1)}, u32[]{:S(2)}, u32[]{:S(2)}) collective-permute-start(bf16[64,576]{1,0:T(8,128)(2,1)S(1)} %fusion.38), channel_id=1, source_target_pairs={{0,8},{2,10},{4,12},{6,14},{8,0},{10,2},{12,4},{14,6},{16,24},{18,... | collective-permute-start | bytes 221192 | tf_op jit(solution)/shard_map/ppermute | solution.py:40
  5.5 2.6 %collective-permute-start.7 = (bf16[64,576]{1,0:T(8,128)(2,1)S(1)}, bf16[64,576]{1,0:T(8,128)(2,1)S(1)}, u32[]{:S(2)}, u32[]{:S(2)}) collective-permute-start(bf16[64,576]{1,0:T(8,128)(2,1)S(1)} %fusion.38), channel_id=1, source_target_pairs={{0,16},{2,18},{4,20},{6,22},{8,24},{10,26},{12,28},{14,30},{16,0},... | collective-permute-start | bytes 221192 | tf_op jit(solution)/shard_map/ppermute | solution.py:40
  10.2 3.6 %collective-permute-start.1 = (bf16[128,512]{1,0:T(8,128)(2,1)S(1)}, bf16[128,512]{1,0:T(8,128)(2,1)S(1)}, u32[]{:S(2)}, u32[]{:S(2)}) collective-permute-start(bf16[128,512]{1,0:T(8,128)(2,1)S(1)} %pad_maximum_fusion.4), channel_id=1, source_target_pairs={{0,16},{2,18},{4,20},{6,22},{8,24},{10,26},{12,28},{14,30},{16,0},... | collective-permute-start | bytes 393224 | tf_op jit(solution)/shard_map/ppermute | solution.py:40
  13.7 2.4 %all_gather.3 = bf16[128,2048]{1,0:T(8,128)(2,1)S(1)} all-gather(bf16[128,1024]{1,0:T(8,128)(2,1)} %param.14), channel_id=1, replica_groups=mesh['sp'=16,'tp'=2] {'tp'}, dimensions={1}, use_global_device_ids=true | all-gather | bytes 786432 | tf_op jit(solution)/shard_map/all_gather | solution.py:300
  19.1 1.6 %collective-permute-start.10 = (bf16[4,64,576]{2,1,0:T(8,128)(2,1)S(1)}, bf16[4,64,576]{2,1,0:T(8,128)(2,1)S(1)}, u32[]{:S(2)}, u32[]{:S(2)}) collective-permute-start(bf16[4,64,576]{2,1,0:T(8,128)(2,1)S(1)} %pad_maximum_fusion.1.refs_4_), channel_id=1, source_target_pairs={{0,4},{2,6},{4,0},{6,2},{8,12},{10,14},{12,8},{14,10},{16,20},{18,... | collective-permute-start | bytes 884744 | tf_op jit(solution)/shard_map/ppermute | solution.py:43
  20.7 1.5 %collective-permute-start.9 = (bf16[4,64,576]{2,1,0:T(8,128)(2,1)S(1)}, bf16[4,64,576]{2,1,0:T(8,128)(2,1)S(1)}, u32[]{:S(2)}, u32[]{:S(2)}) collective-permute-start(bf16[4,64,576]{2,1,0:T(8,128)(2,1)S(1)} %pad_maximum_fusion.1.refs_4_), channel_id=1, source_target_pairs={{0,2},{2,0},{4,6},{6,4},{8,10},{10,8},{12,14},{14,12},{16,18},{18,... | collective-permute-start | bytes 884744 | tf_op jit(solution)/shard_map/ppermute | solution.py:43
  23.0 7.4 %collective-permute-start.3 = (bf16[64,2048]{1,0:T(8,128)(2,1)S(1)}, bf16[64,2048]{1,0:T(8,128)(2,1)S(1)}, u32[]{:S(2)}, u32[]{:S(2)}) collective-permute-start(bf16[64,2048]{1,0:T(8,128)(2,1)S(1)} %constant_dynamic-slice_fusion.1.refs_0_), channel_id=1, source_target_pairs={{0,8},{2,10},{4,12},{6,14},{8,0},{10,2},{12,4},{14,6},{16,24},{18,... | collective-permute-start | bytes 786440 | tf_op jit(solution)/shard_map/ppermute | solution.py:40
  30.4 1.6 %collective-permute-start.30 = (bf16[4,128,512]{2,1,0:T(8,128)(2,1)S(1)}, bf16[4,128,512]{2,1,0:T(8,128)(2,1)S(1)}, u32[]{:S(2)}, u32[]{:S(2)}) collective-permute-start(bf16[4,128,512]{2,1,0:T(8,128)(2,1)S(1)} %pad_maximum_fusion.refs_8_), channel_id=1, source_target_pairs={{0,4},{2,6},{4,0},{6,2},{8,12},{10,14},{12,8},{14,10},{16,20},{18,... | collective-permute-start | bytes 1572872 | tf_op jit(solution)/shard_map/ppermute | solution.py:43
  32.0 1.5 %collective-permute-start.29 = (bf16[4,128,512]{2,1,0:T(8,128)(2,1)S(1)}, bf16[4,128,512]{2,1,0:T(8,128)(2,1)S(1)}, u32[]{:S(2)}, u32[]{:S(2)}) collective-permute-start(bf16[4,128,512]{2,1,0:T(8,128)(2,1)S(1)} %pad_maximum_fusion.refs_8_), channel_id=1, source_target_pairs={{0,2},{2,0},{4,6},{6,4},{8,10},{10,8},{12,14},{14,12},{16,18},{18,... | collective-permute-start | bytes 1572872 | tf_op jit(solution)/shard_map/ppermute | solution.py:43
  34.2 4.0 %collective-permute-done.4.refs_2_ = bf16[64,2048]{1,0:T(8,128)(2,1)S(1)} collective-permute-done((bf16[64,2048]{1,0:T(8,128)(2,1)S(1)}, bf16[64,2048]{1,0:T(8,128)(2,1)S(1)}, u32[]{:S(2)}, u32[]{:S(2)}) %collective-permute-start.4) | collective-permute-done | bytes 262176 | tf_op jit(solution)/shard_map/ppermute | solution.py:40
  38.1 1.5 %collective-permute-start.12 = (bf16[2,64,576]{2,1,0:T(8,128)(2,1)S(1)}, bf16[2,64,576]{2,1,0:T(8,128)(2,1)S(1)}, u32[]{:S(2)}, u32[]{:S(2)}) collective-permute-start(bf16[2,64,576]{2,1,0:T(8,128)(2,1)S(1)} %slice.269), channel_id=1, source_target_pairs={{0,4},{2,6},{4,0},{6,2},{8,12},{10,14},{12,8},{14,10},{16,20},{18,... | collective-permute-start | bytes 442376 | tf_op jit(solution)/shard_map/ppermute | solution.py:43
  40.3 4.1 %collective-permute-done.11.refs_7_ = bf16[2,64,576]{2,1,0:T(8,128)(2,1)S(1)} collective-permute-done((bf16[2,64,576]{2,1,0:T(8,128)(2,1)S(1)}, bf16[2,64,576]{2,1,0:T(8,128)(2,1)S(1)}, u32[]{:S(2)}, u32[]{:S(2)}) %collective-permute-start.11) | collective-permute-done | bytes 147488 | tf_op jit(solution)/shard_map/ppermute | solution.py:43
  44.4 6.5 %collective-permute-start.5 = (bf16[64,2048]{1,0:T(8,128)(2,1)S(1)}, bf16[64,2048]{1,0:T(8,128)(2,1)S(1)}, u32[]{:S(2)}, u32[]{:S(2)}) collective-permute-start(bf16[64,2048]{1,0:T(8,128)(2,1)S(1)} %collective-permute-done.4.refs_2_), channel_id=1, source_target_pairs={{0,8},{2,10},{4,12},{6,14},{8,0},{10,2},{12,4},{14,6},{16,24},{18,... | collective-permute-start | bytes 786440 | tf_op jit(solution)/shard_map/ppermute | solution.py:40
  50.9 5.5 %queries.1.q_ref = bf16[8,128,576]{2,1,0:T(8,128)(2,1)} custom-call(bf16[128,2048]{1,0:T(8,128)(2,1)S(1)} %fusion.3.normed_ref, bf16[2048,1536]{1,0:T(8,128)(2,1)} %w_ref.1, bf16[512,1024]{1,0:T(8,128)(2,1)S(1)} %copy-done.1, f32[384,32]{1,0:T(8,128)S(1)} %get-tuple-element.165.cos_ref.refs_15_, f32[384,32]{1,0:T(8,128)S(1)} %get-tuple-element.164.sin_ref.refs_16_), custom_call_target="tpu_custom_call" | custom-call | flops 805306368 | bytes 6291456 | tf_op jit(solution)/shard_map/queries/pallas_call | solution.py:329
  58.8 1.6 %collective-permute-done.17.refs_13_ = bf16[2,64,576]{2,1,0:T(8,128)(2,1)S(1)} collective-permute-done((bf16[2,64,576]{2,1,0:T(8,128)(2,1)S(1)}, bf16[2,64,576]{2,1,0:T(8,128)(2,1)S(1)}, u32[]{:S(2)}, u32[]{:S(2)}) %collective-permute-start.17) | collective-permute-done | bytes 147488 | tf_op jit(solution)/shard_map/ppermute | solution.py:55
  65.0 4.7 %collective-permute-done.31.refs_11_ = bf16[2,128,512]{2,1,0:T(8,128)(2,1)S(1)} collective-permute-done((bf16[2,128,512]{2,1,0:T(8,128)(2,1)S(1)}, bf16[2,128,512]{2,1,0:T(8,128)(2,1)S(1)}, u32[]{:S(2)}, u32[]{:S(2)}) %collective-permute-start.31) | collective-permute-done | bytes 262176 | tf_op jit(solution)/shard_map/ppermute | solution.py:43
  70.4 2.3 %collective-permute-start.20 = (bf16[256,576]{1,0:T(8,128)(2,1)S(1)}, bf16[256,576]{1,0:T(8,128)(2,1)}, u32[]{:S(2)}, u32[]{:S(2)}) collective-permute-start(bf16[256,576]{1,0:T(8,128)(2,1)S(1)} %latents.1.refs_0_), channel_id=1, source_target_pairs={{0,6},{2,4},{4,2},{6,0},{8,14},{10,12},{12,10},{14,8},{16,22},{18,... | collective-permute-start | bytes 884744 | tf_op jit(solution)/shard_map/ppermute | solution.py:43
  74.1 2.4 %collective-permute-start.33 = (bf16[128,256]{1,0:T(8,128)(2,1)S(1)}, bf16[128,256]{1,0:T(8,128)(2,1)}, u32[]{:S(2)}, u32[]{:S(2)}) collective-permute-start(bf16[128,256]{1,0:T(8,128)(2,1)S(1)} %get-tuple-element.81), channel_id=1, source_target_pairs={{0,24},{2,26},{4,28},{6,30},{8,16},{10,18},{12,20},{14,22},{16,8},... | collective-permute-start | bytes 196616 | tf_op jit(solution)/shard_map/ppermute | solution.py:40
  76.5 4.0 %collective-permute-done.33 = bf16[128,256]{1,0:T(8,128)(2,1)} collective-permute-done((bf16[128,256]{1,0:T(8,128)(2,1)S(1)}, bf16[128,256]{1,0:T(8,128)(2,1)}, u32[]{:S(2)}, u32[]{:S(2)}) %collective-permute-start.33) | collective-permute-done | bytes 65568 | tf_op jit(solution)/shard_map/ppermute | solution.py:40
  82.5 2.8 %collective-permute-done.19.refs_2_ = bf16[256,576]{1,0:T(8,128)(2,1)S(1)} collective-permute-done((bf16[256,576]{1,0:T(8,128)(2,1)S(1)}, bf16[256,576]{1,0:T(8,128)(2,1)S(1)}, u32[]{:S(2)}, u32[]{:S(2)}) %collective-permute-start.19) | collective-permute-done | bytes 294944 | tf_op jit(solution)/shard_map/ppermute | solution.py:43
  86.8 3.8 %collective-permute-start.36 = (bf16[30,1024]{1,0:T(8,128)(2,1)S(1)}, bf16[30,1024]{1,0:T(8,128)(2,1)S(1)}, u32[]{:S(2)}, u32[]{:S(2)}) collective-permute-start(bf16[30,1024]{1,0:T(8,128)(2,1)S(1)} %slice.272), channel_id=1, source_target_pairs={{0,2},{2,4},{4,6},{6,8},{8,10},{10,12},{12,14},{14,16},{16,18},{18... | collective-permute-start | bytes 184328 | tf_op jit(solution)/shard_map/ppermute | solution.py:397
  90.7 9.3 %attention.1 = (bf16[128,1024]{1,0:T(8,128)(2,1)S(1)}, f32[8,128]{1,0:T(8,128)}) custom-call(bf16[8,128,576]{2,1,0:T(8,128)(2,1)S(1)} %copy-done, bf16[512,1024]{1,0:T(8,128)(2,1)S(1)} %copy-done.3, bf16[256,576]{1,0:T(8,128)(2,1)S(1)} %latents.1.refs_0_, bf16[256,576]{1,0:T(8,128)(2,1)S(1)} %collective-permute-done.18.refs_1_, ...), custom_call_target="tpu_custom_call" | custom-call | flops 4563402752 | bytes 2359296 | tf_op jit(solution)/shard_map/attention/pallas_call | solution.py:404
  101.4 2.9 %fusion.43 = (f32[128]{0:T(128)S(1)}, f32[128]{0:T(128)S(1)}, f32[128,1024]{1,0:T(8,128)S(1)}) fusion(f32[158,1024]{1,0:T(8,128)S(1)} %maximum_convert_fusion, f32[1024]{0:T(1024)S(1)} %bitcast.65, f32[1024]{0:T(1024)S(1)} %bitcast.84, f32[1024]{0:T(1024)S(1)} %bitcast.66, f32[1024]{0:T(1024)S(1)} %bitcast.67, f32[1024]{0:T(1024)S(1)} %bitcast.68, ...), kind=kLoop, calls=%fused_computation.150 | loop fusion | flops 8388352 | bytes 16905216 | tf_op jit(solution)/shard_map/reduce_sum | solution.py:434
  105.6 3.1 %fusion = bf16[128,2048]{1,0:T(8,128)(2,1)S(1)} fusion(f32[128,2048]{1,0:T(8,128)S(1)} %fusion.45, bf16[1024,2048]{1,0:T(8,128)(2,1)} %param.26, f32[128,1024]{1,0:T(8,128)S(1)} %get-tuple-element.120, f32[1024]{0:T(1024)S(1)} %copy-done.33, f32[128]{0:T(128)S(1)} %fusion.40, f32[128]{0:T(128)S(1)} %multiply_bitcast_fusion), kind=kOutput, calls=%fused_computation.1 | convolution fusion | flops 538443776 | bytes 6296576 | tf_op jit(solution)/shard_map/dot_general | solution.py:445
  (166 shorter events, 26.0 us)
Async XLA Ops:
  2.4 15.0 %collective-permute-start.6 = (bf16[64,576]{1,0:T(8,128)(2,1)S(1)}, bf16[64,576]{1,0:T(8,128)(2,1)S(1)}, u32[]{:S(2)}, u32[]{:S(2)}) collective-permute-start(bf16[64,576]{1,0:T(8,128)(2,1)S(1)} %fusion.38), channel_id=1, source_target_pairs={{0,8},{2,10},{4,12},{6,14},{8,0},{10,2},{12,4},{14,6},{16,24},{18,... | collective-permute-start | bytes 221192 | tf_op jit(solution)/shard_map/ppermute | solution.py:40
  5.5 12.1 %collective-permute-start.7 = (bf16[64,576]{1,0:T(8,128)(2,1)S(1)}, bf16[64,576]{1,0:T(8,128)(2,1)S(1)}, u32[]{:S(2)}, u32[]{:S(2)}) collective-permute-start(bf16[64,576]{1,0:T(8,128)(2,1)S(1)} %fusion.38), channel_id=1, source_target_pairs={{0,16},{2,18},{4,20},{6,22},{8,24},{10,26},{12,28},{14,30},{16,0},... | collective-permute-start | bytes 221192 | tf_op jit(solution)/shard_map/ppermute | solution.py:40
  8.1 10.9 %collective-permute-start.8 = (bf16[64,576]{1,0:T(8,128)(2,1)S(1)}, bf16[64,576]{1,0:T(8,128)(2,1)S(1)}, u32[]{:S(2)}, u32[]{:S(2)}) collective-permute-start(bf16[64,576]{1,0:T(8,128)(2,1)S(1)} %fusion.38), channel_id=1, source_target_pairs={{0,24},{2,26},{4,28},{6,30},{8,16},{10,18},{12,20},{14,22},{16,8},... | collective-permute-start | bytes 221192 | tf_op jit(solution)/shard_map/ppermute | solution.py:40
  9.2 11.5 %collective-permute-start = (bf16[128,512]{1,0:T(8,128)(2,1)S(1)}, bf16[128,512]{1,0:T(8,128)(2,1)S(1)}, u32[]{:S(2)}, u32[]{:S(2)}) collective-permute-start(bf16[128,512]{1,0:T(8,128)(2,1)S(1)} %pad_maximum_fusion.3), channel_id=1, source_target_pairs={{0,8},{2,10},{4,12},{6,14},{8,0},{10,2},{12,4},{14,6},{16,24},{18,... | collective-permute-start | bytes 393224 | tf_op jit(solution)/shard_map/ppermute | solution.py:40
  10.2 12.8 %collective-permute-start.1 = (bf16[128,512]{1,0:T(8,128)(2,1)S(1)}, bf16[128,512]{1,0:T(8,128)(2,1)S(1)}, u32[]{:S(2)}, u32[]{:S(2)}) collective-permute-start(bf16[128,512]{1,0:T(8,128)(2,1)S(1)} %pad_maximum_fusion.4), channel_id=1, source_target_pairs={{0,16},{2,18},{4,20},{6,22},{8,24},{10,26},{12,28},{14,30},{16,0},... | collective-permute-start | bytes 393224 | tf_op jit(solution)/shard_map/ppermute | solution.py:40
  17.5 12.9 %collective-permute-start.2 = (bf16[128,512]{1,0:T(8,128)(2,1)S(1)}, bf16[128,512]{1,0:T(8,128)(2,1)S(1)}, u32[]{:S(2)}, u32[]{:S(2)}) collective-permute-start(bf16[128,512]{1,0:T(8,128)(2,1)S(1)} %pad_maximum_fusion.5), channel_id=1, source_target_pairs={{0,24},{2,26},{4,28},{6,30},{8,16},{10,18},{12,20},{14,22},{16,8},... | collective-permute-start | bytes 393224 | tf_op jit(solution)/shard_map/ppermute | solution.py:40
  17.6 20.6 %collective-permute-start.4 = (bf16[64,2048]{1,0:T(8,128)(2,1)S(1)}, bf16[64,2048]{1,0:T(8,128)(2,1)S(1)}, u32[]{:S(2)}, u32[]{:S(2)}) collective-permute-start(bf16[64,2048]{1,0:T(8,128)(2,1)S(1)} %constant_dynamic-slice_fusion.1.refs_0_), channel_id=1, source_target_pairs={{0,16},{2,18},{4,20},{6,22},{8,24},{10,26},{12,28},{14,30},{16,0},... | collective-permute-start | bytes 786440 | tf_op jit(solution)/shard_map/ppermute | solution.py:40
  19.1 12.9 %collective-permute-start.10 = (bf16[4,64,576]{2,1,0:T(8,128)(2,1)S(1)}, bf16[4,64,576]{2,1,0:T(8,128)(2,1)S(1)}, u32[]{:S(2)}, u32[]{:S(2)}) collective-permute-start(bf16[4,64,576]{2,1,0:T(8,128)(2,1)S(1)} %pad_maximum_fusion.1.refs_4_), channel_id=1, source_target_pairs={{0,4},{2,6},{4,0},{6,2},{8,12},{10,14},{12,8},{14,10},{16,20},{18,... | collective-permute-start | bytes 884744 | tf_op jit(solution)/shard_map/ppermute | solution.py:43
  20.7 12.9 %collective-permute-start.9 = (bf16[4,64,576]{2,1,0:T(8,128)(2,1)S(1)}, bf16[4,64,576]{2,1,0:T(8,128)(2,1)S(1)}, u32[]{:S(2)}, u32[]{:S(2)}) collective-permute-start(bf16[4,64,576]{2,1,0:T(8,128)(2,1)S(1)} %pad_maximum_fusion.1.refs_4_), channel_id=1, source_target_pairs={{0,2},{2,0},{4,6},{6,4},{8,10},{10,8},{12,14},{14,12},{16,18},{18,... | collective-permute-start | bytes 884744 | tf_op jit(solution)/shard_map/ppermute | solution.py:43
  23.0 33.5 %collective-permute-start.3 = (bf16[64,2048]{1,0:T(8,128)(2,1)S(1)}, bf16[64,2048]{1,0:T(8,128)(2,1)S(1)}, u32[]{:S(2)}, u32[]{:S(2)}) collective-permute-start(bf16[64,2048]{1,0:T(8,128)(2,1)S(1)} %constant_dynamic-slice_fusion.1.refs_0_), channel_id=1, source_target_pairs={{0,8},{2,10},{4,12},{6,14},{8,0},{10,2},{12,4},{14,6},{16,24},{18,... | collective-permute-start | bytes 786440 | tf_op jit(solution)/shard_map/ppermute | solution.py:40
  30.4 27.4 %collective-permute-start.30 = (bf16[4,128,512]{2,1,0:T(8,128)(2,1)S(1)}, bf16[4,128,512]{2,1,0:T(8,128)(2,1)S(1)}, u32[]{:S(2)}, u32[]{:S(2)}) collective-permute-start(bf16[4,128,512]{2,1,0:T(8,128)(2,1)S(1)} %pad_maximum_fusion.refs_8_), channel_id=1, source_target_pairs={{0,4},{2,6},{4,0},{6,2},{8,12},{10,14},{12,8},{14,10},{16,20},{18,... | collective-permute-start | bytes 1572872 | tf_op jit(solution)/shard_map/ppermute | solution.py:43
  32.0 26.2 %collective-permute-start.29 = (bf16[4,128,512]{2,1,0:T(8,128)(2,1)S(1)}, bf16[4,128,512]{2,1,0:T(8,128)(2,1)S(1)}, u32[]{:S(2)}, u32[]{:S(2)}) collective-permute-start(bf16[4,128,512]{2,1,0:T(8,128)(2,1)S(1)} %pad_maximum_fusion.refs_8_), channel_id=1, source_target_pairs={{0,2},{2,0},{4,6},{6,4},{8,10},{10,8},{12,14},{14,12},{16,18},{18,... | collective-permute-start | bytes 1572872 | tf_op jit(solution)/shard_map/ppermute | solution.py:43
  33.5 10.9 %collective-permute-start.11 = (bf16[2,64,576]{2,1,0:T(8,128)(2,1)S(1)}, bf16[2,64,576]{2,1,0:T(8,128)(2,1)S(1)}, u32[]{:S(2)}, u32[]{:S(2)}) collective-permute-start(bf16[2,64,576]{2,1,0:T(8,128)(2,1)S(1)} %slice.268), channel_id=1, source_target_pairs={{0,2},{2,0},{4,6},{6,4},{8,10},{10,8},{12,14},{14,12},{16,18},{18,... | collective-permute-start | bytes 442376 | tf_op jit(solution)/shard_map/ppermute | solution.py:43
  38.1 18.3 %collective-permute-start.12 = (bf16[2,64,576]{2,1,0:T(8,128)(2,1)S(1)}, bf16[2,64,576]{2,1,0:T(8,128)(2,1)S(1)}, u32[]{:S(2)}, u32[]{:S(2)}) collective-permute-start(bf16[2,64,576]{2,1,0:T(8,128)(2,1)S(1)} %slice.269), channel_id=1, source_target_pairs={{0,4},{2,6},{4,0},{6,2},{8,12},{10,14},{12,8},{14,10},{16,20},{18,... | collective-permute-start | bytes 442376 | tf_op jit(solution)/shard_map/ppermute | solution.py:43
  44.4 13.2 %collective-permute-start.5 = (bf16[64,2048]{1,0:T(8,128)(2,1)S(1)}, bf16[64,2048]{1,0:T(8,128)(2,1)S(1)}, u32[]{:S(2)}, u32[]{:S(2)}) collective-permute-start(bf16[64,2048]{1,0:T(8,128)(2,1)S(1)} %collective-permute-done.4.refs_2_), channel_id=1, source_target_pairs={{0,8},{2,10},{4,12},{6,14},{8,0},{10,2},{12,4},{14,6},{16,24},{18,... | collective-permute-start | bytes 786440 | tf_op jit(solution)/shard_map/ppermute | solution.py:40
  60.6 9.2 %collective-permute-start.31 = (bf16[2,128,512]{2,1,0:T(8,128)(2,1)S(1)}, bf16[2,128,512]{2,1,0:T(8,128)(2,1)S(1)}, u32[]{:S(2)}, u32[]{:S(2)}) collective-permute-start(bf16[2,128,512]{2,1,0:T(8,128)(2,1)S(1)} %slice.270), channel_id=1, source_target_pairs={{0,2},{2,0},{4,6},{6,4},{8,10},{10,8},{12,14},{14,12},{16,18},{18,... | collective-permute-start | bytes 786440 | tf_op jit(solution)/shard_map/ppermute | solution.py:43
  62.6 10.1 %collective-permute-start.27 = (bf16[64,2048]{1,0:T(8,128)(2,1)S(1)}, bf16[64,2048]{1,0:T(8,128)(2,1)S(1)}, u32[]{:S(2)}, u32[]{:S(2)}) collective-permute-start(bf16[64,2048]{1,0:T(8,128)(2,1)S(1)} %collective-permute-done.4.refs_2_), channel_id=1, source_target_pairs={{0,1},{1,0},{2,3},{3,2},{4,5},{5,4},{6,7},{7,6},{8,9},{9,8},{10,11... | collective-permute-start | bytes 786440 | tf_op jit(solution)/shard_map/ppermute | solution.py:55
  62.6 10.1 %collective-permute-start.28 = (bf16[64,2048]{1,0:T(8,128)(2,1)S(1)}, bf16[64,2048]{1,0:T(8,128)(2,1)S(1)}, u32[]{:S(2)}, u32[]{:S(2)}) collective-permute-start(bf16[64,2048]{1,0:T(8,128)(2,1)S(1)} %collective-permute-done.5.refs_3_), channel_id=1, source_target_pairs={{0,1},{1,0},{2,3},{3,2},{4,5},{5,4},{6,7},{7,6},{8,9},{9,8},{10,11... | collective-permute-start | bytes 786440 | tf_op jit(solution)/shard_map/ppermute | solution.py:55
  64.4 17.5 %collective-permute-start.18 = (bf16[256,576]{1,0:T(8,128)(2,1)S(1)}, bf16[256,576]{1,0:T(8,128)(2,1)S(1)}, u32[]{:S(2)}, u32[]{:S(2)}) collective-permute-start(bf16[256,576]{1,0:T(8,128)(2,1)S(1)} %latents.1.refs_0_), channel_id=1, source_target_pairs={{0,2},{2,0},{4,6},{6,4},{8,10},{10,8},{12,14},{14,12},{16,18},{18,... | collective-permute-start | bytes 884744 | tf_op jit(solution)/shard_map/ppermute | solution.py:43
  69.7 15.6 %collective-permute-start.19 = (bf16[256,576]{1,0:T(8,128)(2,1)S(1)}, bf16[256,576]{1,0:T(8,128)(2,1)S(1)}, u32[]{:S(2)}, u32[]{:S(2)}) collective-permute-start(bf16[256,576]{1,0:T(8,128)(2,1)S(1)} %latents.1.refs_0_), channel_id=1, source_target_pairs={{0,4},{2,6},{4,0},{6,2},{8,12},{10,14},{12,8},{14,10},{16,20},{18,... | collective-permute-start | bytes 884744 | tf_op jit(solution)/shard_map/ppermute | solution.py:43
  70.4 14.9 %collective-permute-start.20 = (bf16[256,576]{1,0:T(8,128)(2,1)S(1)}, bf16[256,576]{1,0:T(8,128)(2,1)}, u32[]{:S(2)}, u32[]{:S(2)}) collective-permute-start(bf16[256,576]{1,0:T(8,128)(2,1)S(1)} %latents.1.refs_0_), channel_id=1, source_target_pairs={{0,6},{2,4},{4,2},{6,0},{8,14},{10,12},{12,10},{14,8},{16,22},{18,... | collective-permute-start | bytes 884744 | tf_op jit(solution)/shard_map/ppermute | solution.py:43
  82.0 8.7 %collective-permute-start.21 = (bf16[256,576]{1,0:T(8,128)(2,1)S(1)}, bf16[256,576]{1,0:T(8,128)(2,1)S(1)}, u32[]{:S(2)}, u32[]{:S(2)}) collective-permute-start(bf16[256,576]{1,0:T(8,128)(2,1)S(1)} %latents.1.refs_0_), channel_id=1, source_target_pairs={{0,1},{1,0},{2,3},{3,2},{4,5},{5,4},{6,7},{7,6},{8,9},{9,8},{10,11... | collective-permute-start | bytes 884744 | tf_op jit(solution)/shard_map/ppermute | solution.py:55
  82.0 8.7 %collective-permute-start.22 = (bf16[256,576]{1,0:T(8,128)(2,1)S(1)}, bf16[256,576]{1,0:T(8,128)(2,1)S(1)}, u32[]{:S(2)}, u32[]{:S(2)}) collective-permute-start(bf16[256,576]{1,0:T(8,128)(2,1)S(1)} %collective-permute-done.18.refs_1_), channel_id=1, source_target_pairs={{0,1},{1,0},{2,3},{3,2},{4,5},{5,4},{6,7},{7,6},{8,9},{9,8},{10,11... | collective-permute-start | bytes 884744 | tf_op jit(solution)/shard_map/ppermute | solution.py:55
  86.8 14.2 %collective-permute-start.36 = (bf16[30,1024]{1,0:T(8,128)(2,1)S(1)}, bf16[30,1024]{1,0:T(8,128)(2,1)S(1)}, u32[]{:S(2)}, u32[]{:S(2)}) collective-permute-start(bf16[30,1024]{1,0:T(8,128)(2,1)S(1)} %slice.272), channel_id=1, source_target_pairs={{0,2},{2,4},{4,6},{6,8},{8,10},{10,12},{12,14},{14,16},{16,18},{18... | collective-permute-start | bytes 184328 | tf_op jit(solution)/shard_map/ppermute | solution.py:397
  (49 other events, 268.6 us)

commit v7 on v4

--- a/solution.py
+++ b/solution.py
@@ -67,15 +67,6 @@
 
 def behind(index, distance, count):
     return lax.rem(index - distance + count, count)
-
-
-def untangled(blocks, index):
-    bit = 1
-    while bit < len(blocks):
-        flag = (index & bit) > 0
-        blocks = [jnp.where(flag, blocks[i ^ bit], b) for i, b in enumerate(blocks)]
-        bit *= 2
-    return blocks
 
 
 def copy_all(pairs, sem):
@@ -337,7 +328,9 @@
         name="queries",
     )(query_rows, w_query, key_up_weight, cosine, sine)
 
-    rows, tables, _ = lax.optimization_barrier((rows, tables, queries))
+    tables, _ = lax.optimization_barrier((tables, queries))
+    tap_rows = [conv_taps[n].astype(jnp.float32) for n in range(conv_taps.shape[0])]
+    rows, tap_rows, _ = lax.optimization_barrier((rows, tap_rows, queries))
     if split_rows:
         tables = sum(place.tp_gather(tables), [])
 
@@ -360,7 +353,9 @@
     )(*rows, *tables, latent_norm_gain[None, :], cosine, sine)
     _, *weight_blocks = lax.optimization_barrier((latent, *weight_blocks))
     latents = place.inner_gather(latent)
-    latents = sum(place.tp_gather(latents), [])
+    own = place.tp_gather(latents[:1])
+    others = place.tp_gather(latents[1:])
+    latents = sum([a + b for a, b in zip(own, others)], [])
 
     all_rows = sum(place.tp_gather(rows), [])
     gated = pl.pallas_call(
@@ -381,7 +376,9 @@
         name="gated",
     )(*all_rows, *weight_blocks)
     home = [gated[0]] + [place.outer_swap(gated[j], j) for j in range(1, outer)]
-    gated_rows = jnp.concatenate(untangled(home, zi), axis=1)
+    gated_rows = jnp.zeros((row_count, outer * width), bf16)
+    for j in range(outer):
+        gated_rows = lax.dynamic_update_slice_in_dim(gated_rows, home[j], (zi ^ j) * width, 1)
 
     conv_reach = conv_taps.shape[0] - 1
     prior_rows = lax.ppermute(
@@ -411,17 +408,18 @@
         name="attention",
     )(queries, value_up_weight, *latents)
 
-    attn_part = jnp.dot(attention, w_merge_attn, preferred_element_type=jnp.float32)
-    prior_rows, gated_rows, _ = lax.optimization_barrier((prior_rows, gated_rows, attn_part))
+    prior_rows, gated_rows, _ = lax.optimization_barrier((prior_rows, gated_rows, attention))
     padded = jnp.concatenate([prior_rows, gated_rows], axis=0).astype(jnp.float32)
     mixed = jnp.zeros(gated_rows.shape, jnp.float32)
     for tap_index in range(conv_taps.shape[0]):
         mixed = (
             mixed
-            + conv_taps[tap_index].astype(jnp.float32) * padded[tap_index : tap_index + row_count]
+            + tap_rows[tap_index] * padded[tap_index : tap_index + row_count]
         )
     channel_total = mixed.shape[1] * tp_count
     stats = jnp.stack([jnp.sum(mixed, axis=1), jnp.sum(mixed * mixed, axis=1)])
+    stats, attention = lax.optimization_barrier((stats, attention))
+    attn_part = jnp.dot(attention, w_merge_attn, preferred_element_type=jnp.float32)
     stat_sum, stat_squares = sum(
         [place.tp_shift(stats, t) for t in range(1, tp_count)], start=stats
     )

time: 115 us -> 122 us (1.061)
  waiting for transfers between devices: 38.5 us -> 45.6 us
  local copies, waits for them, and re-layouts: 2.95 us -> 9.38 us
  starting transfers between devices: 39.4 us -> 36 us
  other arithmetic: 8.35 us -> 6.13 us
  Pallas kernels: 17.6 us -> 19.8 us
  matrix products: 3.78 us -> 1.6 us
    ppermute x12, waiting for transfers between devices: 13.2 us -> 25.2 us  [outer_swap(): lax.ppermute(block, 'sp', [(i, i ^ mask) for i in range(self.sp_count)])]
    unnamed x73 -> x35, local copies, waits for them, and re-layouts: 1.69 us -> 8.06 us
    ppermute x9, waiting for transfers between devices: 22.8 us -> 18 us  [inner_swap(): lax.ppermute(block, 'sp', [(i, i ^ mask) for i in range(self.sp_count)])]
    ppermute x12, starting transfers between devices: 21.7 us -> 19.5 us  [outer_swap(): lax.ppermute(block, 'sp', [(i, i ^ mask) for i in range(self.sp_count)])]
    dot_general x1, matrix products: 3.07 us -> 0.88 us  [local(): jnp.dot(conv_out, w_merge_conv, preferred_element_type=jnp.float32)]
    mul x2 -> x0, other arithmetic: 1.32 us -> none  [local(): conv_taps[tap_index].astype(jnp.float32)]
  transfers between devices with their start and end apart: 36 -> 36, of which waited for: 11 -> 12; matrix products, arithmetic and copies ran while one was open for 5% -> 3% of each run, Pallas kernels for 15% -> 16%
where the time goes in v7:
time: 122 us
  waiting for transfers between devices  45.6 us (37%)
  starting transfers between devices  36 us (30%)
  Pallas kernels  19.8 us (16%)
  local copies, waits for them, and re-layouts  9.38 us (8%)
  other arithmetic  6.13 us (5%)
  blocking collectives  2.38 us (2%)
  matrix products  1.6 us (1%)
    ppermute x12, waiting for transfers between devices, outer_swap(): lax.ppermute(block, 'sp', [(i, i ^ mask) for i in range(self.sp_count)])  25.2 us
    ppermute x12, starting transfers between devices, outer_swap(): lax.ppermute(block, 'sp', [(i, i ^ mask) for i in range(self.sp_count)])  19.5 us
    ppermute x9, waiting for transfers between devices, inner_swap(): lax.ppermute(block, 'sp', [(i, i ^ mask) for i in range(self.sp_count)])  18 us
    ppermute x9, starting transfers between devices, inner_swap(): lax.ppermute(block, 'sp', [(i, i ^ mask) for i in range(self.sp_count)])  10.7 us
    pallas_call x1, Pallas kernels, local(): pl.pallas_call(functools.partial(attention_kernel, place, score_scale, ra...  9.62 us
    unnamed x35, local copies, waits for them, and re-layouts  8.06 us
    pallas_call x1, Pallas kernels, local(): pl.pallas_call(functools.partial(query_kernel, rank), out_shape=jax.Shape...  5.53 us
    ppermute x1, starting transfers between devices, local(): lax.ppermute(gated_rows[row_count - conv_reach:], 'sp', [(i, i + 1) for i...  3.55 us
  transfers between devices with their start and end apart: 36, of which 12 were waited for; matrix products, arithmetic and copies ran while one was open for 3% of the time, Pallas kernels for 16%

profile of v7, /device:TPU:0, one launch (start us, length us, event | category | flops | bytes accessed | tf_op | source)
XLA Modules:
  0.0 122.0 jit_solution(2318286722179045723)
XLA Ops:
  2.4 3.1 %collective-permute-start = (bf16[64,576]{1,0:T(8,128)(2,1)S(1)}, bf16[64,576]{1,0:T(8,128)(2,1)S(1)}, u32[]{:S(2)}, u32[]{:S(2)}) collective-permute-start(bf16[64,576]{1,0:T(8,128)(2,1)S(1)} %fusion.38), channel_id=1, source_target_pairs={{0,8},{2,10},{4,12},{6,14},{8,0},{10,2},{12,4},{14,6},{16,24},{18,... | collective-permute-start | bytes 221192 | tf_op jit(solution)/shard_map/ppermute | solution.py:40
  5.5 2.6 %collective-permute-start.1 = (bf16[64,576]{1,0:T(8,128)(2,1)S(1)}, bf16[64,576]{1,0:T(8,128)(2,1)S(1)}, u32[]{:S(2)}, u32[]{:S(2)}) collective-permute-start(bf16[64,576]{1,0:T(8,128)(2,1)S(1)} %fusion.38), channel_id=1, source_target_pairs={{0,16},{2,18},{4,20},{6,22},{8,24},{10,26},{12,28},{14,30},{16,0},... | collective-permute-start | bytes 221192 | tf_op jit(solution)/shard_map/ppermute | solution.py:40
  10.2 3.6 %collective-permute-start.7 = (bf16[128,512]{1,0:T(8,128)(2,1)S(1)}, bf16[128,512]{1,0:T(8,128)(2,1)S(1)}, u32[]{:S(2)}, u32[]{:S(2)}) collective-permute-start(bf16[128,512]{1,0:T(8,128)(2,1)S(1)} %pad_maximum_fusion.3), channel_id=1, source_target_pairs={{0,16},{2,18},{4,20},{6,22},{8,24},{10,26},{12,28},{14,30},{16,0},... | collective-permute-start | bytes 393224 | tf_op jit(solution)/shard_map/ppermute | solution.py:40
  15.3 1.6 %collective-permute-start.13 = (bf16[4,64,576]{2,1,0:T(8,128)(2,1)S(1)}, bf16[4,64,576]{2,1,0:T(8,128)(2,1)S(1)}, u32[]{:S(2)}, u32[]{:S(2)}) collective-permute-start(bf16[4,64,576]{2,1,0:T(8,128)(2,1)S(1)} %pad_maximum_fusion.1.refs_4_), channel_id=1, source_target_pairs={{0,2},{2,0},{4,6},{6,4},{8,10},{10,8},{12,14},{14,12},{16,18},{18,... | collective-permute-start | bytes 884744 | tf_op jit(solution)/shard_map/ppermute | solution.py:43
  16.8 1.5 %collective-permute-start.14 = (bf16[4,64,576]{2,1,0:T(8,128)(2,1)S(1)}, bf16[4,64,576]{2,1,0:T(8,128)(2,1)S(1)}, u32[]{:S(2)}, u32[]{:S(2)}) collective-permute-start(bf16[4,64,576]{2,1,0:T(8,128)(2,1)S(1)} %pad_maximum_fusion.1.refs_4_), channel_id=1, source_target_pairs={{0,4},{2,6},{4,0},{6,2},{8,12},{10,14},{12,8},{14,10},{16,20},{18,... | collective-permute-start | bytes 884744 | tf_op jit(solution)/shard_map/ppermute | solution.py:43
  18.3 2.4 %all_gather.3 = bf16[128,2048]{1,0:T(8,128)(2,1)S(1)} all-gather(bf16[128,1024]{1,0:T(8,128)(2,1)} %param.14), channel_id=1, replica_groups=mesh['sp'=16,'tp'=2] {'tp'}, dimensions={1}, use_global_device_ids=true | all-gather | bytes 786432 | tf_op jit(solution)/shard_map/all_gather | solution.py:283
  21.2 8.7 %collective-permute-start.4 = (bf16[64,2048]{1,0:T(8,128)(2,1)S(1)}, bf16[64,2048]{1,0:T(8,128)(2,1)S(1)}, u32[]{:S(2)}, u32[]{:S(2)}) collective-permute-start(bf16[64,2048]{1,0:T(8,128)(2,1)S(1)} %constant_dynamic-slice_fusion.9.refs_0_), channel_id=1, source_target_pairs={{0,16},{2,18},{4,20},{6,22},{8,24},{10,26},{12,28},{14,30},{16,0},... | collective-permute-start | bytes 786440 | tf_op jit(solution)/shard_map/ppermute | solution.py:40
  30.6 11.7 %collective-permute-done.4.refs_2_ = bf16[64,2048]{1,0:T(8,128)(2,1)S(1)} collective-permute-done((bf16[64,2048]{1,0:T(8,128)(2,1)S(1)}, bf16[64,2048]{1,0:T(8,128)(2,1)S(1)}, u32[]{:S(2)}, u32[]{:S(2)}) %collective-permute-start.4) | collective-permute-done | bytes 262176 | tf_op jit(solution)/shard_map/ppermute | solution.py:40
  44.1 5.5 %queries.1.q_ref = bf16[8,128,576]{2,1,0:T(8,128)(2,1)} custom-call(bf16[128,2048]{1,0:T(8,128)(2,1)S(1)} %fusion.3.normed_ref, bf16[2048,1536]{1,0:T(8,128)(2,1)} %w_ref.1, bf16[512,1024]{1,0:T(8,128)(2,1)S(1)} %copy-done.1, f32[384,32]{1,0:T(8,128)S(1)} %get-tuple-element.165.cos_ref.refs_13_, f32[384,32]{1,0:T(8,128)S(1)} %get-tuple-element.164.sin_ref.refs_14_), custom_call_target="tpu_custom_call" | custom-call | flops 805306368 | bytes 6291456 | tf_op jit(solution)/shard_map/queries/pallas_call | solution.py:312
  49.6 2.5 %collective-permute-start.22 = (bf16[4,128,512]{2,1,0:T(8,128)(2,1)S(1)}, bf16[4,128,512]{2,1,0:T(8,128)(2,1)S(1)}, u32[]{:S(2)}, u32[]{:S(2)}) collective-permute-start(bf16[4,128,512]{2,1,0:T(8,128)(2,1)S(1)} %pad_maximum_fusion.refs_8_), channel_id=1, source_target_pairs={{0,6},{2,4},{4,2},{6,0},{8,14},{10,12},{12,10},{14,8},{16,22},{18,... | collective-permute-start | bytes 1572872 | tf_op jit(solution)/shard_map/ppermute | solution.py:43
  52.7 4.3 %collective-permute-done.20.refs_9_ = bf16[4,128,512]{2,1,0:T(8,128)(2,1)S(1)} collective-permute-done((bf16[4,128,512]{2,1,0:T(8,128)(2,1)S(1)}, bf16[4,128,512]{2,1,0:T(8,128)(2,1)S(1)}, u32[]{:S(2)}, u32[]{:S(2)}) %collective-permute-start.20) | collective-permute-done | bytes 524320 | tf_op jit(solution)/shard_map/ppermute | solution.py:43
  57.0 10.5 %collective-permute-done.21.refs_10_ = bf16[4,128,512]{2,1,0:T(8,128)(2,1)S(1)} collective-permute-done((bf16[4,128,512]{2,1,0:T(8,128)(2,1)S(1)}, bf16[4,128,512]{2,1,0:T(8,128)(2,1)S(1)}, u32[]{:S(2)}, u32[]{:S(2)}) %collective-permute-start.21) | collective-permute-done | bytes 524320 | tf_op jit(solution)/shard_map/ppermute | solution.py:43
  69.3 2.1 %latents.1.refs_0_ = bf16[256,576]{1,0:T(8,128)(2,1)} custom-call(bf16[64,2048]{1,0:T(8,128)(2,1)S(1)} %constant_dynamic-slice_fusion.9.refs_0_, bf16[64,2048]{1,0:T(8,128)(2,1)S(1)} %collective-permute-done.3.refs_1_, bf16[64,2048]{1,0:T(8,128)(2,1)S(1)} %collective-permute-done.4.refs_2_, bf16[64,2048]{1,0:T(8,128)(2,1)S(1)} %collective-permute-done.5.refs_3_, ...), custom_call_target="tpu_custom_call" | custom-call | flops 603979776 | bytes 3407872 | tf_op jit(solution)/shard_map/latents/pallas_call | solution.py:337
  72.1 1.5 %collective-permute-start.27 = (bf16[256,576]{1,0:T(8,128)(2,1)}, bf16[256,576]{1,0:T(8,128)(2,1)}, u32[]{:S(2)}, u32[]{:S(2)}) collective-permute-start(bf16[256,576]{1,0:T(8,128)(2,1)} %latents.1.refs_0_), channel_id=1, source_target_pairs={{0,2},{2,0},{4,6},{6,4},{8,10},{10,8},{12,14},{14,12},{16,18},{18,... | collective-permute-start | bytes 884744 | tf_op jit(solution)/shard_map/ppermute | solution.py:43
  75.6 1.5 %collective-permute-start.29 = (bf16[256,576]{1,0:T(8,128)(2,1)}, bf16[256,576]{1,0:T(8,128)(2,1)}, u32[]{:S(2)}, u32[]{:S(2)}) collective-permute-start(bf16[256,576]{1,0:T(8,128)(2,1)} %latents.1.refs_0_), channel_id=1, source_target_pairs={{0,6},{2,4},{4,2},{6,0},{8,14},{10,12},{12,10},{14,8},{16,22},{18,... | collective-permute-start | bytes 884744 | tf_op jit(solution)/shard_map/ppermute | solution.py:43
  81.1 2.5 %gated.1 = (bf16[128,256]{1,0:T(8,128)(2,1)S(1)}, bf16[128,256]{1,0:T(8,128)(2,1)S(1)}, bf16[128,256]{1,0:T(8,128)(2,1)S(1)}, bf16[128,256]{1,0:T(8,128)(2,1)S(1)}) custom-call(bf16[64,2048]{1,0:T(8,128)(2,1)S(1)} %constant_dynamic-slice_fusion.9.refs_0_, bf16[64,2048]{1,0:T(8,128)(2,1)S(1)} %collective-permute-done.3.refs_1_, ...), custom_call_target="tpu_custom_call" | custom-call | flops 1073741824 | bytes 4194304 | tf_op jit(solution)/shard_map/gated/pallas_call | solution.py:361
  83.7 4.5 %collective-permute-done.23 = bf16[128,256]{1,0:T(8,128)(2,1)S(1)} collective-permute-done((bf16[128,256]{1,0:T(8,128)(2,1)S(1)}, bf16[128,256]{1,0:T(8,128)(2,1)S(1)}, u32[]{:S(2)}, u32[]{:S(2)}) %collective-permute-start.23) | collective-permute-done | bytes 65568 | tf_op jit(solution)/shard_map/ppermute | solution.py:40
  88.2 3.2 %collective-permute-done.28.refs_2_ = bf16[256,576]{1,0:T(8,128)(2,1)} collective-permute-done((bf16[256,576]{1,0:T(8,128)(2,1)}, bf16[256,576]{1,0:T(8,128)(2,1)}, u32[]{:S(2)}, u32[]{:S(2)}) %collective-permute-start.28) | collective-permute-done | bytes 294944 | tf_op jit(solution)/shard_map/ppermute | solution.py:43
  91.9 2.2 %collective-permute-done.24 = bf16[128,256]{1,0:T(8,128)(2,1)S(1)} collective-permute-done((bf16[128,256]{1,0:T(8,128)(2,1)S(1)}, bf16[128,256]{1,0:T(8,128)(2,1)S(1)}, u32[]{:S(2)}, u32[]{:S(2)}) %collective-permute-start.24) | collective-permute-done | bytes 65568 | tf_op jit(solution)/shard_map/ppermute | solution.py:40
  94.6 5.6 %collective-permute-done.25 = bf16[128,256]{1,0:T(8,128)(2,1)S(1)} collective-permute-done((bf16[128,256]{1,0:T(8,128)(2,1)S(1)}, bf16[128,256]{1,0:T(8,128)(2,1)S(1)}, u32[]{:S(2)}, u32[]{:S(2)}) %collective-permute-start.25) | collective-permute-done | bytes 65568 | tf_op jit(solution)/shard_map/ppermute | solution.py:40
  100.2 3.6 %collective-permute-start.26 = (bf16[30,1024]{1,0:T(8,128)(2,1)S(1)}, bf16[30,1024]{1,0:T(8,128)(2,1)S(1)}, u32[]{:S(2)}, u32[]{:S(2)}) collective-permute-start(bf16[30,1024]{1,0:T(8,128)(2,1)S(1)} %slice.252), channel_id=1, source_target_pairs={{0,2},{2,4},{4,6},{6,8},{8,10},{10,12},{12,14},{14,16},{16,18},{18... | collective-permute-start | bytes 184328 | tf_op jit(solution)/shard_map/ppermute | solution.py:384
  103.9 9.6 %attention.1 = (bf16[128,1024]{1,0:T(8,128)(2,1)S(1)}, f32[8,128]{1,0:T(8,128)}) custom-call(bf16[8,128,576]{2,1,0:T(8,128)(2,1)S(1)} %copy-done, bf16[512,1024]{1,0:T(8,128)(2,1)S(1)} %copy-done.11, bf16[256,576]{1,0:T(8,128)(2,1)} %latents.1.refs_0_, bf16[256,576]{1,0:T(8,128)(2,1)} %collective-permute-done.27.refs_1_, ...), custom_call_target="tpu_custom_call" | custom-call | flops 4563402752 | bytes 2359296 | tf_op jit(solution)/shard_map/attention/pallas_call | solution.py:391
  113.6 2.9 %fusion.42 = (f32[128]{0:T(128)S(1)}, f32[128]{0:T(128)S(1)}, f32[128,1024]{1,0:T(8,128)S(1)}) fusion(f32[158,1024]{1,0:T(8,128)S(1)} %maximum_convert_fusion, f32[1024]{0:T(1024)S(1)} %bitcast.65, f32[1024]{0:T(1024)S(1)} %bitcast.84, f32[1024]{0:T(1024)S(1)} %bitcast.66, f32[1024]{0:T(1024)S(1)} %bitcast.67, f32[1024]{0:T(1024)S(1)} %bitcast.68, ...), kind=kLoop, calls=%fused_computation.144 | loop fusion | flops 8388352 | bytes 16905216 | tf_op jit(solution)/shard_map/reduce_sum | solution.py:420
  119.7 1.5 %collective-permute-done.35 = bf16[64,2048]{1,0:T(8,128)(2,1)S(1)} collective-permute-done((bf16[64,2048]{1,0:T(8,128)(2,1)S(1)}, bf16[64,2048]{1,0:T(8,128)(2,1)S(1)}, u32[]{:S(2)}, u32[]{:S(2)}) %collective-permute-start.35) | collective-permute-done | bytes 262176 | tf_op jit(solution)/shard_map/ppermute | solution.py:47
  (125 shorter events, 22.4 us)
Async XLA Ops:
  2.4 11.5 %collective-permute-start = (bf16[64,576]{1,0:T(8,128)(2,1)S(1)}, bf16[64,576]{1,0:T(8,128)(2,1)S(1)}, u32[]{:S(2)}, u32[]{:S(2)}) collective-permute-start(bf16[64,576]{1,0:T(8,128)(2,1)S(1)} %fusion.38), channel_id=1, source_target_pairs={{0,8},{2,10},{4,12},{6,14},{8,0},{10,2},{12,4},{14,6},{16,24},{18,... | collective-permute-start | bytes 221192 | tf_op jit(solution)/shard_map/ppermute | solution.py:40
  9.2 12.0 %collective-permute-start.6 = (bf16[128,512]{1,0:T(8,128)(2,1)S(1)}, bf16[128,512]{1,0:T(8,128)(2,1)S(1)}, u32[]{:S(2)}, u32[]{:S(2)}) collective-permute-start(bf16[128,512]{1,0:T(8,128)(2,1)S(1)} %pad_maximum_fusion.2), channel_id=1, source_target_pairs={{0,8},{2,10},{4,12},{6,14},{8,0},{10,2},{12,4},{14,6},{16,24},{18,... | collective-permute-start | bytes 393224 | tf_op jit(solution)/shard_map/ppermute | solution.py:40
  10.2 19.7 %collective-permute-start.7 = (bf16[128,512]{1,0:T(8,128)(2,1)S(1)}, bf16[128,512]{1,0:T(8,128)(2,1)S(1)}, u32[]{:S(2)}, u32[]{:S(2)}) collective-permute-start(bf16[128,512]{1,0:T(8,128)(2,1)S(1)} %pad_maximum_fusion.3), channel_id=1, source_target_pairs={{0,16},{2,18},{4,20},{6,22},{8,24},{10,26},{12,28},{14,30},{16,0},... | collective-permute-start | bytes 393224 | tf_op jit(solution)/shard_map/ppermute | solution.py:40
  13.9 16.5 %collective-permute-start.8 = (bf16[128,512]{1,0:T(8,128)(2,1)S(1)}, bf16[128,512]{1,0:T(8,128)(2,1)S(1)}, u32[]{:S(2)}, u32[]{:S(2)}) collective-permute-start(bf16[128,512]{1,0:T(8,128)(2,1)S(1)} %pad_maximum_fusion.4), channel_id=1, source_target_pairs={{0,24},{2,26},{4,28},{6,30},{8,16},{10,18},{12,20},{14,22},{16,8},... | collective-permute-start | bytes 393224 | tf_op jit(solution)/shard_map/ppermute | solution.py:40
  15.3 27.5 %collective-permute-start.13 = (bf16[4,64,576]{2,1,0:T(8,128)(2,1)S(1)}, bf16[4,64,576]{2,1,0:T(8,128)(2,1)S(1)}, u32[]{:S(2)}, u32[]{:S(2)}) collective-permute-start(bf16[4,64,576]{2,1,0:T(8,128)(2,1)S(1)} %pad_maximum_fusion.1.refs_4_), channel_id=1, source_target_pairs={{0,2},{2,0},{4,6},{6,4},{8,10},{10,8},{12,14},{14,12},{16,18},{18,... | collective-permute-start | bytes 884744 | tf_op jit(solution)/shard_map/ppermute | solution.py:43
  16.8 26.5 %collective-permute-start.14 = (bf16[4,64,576]{2,1,0:T(8,128)(2,1)S(1)}, bf16[4,64,576]{2,1,0:T(8,128)(2,1)S(1)}, u32[]{:S(2)}, u32[]{:S(2)}) collective-permute-start(bf16[4,64,576]{2,1,0:T(8,128)(2,1)S(1)} %pad_maximum_fusion.1.refs_4_), channel_id=1, source_target_pairs={{0,4},{2,6},{4,0},{6,2},{8,12},{10,14},{12,8},{14,10},{16,20},{18,... | collective-permute-start | bytes 884744 | tf_op jit(solution)/shard_map/ppermute | solution.py:43
  21.2 21.1 %collective-permute-start.4 = (bf16[64,2048]{1,0:T(8,128)(2,1)S(1)}, bf16[64,2048]{1,0:T(8,128)(2,1)S(1)}, u32[]{:S(2)}, u32[]{:S(2)}) collective-permute-start(bf16[64,2048]{1,0:T(8,128)(2,1)S(1)} %constant_dynamic-slice_fusion.9.refs_0_), channel_id=1, source_target_pairs={{0,16},{2,18},{4,20},{6,22},{8,24},{10,26},{12,28},{14,30},{16,0},... | collective-permute-start | bytes 786440 | tf_op jit(solution)/shard_map/ppermute | solution.py:40
  29.9 19.7 %collective-permute-start.15 = (bf16[4,64,576]{2,1,0:T(8,128)(2,1)S(1)}, bf16[4,64,576]{2,1,0:T(8,128)(2,1)S(1)}, u32[]{:S(2)}, u32[]{:S(2)}) collective-permute-start(bf16[4,64,576]{2,1,0:T(8,128)(2,1)S(1)} %pad_maximum_fusion.1.refs_4_), channel_id=1, source_target_pairs={{0,6},{2,4},{4,2},{6,0},{8,14},{10,12},{12,10},{14,8},{16,22},{18,... | collective-permute-start | bytes 884744 | tf_op jit(solution)/shard_map/ppermute | solution.py:43
  30.5 21.6 %collective-permute-start.3 = (bf16[64,2048]{1,0:T(8,128)(2,1)S(1)}, bf16[64,2048]{1,0:T(8,128)(2,1)S(1)}, u32[]{:S(2)}, u32[]{:S(2)}) collective-permute-start(bf16[64,2048]{1,0:T(8,128)(2,1)S(1)} %constant_dynamic-slice_fusion.9.refs_0_), channel_id=1, source_target_pairs={{0,8},{2,10},{4,12},{6,14},{8,0},{10,2},{12,4},{14,6},{16,24},{18,... | collective-permute-start | bytes 786440 | tf_op jit(solution)/shard_map/ppermute | solution.py:40
  42.2 14.8 %collective-permute-start.20 = (bf16[4,128,512]{2,1,0:T(8,128)(2,1)S(1)}, bf16[4,128,512]{2,1,0:T(8,128)(2,1)S(1)}, u32[]{:S(2)}, u32[]{:S(2)}) collective-permute-start(bf16[4,128,512]{2,1,0:T(8,128)(2,1)S(1)} %pad_maximum_fusion.refs_8_), channel_id=1, source_target_pairs={{0,2},{2,0},{4,6},{6,4},{8,10},{10,8},{12,14},{14,12},{16,18},{18,... | collective-permute-start | bytes 1572872 | tf_op jit(solution)/shard_map/ppermute | solution.py:43
  42.8 24.7 %collective-permute-start.21 = (bf16[4,128,512]{2,1,0:T(8,128)(2,1)S(1)}, bf16[4,128,512]{2,1,0:T(8,128)(2,1)S(1)}, u32[]{:S(2)}, u32[]{:S(2)}) collective-permute-start(bf16[4,128,512]{2,1,0:T(8,128)(2,1)S(1)} %pad_maximum_fusion.refs_8_), channel_id=1, source_target_pairs={{0,4},{2,6},{4,0},{6,2},{8,12},{10,14},{12,8},{14,10},{16,20},{18,... | collective-permute-start | bytes 1572872 | tf_op jit(solution)/shard_map/ppermute | solution.py:43
  43.3 8.9 %collective-permute-start.5 = (bf16[64,2048]{1,0:T(8,128)(2,1)S(1)}, bf16[64,2048]{1,0:T(8,128)(2,1)S(1)}, u32[]{:S(2)}, u32[]{:S(2)}) collective-permute-start(bf16[64,2048]{1,0:T(8,128)(2,1)S(1)} %collective-permute-done.4.refs_2_), channel_id=1, source_target_pairs={{0,8},{2,10},{4,12},{6,14},{8,0},{10,2},{12,4},{14,6},{16,24},{18,... | collective-permute-start | bytes 786440 | tf_op jit(solution)/shard_map/ppermute | solution.py:40
  49.6 21.7 %collective-permute-start.22 = (bf16[4,128,512]{2,1,0:T(8,128)(2,1)S(1)}, bf16[4,128,512]{2,1,0:T(8,128)(2,1)S(1)}, u32[]{:S(2)}, u32[]{:S(2)}) collective-permute-start(bf16[4,128,512]{2,1,0:T(8,128)(2,1)S(1)} %pad_maximum_fusion.refs_8_), channel_id=1, source_target_pairs={{0,6},{2,4},{4,2},{6,0},{8,14},{10,12},{12,10},{14,8},{16,22},{18,... | collective-permute-start | bytes 1572872 | tf_op jit(solution)/shard_map/ppermute | solution.py:43
  52.1 15.4 %collective-permute-start.16 = (bf16[4,64,576]{2,1,0:T(8,128)(2,1)S(1)}, bf16[4,64,576]{2,1,0:T(8,128)(2,1)S(1)}, u32[]{:S(2)}, u32[]{:S(2)}) collective-permute-start(bf16[4,64,576]{2,1,0:T(8,128)(2,1)S(1)} %pad_maximum_fusion.1.refs_4_), channel_id=1, source_target_pairs={{0,1},{1,0},{2,3},{3,2},{4,5},{5,4},{6,7},{7,6},{8,9},{9,8},{10,11... | collective-permute-start | bytes 884744 | tf_op jit(solution)/shard_map/ppermute | solution.py:47
  52.1 16.0 %collective-permute-start.17 = (bf16[4,64,576]{2,1,0:T(8,128)(2,1)S(1)}, bf16[4,64,576]{2,1,0:T(8,128)(2,1)S(1)}, u32[]{:S(2)}, u32[]{:S(2)}) collective-permute-start(bf16[4,64,576]{2,1,0:T(8,128)(2,1)S(1)} %collective-permute-done.13.refs_5_), channel_id=1, source_target_pairs={{0,1},{1,0},{2,3},{3,2},{4,5},{5,4},{6,7},{7,6},{8,9},{9,8},{10,11... | collective-permute-start | bytes 884744 | tf_op jit(solution)/shard_map/ppermute | solution.py:47
  57.0 11.2 %collective-permute-start.18 = (bf16[4,64,576]{2,1,0:T(8,128)(2,1)S(1)}, bf16[4,64,576]{2,1,0:T(8,128)(2,1)S(1)}, u32[]{:S(2)}, u32[]{:S(2)}) collective-permute-start(bf16[4,64,576]{2,1,0:T(8,128)(2,1)S(1)} %collective-permute-done.14.refs_6_), channel_id=1, source_target_pairs={{0,1},{1,0},{2,3},{3,2},{4,5},{5,4},{6,7},{7,6},{8,9},{9,8},{10,11... | collective-permute-start | bytes 884744 | tf_op jit(solution)/shard_map/ppermute | solution.py:47
  72.1 16.0 %collective-permute-start.27 = (bf16[256,576]{1,0:T(8,128)(2,1)}, bf16[256,576]{1,0:T(8,128)(2,1)}, u32[]{:S(2)}, u32[]{:S(2)}) collective-permute-start(bf16[256,576]{1,0:T(8,128)(2,1)} %latents.1.refs_0_), channel_id=1, source_target_pairs={{0,2},{2,0},{4,6},{6,4},{8,10},{10,8},{12,14},{14,12},{16,18},{18,... | collective-permute-start | bytes 884744 | tf_op jit(solution)/shard_map/ppermute | solution.py:43
  74.3 17.0 %collective-permute-start.28 = (bf16[256,576]{1,0:T(8,128)(2,1)}, bf16[256,576]{1,0:T(8,128)(2,1)}, u32[]{:S(2)}, u32[]{:S(2)}) collective-permute-start(bf16[256,576]{1,0:T(8,128)(2,1)} %latents.1.refs_0_), channel_id=1, source_target_pairs={{0,4},{2,6},{4,0},{6,2},{8,12},{10,14},{12,8},{14,10},{16,20},{18,... | collective-permute-start | bytes 884744 | tf_op jit(solution)/shard_map/ppermute | solution.py:43
  75.6 15.8 %collective-permute-start.29 = (bf16[256,576]{1,0:T(8,128)(2,1)}, bf16[256,576]{1,0:T(8,128)(2,1)}, u32[]{:S(2)}, u32[]{:S(2)}) collective-permute-start(bf16[256,576]{1,0:T(8,128)(2,1)} %latents.1.refs_0_), channel_id=1, source_target_pairs={{0,6},{2,4},{4,2},{6,0},{8,14},{10,12},{12,10},{14,8},{16,22},{18,... | collective-permute-start | bytes 884744 | tf_op jit(solution)/shard_map/ppermute | solution.py:43
  77.1 26.7 %collective-permute-start.30 = (bf16[256,576]{1,0:T(8,128)(2,1)}, bf16[256,576]{1,0:T(8,128)(2,1)S(1)}, u32[]{:S(2)}, u32[]{:S(2)}) collective-permute-start(bf16[256,576]{1,0:T(8,128)(2,1)} %latents.1.refs_0_), channel_id=1, source_target_pairs={{0,1},{1,0},{2,3},{3,2},{4,5},{5,4},{6,7},{7,6},{8,9},{9,8},{10,11... | collective-permute-start | bytes 884744 | tf_op jit(solution)/shard_map/ppermute | solution.py:47
  88.2 15.6 %collective-permute-start.31 = (bf16[256,576]{1,0:T(8,128)(2,1)}, bf16[256,576]{1,0:T(8,128)(2,1)S(1)}, u32[]{:S(2)}, u32[]{:S(2)}) collective-permute-start(bf16[256,576]{1,0:T(8,128)(2,1)} %collective-permute-done.27.refs_1_), channel_id=1, source_target_pairs={{0,1},{1,0},{2,3},{3,2},{4,5},{5,4},{6,7},{7,6},{8,9},{9,8},{10,11... | collective-permute-start | bytes 884744 | tf_op jit(solution)/shard_map/ppermute | solution.py:47
  91.4 12.4 %collective-permute-start.32 = (bf16[256,576]{1,0:T(8,128)(2,1)}, bf16[256,576]{1,0:T(8,128)(2,1)S(1)}, u32[]{:S(2)}, u32[]{:S(2)}) collective-permute-start(bf16[256,576]{1,0:T(8,128)(2,1)} %collective-permute-done.28.refs_2_), channel_id=1, source_target_pairs={{0,1},{1,0},{2,3},{3,2},{4,5},{5,4},{6,7},{7,6},{8,9},{9,8},{10,11... | collective-permute-start | bytes 884744 | tf_op jit(solution)/shard_map/ppermute | solution.py:47
  91.4 12.4 %collective-permute-start.33 = (bf16[256,576]{1,0:T(8,128)(2,1)}, bf16[256,576]{1,0:T(8,128)(2,1)S(1)}, u32[]{:S(2)}, u32[]{:S(2)}) collective-permute-start(bf16[256,576]{1,0:T(8,128)(2,1)} %collective-permute-done.29.refs_3_), channel_id=1, source_target_pairs={{0,1},{1,0},{2,3},{3,2},{4,5},{5,4},{6,7},{7,6},{8,9},{9,8},{10,11... | collective-permute-start | bytes 884744 | tf_op jit(solution)/shard_map/ppermute | solution.py:47
  100.2 13.2 %collective-permute-start.26 = (bf16[30,1024]{1,0:T(8,128)(2,1)S(1)}, bf16[30,1024]{1,0:T(8,128)(2,1)S(1)}, u32[]{:S(2)}, u32[]{:S(2)}) collective-permute-start(bf16[30,1024]{1,0:T(8,128)(2,1)S(1)} %slice.252), channel_id=1, source_target_pairs={{0,2},{2,4},{4,6},{6,8},{8,10},{10,12},{12,14},{14,16},{16,18},{18... | collective-permute-start | bytes 184328 | tf_op jit(solution)/shard_map/ppermute | solution.py:384
  (29 other events, 242.5 us)

commit v8 on v7

--- a/solution.py
+++ b/solution.py
@@ -177,16 +177,22 @@
         outs[j][...] = (value * jax.nn.sigmoid(gate)).astype(jnp.bfloat16)
 
 
-def attention_kernel(place, scale, rank, q_ref, up_ref, *refs):
+def attention_kernel(place, scale, rank, q_ref, upper_ref, *refs):
     outer, inner, tp = place.outer, place.inner, place.tp_count
     n_k = tp * inner
     key_refs = refs[:n_k]
-    out_ref, lse_ref, keys = refs[n_k:]
+    out_ref, lse_ref, keys, up_ref, sem = refs[n_k:]
+    up_copy = pltpu.make_async_copy(upper_ref, up_ref, sem.at[n_k])
+    up_copy.start()
     zi, xi, ti = place.indices()
     heads, count, depth = q_ref.shape
     piece = key_refs[0].shape[0]
     share = piece // outer
-    for n in range(n_k):
+    early = n_k // tp
+    copies = copy_all(
+        [(key_refs[n], keys.at[n * piece : (n + 1) * piece]) for n in range(early, n_k)], sem
+    )
+    for n in range(early):
         keys[n * piece : (n + 1) * piece] = key_refs[n][...]
     lane = lax.broadcasted_iota(jnp.int32, (1, piece), 1)
     back = zi ^ lax.shift_right_logical(lane, share.bit_length() - 1)
@@ -206,9 +212,20 @@
     sums = []
     for g in range(heads // together):
         queries = q_ref[g * together : (g + 1) * together].reshape(size, depth)
-        scores = lax.dot_general(
-            queries, keys[...], (((1,), (1,)), ((), ())), preferred_element_type=jnp.float32
-        )
+        scores = []
+        for n in range(tp):
+            if g == 0 and n == 1:
+                for c in copies:
+                    c.wait()
+            scores.append(
+                lax.dot_general(
+                    queries,
+                    keys[n * early * piece : (n + 1) * early * piece],
+                    (((1,), (1,)), ((), ())),
+                    preferred_element_type=jnp.float32,
+                )
+            )
+        scores = jnp.concatenate(scores, axis=1)
         scores = jnp.where(allowed, scores, masked_score)
         top = jnp.max(scores, axis=-1, keepdims=True)
         weights = jnp.exp2((scores - top) * (scale * math.log2(math.e)))
@@ -216,6 +233,8 @@
         weighted = jnp.dot(
             weights.astype(jnp.bfloat16), keys[:, :rank], preferred_element_type=jnp.float32
         )
+        if g == 0:
+            up_copy.wait()
         latent_out = (weighted / total).astype(jnp.bfloat16)
         group_sums = top * scale + jnp.log(total)
         for i in range(together):
@@ -394,10 +413,15 @@
             jax.ShapeDtypeStruct((row_count, head_count * VALUE_HEAD_WIDTH), bf16),
             jax.ShapeDtypeStruct((head_count, row_count), jnp.float32),
         ],
-        in_specs=[whole_vmem()] * (2 + len(latents)),
+        in_specs=[whole_vmem()]
+        + [pl.BlockSpec(memory_space=pl.ANY)]
+        + [whole_vmem()] * inner
+        + [pl.BlockSpec(memory_space=pl.ANY)] * (len(latents) - inner),
         out_specs=[whole_vmem()] * 2,
         scratch_shapes=[
             pltpu.VMEM((key_total, rank + QK_ROPE), bf16),
+            pltpu.VMEM(value_up_weight.shape, bf16),
+            pltpu.SemaphoreType.DMA((len(latents) + 1,)),
         ],
         compiler_params=pltpu.CompilerParams(vmem_limit_bytes=32 << 20),
         cost_estimate=pl.CostEstimate(

time: 122 us -> 123 us (level)
  transfers between devices with their start and end apart: 36 -> 36, of which waited for: 12 -> 12; matrix products, arithmetic and copies ran while one was open for 3% -> 3% of each run, Pallas kernels for 16% -> 17%
where the time goes in v8:
time: 123 us
  waiting for transfers between devices  45.6 us (37%)
  starting transfers between devices  36 us (29%)
  Pallas kernels  20.6 us (17%)
  local copies, waits for them, and re-layouts  9.38 us (8%)
  other arithmetic  6.13 us (5%)
  blocking collectives  2.38 us (2%)
  matrix products  1.6 us (1%)
    ppermute x12, waiting for transfers between devices, outer_swap(): lax.ppermute(block, 'sp', [(i, i ^ mask) for i in range(self.sp_count)])  25.2 us
    ppermute x12, starting transfers between devices, outer_swap(): lax.ppermute(block, 'sp', [(i, i ^ mask) for i in range(self.sp_count)])  19.5 us
    ppermute x9, waiting for transfers between devices, inner_swap(): lax.ppermute(block, 'sp', [(i, i ^ mask) for i in range(self.sp_count)])  18 us
    ppermute x9, starting transfers between devices, inner_swap(): lax.ppermute(block, 'sp', [(i, i ^ mask) for i in range(self.sp_count)])  10.7 us
    pallas_call x1, Pallas kernels, local(): pl.pallas_call(functools.partial(attention_kernel, place, score_scale, ra...  10.5 us
    unnamed x35, local copies, waits for them, and re-layouts  8.06 us
    pallas_call x1, Pallas kernels, local(): pl.pallas_call(functools.partial(query_kernel, rank), out_shape=jax.Shape...  5.53 us
    ppermute x1, starting transfers between devices, local(): lax.ppermute(gated_rows[row_count - conv_reach:], 'sp', [(i, i + 1) for i...  3.55 us
  transfers between devices with their start and end apart: 36, of which 12 were waited for; matrix products, arithmetic and copies ran while one was open for 3% of the time, Pallas kernels for 17%

profile of v8, /device:TPU:0, one launch (start us, length us, event | category | flops | bytes accessed | tf_op | source)
XLA Modules:
  0.0 122.9 jit_solution(472839981822548871)
XLA Ops:
  2.4 3.1 %collective-permute-start = (bf16[64,576]{1,0:T(8,128)(2,1)S(1)}, bf16[64,576]{1,0:T(8,128)(2,1)S(1)}, u32[]{:S(2)}, u32[]{:S(2)}) collective-permute-start(bf16[64,576]{1,0:T(8,128)(2,1)S(1)} %fusion.38), channel_id=1, source_target_pairs={{0,8},{2,10},{4,12},{6,14},{8,0},{10,2},{12,4},{14,6},{16,24},{18,... | collective-permute-start | bytes 221192 | tf_op jit(solution)/shard_map/ppermute | solution.py:40
  5.5 2.6 %collective-permute-start.1 = (bf16[64,576]{1,0:T(8,128)(2,1)S(1)}, bf16[64,576]{1,0:T(8,128)(2,1)S(1)}, u32[]{:S(2)}, u32[]{:S(2)}) collective-permute-start(bf16[64,576]{1,0:T(8,128)(2,1)S(1)} %fusion.38), channel_id=1, source_target_pairs={{0,16},{2,18},{4,20},{6,22},{8,24},{10,26},{12,28},{14,30},{16,0},... | collective-permute-start | bytes 221192 | tf_op jit(solution)/shard_map/ppermute | solution.py:40
  10.2 3.6 %collective-permute-start.7 = (bf16[128,512]{1,0:T(8,128)(2,1)S(1)}, bf16[128,512]{1,0:T(8,128)(2,1)S(1)}, u32[]{:S(2)}, u32[]{:S(2)}) collective-permute-start(bf16[128,512]{1,0:T(8,128)(2,1)S(1)} %pad_maximum_fusion.3), channel_id=1, source_target_pairs={{0,16},{2,18},{4,20},{6,22},{8,24},{10,26},{12,28},{14,30},{16,0},... | collective-permute-start | bytes 393224 | tf_op jit(solution)/shard_map/ppermute | solution.py:40
  15.3 1.6 %collective-permute-start.13 = (bf16[4,64,576]{2,1,0:T(8,128)(2,1)S(1)}, bf16[4,64,576]{2,1,0:T(8,128)(2,1)S(1)}, u32[]{:S(2)}, u32[]{:S(2)}) collective-permute-start(bf16[4,64,576]{2,1,0:T(8,128)(2,1)S(1)} %pad_maximum_fusion.1.refs_4_), channel_id=1, source_target_pairs={{0,2},{2,0},{4,6},{6,4},{8,10},{10,8},{12,14},{14,12},{16,18},{18,... | collective-permute-start | bytes 884744 | tf_op jit(solution)/shard_map/ppermute | solution.py:43
  16.8 1.5 %collective-permute-start.14 = (bf16[4,64,576]{2,1,0:T(8,128)(2,1)S(1)}, bf16[4,64,576]{2,1,0:T(8,128)(2,1)S(1)}, u32[]{:S(2)}, u32[]{:S(2)}) collective-permute-start(bf16[4,64,576]{2,1,0:T(8,128)(2,1)S(1)} %pad_maximum_fusion.1.refs_4_), channel_id=1, source_target_pairs={{0,4},{2,6},{4,0},{6,2},{8,12},{10,14},{12,8},{14,10},{16,20},{18,... | collective-permute-start | bytes 884744 | tf_op jit(solution)/shard_map/ppermute | solution.py:43
  18.3 2.4 %all_gather.3 = bf16[128,2048]{1,0:T(8,128)(2,1)S(1)} all-gather(bf16[128,1024]{1,0:T(8,128)(2,1)} %param.14), channel_id=1, replica_groups=mesh['sp'=16,'tp'=2] {'tp'}, dimensions={1}, use_global_device_ids=true | all-gather | bytes 786432 | tf_op jit(solution)/shard_map/all_gather | solution.py:302
  21.2 8.7 %collective-permute-start.4 = (bf16[64,2048]{1,0:T(8,128)(2,1)S(1)}, bf16[64,2048]{1,0:T(8,128)(2,1)S(1)}, u32[]{:S(2)}, u32[]{:S(2)}) collective-permute-start(bf16[64,2048]{1,0:T(8,128)(2,1)S(1)} %constant_dynamic-slice_fusion.9.refs_0_), channel_id=1, source_target_pairs={{0,16},{2,18},{4,20},{6,22},{8,24},{10,26},{12,28},{14,30},{16,0},... | collective-permute-start | bytes 786440 | tf_op jit(solution)/shard_map/ppermute | solution.py:40
  30.6 11.7 %collective-permute-done.4.refs_2_ = bf16[64,2048]{1,0:T(8,128)(2,1)S(1)} collective-permute-done((bf16[64,2048]{1,0:T(8,128)(2,1)S(1)}, bf16[64,2048]{1,0:T(8,128)(2,1)S(1)}, u32[]{:S(2)}, u32[]{:S(2)}) %collective-permute-start.4) | collective-permute-done | bytes 262176 | tf_op jit(solution)/shard_map/ppermute | solution.py:40
  44.1 5.5 %queries.1.q_ref = bf16[8,128,576]{2,1,0:T(8,128)(2,1)} custom-call(bf16[128,2048]{1,0:T(8,128)(2,1)S(1)} %fusion.3.normed_ref, bf16[2048,1536]{1,0:T(8,128)(2,1)} %w_ref.1, bf16[512,1024]{1,0:T(8,128)(2,1)S(1)} %copy-done.1, f32[384,32]{1,0:T(8,128)S(1)} %get-tuple-element.165.cos_ref.refs_13_, f32[384,32]{1,0:T(8,128)S(1)} %get-tuple-element.164.sin_ref.refs_14_), custom_call_target="tpu_custom_call" | custom-call | flops 805306368 | bytes 6291456 | tf_op jit(solution)/shard_map/queries/pallas_call | solution.py:331
  49.6 2.5 %collective-permute-start.22 = (bf16[4,128,512]{2,1,0:T(8,128)(2,1)S(1)}, bf16[4,128,512]{2,1,0:T(8,128)(2,1)S(1)}, u32[]{:S(2)}, u32[]{:S(2)}) collective-permute-start(bf16[4,128,512]{2,1,0:T(8,128)(2,1)S(1)} %pad_maximum_fusion.refs_8_), channel_id=1, source_target_pairs={{0,6},{2,4},{4,2},{6,0},{8,14},{10,12},{12,10},{14,8},{16,22},{18,... | collective-permute-start | bytes 1572872 | tf_op jit(solution)/shard_map/ppermute | solution.py:43
  52.7 4.3 %collective-permute-done.20.refs_9_ = bf16[4,128,512]{2,1,0:T(8,128)(2,1)S(1)} collective-permute-done((bf16[4,128,512]{2,1,0:T(8,128)(2,1)S(1)}, bf16[4,128,512]{2,1,0:T(8,128)(2,1)S(1)}, u32[]{:S(2)}, u32[]{:S(2)}) %collective-permute-start.20) | collective-permute-done | bytes 524320 | tf_op jit(solution)/shard_map/ppermute | solution.py:43
  57.0 10.5 %collective-permute-done.21.refs_10_ = bf16[4,128,512]{2,1,0:T(8,128)(2,1)S(1)} collective-permute-done((bf16[4,128,512]{2,1,0:T(8,128)(2,1)S(1)}, bf16[4,128,512]{2,1,0:T(8,128)(2,1)S(1)}, u32[]{:S(2)}, u32[]{:S(2)}) %collective-permute-start.21) | collective-permute-done | bytes 524320 | tf_op jit(solution)/shard_map/ppermute | solution.py:43
  69.3 2.1 %latents.1.refs_0_ = bf16[256,576]{1,0:T(8,128)(2,1)} custom-call(bf16[64,2048]{1,0:T(8,128)(2,1)S(1)} %constant_dynamic-slice_fusion.9.refs_0_, bf16[64,2048]{1,0:T(8,128)(2,1)S(1)} %collective-permute-done.3.refs_1_, bf16[64,2048]{1,0:T(8,128)(2,1)S(1)} %collective-permute-done.4.refs_2_, bf16[64,2048]{1,0:T(8,128)(2,1)S(1)} %collective-permute-done.5.refs_3_, ...), custom_call_target="tpu_custom_call" | custom-call | flops 603979776 | bytes 3407872 | tf_op jit(solution)/shard_map/latents/pallas_call | solution.py:356
  72.1 1.5 %collective-permute-start.27 = (bf16[256,576]{1,0:T(8,128)(2,1)}, bf16[256,576]{1,0:T(8,128)(2,1)}, u32[]{:S(2)}, u32[]{:S(2)}) collective-permute-start(bf16[256,576]{1,0:T(8,128)(2,1)} %latents.1.refs_0_), channel_id=1, source_target_pairs={{0,2},{2,0},{4,6},{6,4},{8,10},{10,8},{12,14},{14,12},{16,18},{18,... | collective-permute-start | bytes 884744 | tf_op jit(solution)/shard_map/ppermute | solution.py:43
  75.6 1.5 %collective-permute-start.29 = (bf16[256,576]{1,0:T(8,128)(2,1)}, bf16[256,576]{1,0:T(8,128)(2,1)}, u32[]{:S(2)}, u32[]{:S(2)}) collective-permute-start(bf16[256,576]{1,0:T(8,128)(2,1)} %latents.1.refs_0_), channel_id=1, source_target_pairs={{0,6},{2,4},{4,2},{6,0},{8,14},{10,12},{12,10},{14,8},{16,22},{18,... | collective-permute-start | bytes 884744 | tf_op jit(solution)/shard_map/ppermute | solution.py:43
  81.1 2.5 %gated.1 = (bf16[128,256]{1,0:T(8,128)(2,1)S(1)}, bf16[128,256]{1,0:T(8,128)(2,1)S(1)}, bf16[128,256]{1,0:T(8,128)(2,1)S(1)}, bf16[128,256]{1,0:T(8,128)(2,1)S(1)}) custom-call(bf16[64,2048]{1,0:T(8,128)(2,1)S(1)} %constant_dynamic-slice_fusion.9.refs_0_, bf16[64,2048]{1,0:T(8,128)(2,1)S(1)} %collective-permute-done.3.refs_1_, ...), custom_call_target="tpu_custom_call" | custom-call | flops 1073741824 | bytes 4194304 | tf_op jit(solution)/shard_map/gated/pallas_call | solution.py:380
  83.7 4.5 %collective-permute-done.23 = bf16[128,256]{1,0:T(8,128)(2,1)S(1)} collective-permute-done((bf16[128,256]{1,0:T(8,128)(2,1)S(1)}, bf16[128,256]{1,0:T(8,128)(2,1)S(1)}, u32[]{:S(2)}, u32[]{:S(2)}) %collective-permute-start.23) | collective-permute-done | bytes 65568 | tf_op jit(solution)/shard_map/ppermute | solution.py:40
  88.2 3.2 %collective-permute-done.28.refs_2_ = bf16[256,576]{1,0:T(8,128)(2,1)} collective-permute-done((bf16[256,576]{1,0:T(8,128)(2,1)}, bf16[256,576]{1,0:T(8,128)(2,1)}, u32[]{:S(2)}, u32[]{:S(2)}) %collective-permute-start.28) | collective-permute-done | bytes 294944 | tf_op jit(solution)/shard_map/ppermute | solution.py:43
  91.9 2.2 %collective-permute-done.24 = bf16[128,256]{1,0:T(8,128)(2,1)S(1)} collective-permute-done((bf16[128,256]{1,0:T(8,128)(2,1)S(1)}, bf16[128,256]{1,0:T(8,128)(2,1)S(1)}, u32[]{:S(2)}, u32[]{:S(2)}) %collective-permute-start.24) | collective-permute-done | bytes 65568 | tf_op jit(solution)/shard_map/ppermute | solution.py:40
  94.6 5.6 %collective-permute-done.25 = bf16[128,256]{1,0:T(8,128)(2,1)S(1)} collective-permute-done((bf16[128,256]{1,0:T(8,128)(2,1)S(1)}, bf16[128,256]{1,0:T(8,128)(2,1)S(1)}, u32[]{:S(2)}, u32[]{:S(2)}) %collective-permute-start.25) | collective-permute-done | bytes 65568 | tf_op jit(solution)/shard_map/ppermute | solution.py:40
  100.2 3.6 %collective-permute-start.26 = (bf16[30,1024]{1,0:T(8,128)(2,1)S(1)}, bf16[30,1024]{1,0:T(8,128)(2,1)S(1)}, u32[]{:S(2)}, u32[]{:S(2)}) collective-permute-start(bf16[30,1024]{1,0:T(8,128)(2,1)S(1)} %slice.252), channel_id=1, source_target_pairs={{0,2},{2,4},{4,6},{6,8},{8,10},{10,12},{12,14},{14,16},{16,18},{18... | collective-permute-start | bytes 184328 | tf_op jit(solution)/shard_map/ppermute | solution.py:403
  103.9 10.5 %attention.1 = (bf16[128,1024]{1,0:T(8,128)(2,1)S(1)}, f32[8,128]{1,0:T(8,128)}) custom-call(bf16[8,128,576]{2,1,0:T(8,128)(2,1)S(1)} %copy-done, bf16[512,1024]{1,0:T(8,128)(2,1)S(1)} %copy-done.11, bf16[256,576]{1,0:T(8,128)(2,1)} %latents.1.refs_0_, bf16[256,576]{1,0:T(8,128)(2,1)} %collective-permute-done.27.refs_1_, ...), custom_call_target="tpu_custom_call" | custom-call | flops 4563402752 | bytes 2359296 | tf_op jit(solution)/shard_map/attention/pallas_call | solution.py:410
  114.5 2.9 %fusion.42 = (f32[128]{0:T(128)S(1)}, f32[128]{0:T(128)S(1)}, f32[128,1024]{1,0:T(8,128)S(1)}) fusion(f32[158,1024]{1,0:T(8,128)S(1)} %maximum_convert_fusion, f32[1024]{0:T(1024)S(1)} %bitcast.65, f32[1024]{0:T(1024)S(1)} %bitcast.84, f32[1024]{0:T(1024)S(1)} %bitcast.66, f32[1024]{0:T(1024)S(1)} %bitcast.67, f32[1024]{0:T(1024)S(1)} %bitcast.68, ...), kind=kLoop, calls=%fused_computation.144 | loop fusion | flops 8388352 | bytes 16905216 | tf_op jit(solution)/shard_map/reduce_sum | solution.py:444
  120.6 1.5 %collective-permute-done.35 = bf16[64,2048]{1,0:T(8,128)(2,1)S(1)} collective-permute-done((bf16[64,2048]{1,0:T(8,128)(2,1)S(1)}, bf16[64,2048]{1,0:T(8,128)(2,1)S(1)}, u32[]{:S(2)}, u32[]{:S(2)}) %collective-permute-start.35) | collective-permute-done | bytes 262176 | tf_op jit(solution)/shard_map/ppermute | solution.py:47
  (125 shorter events, 22.4 us)
Async XLA Ops:
  2.4 11.5 %collective-permute-start = (bf16[64,576]{1,0:T(8,128)(2,1)S(1)}, bf16[64,576]{1,0:T(8,128)(2,1)S(1)}, u32[]{:S(2)}, u32[]{:S(2)}) collective-permute-start(bf16[64,576]{1,0:T(8,128)(2,1)S(1)} %fusion.38), channel_id=1, source_target_pairs={{0,8},{2,10},{4,12},{6,14},{8,0},{10,2},{12,4},{14,6},{16,24},{18,... | collective-permute-start | bytes 221192 | tf_op jit(solution)/shard_map/ppermute | solution.py:40
  9.2 12.0 %collective-permute-start.6 = (bf16[128,512]{1,0:T(8,128)(2,1)S(1)}, bf16[128,512]{1,0:T(8,128)(2,1)S(1)}, u32[]{:S(2)}, u32[]{:S(2)}) collective-permute-start(bf16[128,512]{1,0:T(8,128)(2,1)S(1)} %pad_maximum_fusion.2), channel_id=1, source_target_pairs={{0,8},{2,10},{4,12},{6,14},{8,0},{10,2},{12,4},{14,6},{16,24},{18,... | collective-permute-start | bytes 393224 | tf_op jit(solution)/shard_map/ppermute | solution.py:40
  10.2 19.7 %collective-permute-start.7 = (bf16[128,512]{1,0:T(8,128)(2,1)S(1)}, bf16[128,512]{1,0:T(8,128)(2,1)S(1)}, u32[]{:S(2)}, u32[]{:S(2)}) collective-permute-start(bf16[128,512]{1,0:T(8,128)(2,1)S(1)} %pad_maximum_fusion.3), channel_id=1, source_target_pairs={{0,16},{2,18},{4,20},{6,22},{8,24},{10,26},{12,28},{14,30},{16,0},... | collective-permute-start | bytes 393224 | tf_op jit(solution)/shard_map/ppermute | solution.py:40
  13.9 16.5 %collective-permute-start.8 = (bf16[128,512]{1,0:T(8,128)(2,1)S(1)}, bf16[128,512]{1,0:T(8,128)(2,1)S(1)}, u32[]{:S(2)}, u32[]{:S(2)}) collective-permute-start(bf16[128,512]{1,0:T(8,128)(2,1)S(1)} %pad_maximum_fusion.4), channel_id=1, source_target_pairs={{0,24},{2,26},{4,28},{6,30},{8,16},{10,18},{12,20},{14,22},{16,8},... | collective-permute-start | bytes 393224 | tf_op jit(solution)/shard_map/ppermute | solution.py:40
  15.3 27.5 %collective-permute-start.13 = (bf16[4,64,576]{2,1,0:T(8,128)(2,1)S(1)}, bf16[4,64,576]{2,1,0:T(8,128)(2,1)S(1)}, u32[]{:S(2)}, u32[]{:S(2)}) collective-permute-start(bf16[4,64,576]{2,1,0:T(8,128)(2,1)S(1)} %pad_maximum_fusion.1.refs_4_), channel_id=1, source_target_pairs={{0,2},{2,0},{4,6},{6,4},{8,10},{10,8},{12,14},{14,12},{16,18},{18,... | collective-permute-start | bytes 884744 | tf_op jit(solution)/shard_map/ppermute | solution.py:43
  16.8 26.5 %collective-permute-start.14 = (bf16[4,64,576]{2,1,0:T(8,128)(2,1)S(1)}, bf16[4,64,576]{2,1,0:T(8,128)(2,1)S(1)}, u32[]{:S(2)}, u32[]{:S(2)}) collective-permute-start(bf16[4,64,576]{2,1,0:T(8,128)(2,1)S(1)} %pad_maximum_fusion.1.refs_4_), channel_id=1, source_target_pairs={{0,4},{2,6},{4,0},{6,2},{8,12},{10,14},{12,8},{14,10},{16,20},{18,... | collective-permute-start | bytes 884744 | tf_op jit(solution)/shard_map/ppermute | solution.py:43
  21.2 21.1 %collective-permute-start.4 = (bf16[64,2048]{1,0:T(8,128)(2,1)S(1)}, bf16[64,2048]{1,0:T(8,128)(2,1)S(1)}, u32[]{:S(2)}, u32[]{:S(2)}) collective-permute-start(bf16[64,2048]{1,0:T(8,128)(2,1)S(1)} %constant_dynamic-slice_fusion.9.refs_0_), channel_id=1, source_target_pairs={{0,16},{2,18},{4,20},{6,22},{8,24},{10,26},{12,28},{14,30},{16,0},... | collective-permute-start | bytes 786440 | tf_op jit(solution)/shard_map/ppermute | solution.py:40
  29.9 19.7 %collective-permute-start.15 = (bf16[4,64,576]{2,1,0:T(8,128)(2,1)S(1)}, bf16[4,64,576]{2,1,0:T(8,128)(2,1)S(1)}, u32[]{:S(2)}, u32[]{:S(2)}) collective-permute-start(bf16[4,64,576]{2,1,0:T(8,128)(2,1)S(1)} %pad_maximum_fusion.1.refs_4_), channel_id=1, source_target_pairs={{0,6},{2,4},{4,2},{6,0},{8,14},{10,12},{12,10},{14,8},{16,22},{18,... | collective-permute-start | bytes 884744 | tf_op jit(solution)/shard_map/ppermute | solution.py:43
  30.5 21.6 %collective-permute-start.3 = (bf16[64,2048]{1,0:T(8,128)(2,1)S(1)}, bf16[64,2048]{1,0:T(8,128)(2,1)S(1)}, u32[]{:S(2)}, u32[]{:S(2)}) collective-permute-start(bf16[64,2048]{1,0:T(8,128)(2,1)S(1)} %constant_dynamic-slice_fusion.9.refs_0_), channel_id=1, source_target_pairs={{0,8},{2,10},{4,12},{6,14},{8,0},{10,2},{12,4},{14,6},{16,24},{18,... | collective-permute-start | bytes 786440 | tf_op jit(solution)/shard_map/ppermute | solution.py:40
  42.2 14.8 %collective-permute-start.20 = (bf16[4,128,512]{2,1,0:T(8,128)(2,1)S(1)}, bf16[4,128,512]{2,1,0:T(8,128)(2,1)S(1)}, u32[]{:S(2)}, u32[]{:S(2)}) collective-permute-start(bf16[4,128,512]{2,1,0:T(8,128)(2,1)S(1)} %pad_maximum_fusion.refs_8_), channel_id=1, source_target_pairs={{0,2},{2,0},{4,6},{6,4},{8,10},{10,8},{12,14},{14,12},{16,18},{18,... | collective-permute-start | bytes 1572872 | tf_op jit(solution)/shard_map/ppermute | solution.py:43
  42.8 24.7 %collective-permute-start.21 = (bf16[4,128,512]{2,1,0:T(8,128)(2,1)S(1)}, bf16[4,128,512]{2,1,0:T(8,128)(2,1)S(1)}, u32[]{:S(2)}, u32[]{:S(2)}) collective-permute-start(bf16[4,128,512]{2,1,0:T(8,128)(2,1)S(1)} %pad_maximum_fusion.refs_8_), channel_id=1, source_target_pairs={{0,4},{2,6},{4,0},{6,2},{8,12},{10,14},{12,8},{14,10},{16,20},{18,... | collective-permute-start | bytes 1572872 | tf_op jit(solution)/shard_map/ppermute | solution.py:43
  43.3 8.9 %collective-permute-start.5 = (bf16[64,2048]{1,0:T(8,128)(2,1)S(1)}, bf16[64,2048]{1,0:T(8,128)(2,1)S(1)}, u32[]{:S(2)}, u32[]{:S(2)}) collective-permute-start(bf16[64,2048]{1,0:T(8,128)(2,1)S(1)} %collective-permute-done.4.refs_2_), channel_id=1, source_target_pairs={{0,8},{2,10},{4,12},{6,14},{8,0},{10,2},{12,4},{14,6},{16,24},{18,... | collective-permute-start | bytes 786440 | tf_op jit(solution)/shard_map/ppermute | solution.py:40
  49.6 21.7 %collective-permute-start.22 = (bf16[4,128,512]{2,1,0:T(8,128)(2,1)S(1)}, bf16[4,128,512]{2,1,0:T(8,128)(2,1)S(1)}, u32[]{:S(2)}, u32[]{:S(2)}) collective-permute-start(bf16[4,128,512]{2,1,0:T(8,128)(2,1)S(1)} %pad_maximum_fusion.refs_8_), channel_id=1, source_target_pairs={{0,6},{2,4},{4,2},{6,0},{8,14},{10,12},{12,10},{14,8},{16,22},{18,... | collective-permute-start | bytes 1572872 | tf_op jit(solution)/shard_map/ppermute | solution.py:43
  52.1 15.4 %collective-permute-start.16 = (bf16[4,64,576]{2,1,0:T(8,128)(2,1)S(1)}, bf16[4,64,576]{2,1,0:T(8,128)(2,1)S(1)}, u32[]{:S(2)}, u32[]{:S(2)}) collective-permute-start(bf16[4,64,576]{2,1,0:T(8,128)(2,1)S(1)} %pad_maximum_fusion.1.refs_4_), channel_id=1, source_target_pairs={{0,1},{1,0},{2,3},{3,2},{4,5},{5,4},{6,7},{7,6},{8,9},{9,8},{10,11... | collective-permute-start | bytes 884744 | tf_op jit(solution)/shard_map/ppermute | solution.py:47
  52.1 16.0 %collective-permute-start.17 = (bf16[4,64,576]{2,1,0:T(8,128)(2,1)S(1)}, bf16[4,64,576]{2,1,0:T(8,128)(2,1)S(1)}, u32[]{:S(2)}, u32[]{:S(2)}) collective-permute-start(bf16[4,64,576]{2,1,0:T(8,128)(2,1)S(1)} %collective-permute-done.13.refs_5_), channel_id=1, source_target_pairs={{0,1},{1,0},{2,3},{3,2},{4,5},{5,4},{6,7},{7,6},{8,9},{9,8},{10,11... | collective-permute-start | bytes 884744 | tf_op jit(solution)/shard_map/ppermute | solution.py:47
  57.0 11.2 %collective-permute-start.18 = (bf16[4,64,576]{2,1,0:T(8,128)(2,1)S(1)}, bf16[4,64,576]{2,1,0:T(8,128)(2,1)S(1)}, u32[]{:S(2)}, u32[]{:S(2)}) collective-permute-start(bf16[4,64,576]{2,1,0:T(8,128)(2,1)S(1)} %collective-permute-done.14.refs_6_), channel_id=1, source_target_pairs={{0,1},{1,0},{2,3},{3,2},{4,5},{5,4},{6,7},{7,6},{8,9},{9,8},{10,11... | collective-permute-start | bytes 884744 | tf_op jit(solution)/shard_map/ppermute | solution.py:47
  72.1 16.0 %collective-permute-start.27 = (bf16[256,576]{1,0:T(8,128)(2,1)}, bf16[256,576]{1,0:T(8,128)(2,1)}, u32[]{:S(2)}, u32[]{:S(2)}) collective-permute-start(bf16[256,576]{1,0:T(8,128)(2,1)} %latents.1.refs_0_), channel_id=1, source_target_pairs={{0,2},{2,0},{4,6},{6,4},{8,10},{10,8},{12,14},{14,12},{16,18},{18,... | collective-permute-start | bytes 884744 | tf_op jit(solution)/shard_map/ppermute | solution.py:43
  74.3 17.0 %collective-permute-start.28 = (bf16[256,576]{1,0:T(8,128)(2,1)}, bf16[256,576]{1,0:T(8,128)(2,1)}, u32[]{:S(2)}, u32[]{:S(2)}) collective-permute-start(bf16[256,576]{1,0:T(8,128)(2,1)} %latents.1.refs_0_), channel_id=1, source_target_pairs={{0,4},{2,6},{4,0},{6,2},{8,12},{10,14},{12,8},{14,10},{16,20},{18,... | collective-permute-start | bytes 884744 | tf_op jit(solution)/shard_map/ppermute | solution.py:43
  75.6 15.8 %collective-permute-start.29 = (bf16[256,576]{1,0:T(8,128)(2,1)}, bf16[256,576]{1,0:T(8,128)(2,1)}, u32[]{:S(2)}, u32[]{:S(2)}) collective-permute-start(bf16[256,576]{1,0:T(8,128)(2,1)} %latents.1.refs_0_), channel_id=1, source_target_pairs={{0,6},{2,4},{4,2},{6,0},{8,14},{10,12},{12,10},{14,8},{16,22},{18,... | collective-permute-start | bytes 884744 | tf_op jit(solution)/shard_map/ppermute | solution.py:43
  77.1 26.7 %collective-permute-start.30 = (bf16[256,576]{1,0:T(8,128)(2,1)}, bf16[256,576]{1,0:T(8,128)(2,1)S(1)}, u32[]{:S(2)}, u32[]{:S(2)}) collective-permute-start(bf16[256,576]{1,0:T(8,128)(2,1)} %latents.1.refs_0_), channel_id=1, source_target_pairs={{0,1},{1,0},{2,3},{3,2},{4,5},{5,4},{6,7},{7,6},{8,9},{9,8},{10,11... | collective-permute-start | bytes 884744 | tf_op jit(solution)/shard_map/ppermute | solution.py:47
  88.2 15.6 %collective-permute-start.31 = (bf16[256,576]{1,0:T(8,128)(2,1)}, bf16[256,576]{1,0:T(8,128)(2,1)S(1)}, u32[]{:S(2)}, u32[]{:S(2)}) collective-permute-start(bf16[256,576]{1,0:T(8,128)(2,1)} %collective-permute-done.27.refs_1_), channel_id=1, source_target_pairs={{0,1},{1,0},{2,3},{3,2},{4,5},{5,4},{6,7},{7,6},{8,9},{9,8},{10,11... | collective-permute-start | bytes 884744 | tf_op jit(solution)/shard_map/ppermute | solution.py:47
  91.4 12.4 %collective-permute-start.32 = (bf16[256,576]{1,0:T(8,128)(2,1)}, bf16[256,576]{1,0:T(8,128)(2,1)S(1)}, u32[]{:S(2)}, u32[]{:S(2)}) collective-permute-start(bf16[256,576]{1,0:T(8,128)(2,1)} %collective-permute-done.28.refs_2_), channel_id=1, source_target_pairs={{0,1},{1,0},{2,3},{3,2},{4,5},{5,4},{6,7},{7,6},{8,9},{9,8},{10,11... | collective-permute-start | bytes 884744 | tf_op jit(solution)/shard_map/ppermute | solution.py:47
  91.4 12.4 %collective-permute-start.33 = (bf16[256,576]{1,0:T(8,128)(2,1)}, bf16[256,576]{1,0:T(8,128)(2,1)S(1)}, u32[]{:S(2)}, u32[]{:S(2)}) collective-permute-start(bf16[256,576]{1,0:T(8,128)(2,1)} %collective-permute-done.29.refs_3_), channel_id=1, source_target_pairs={{0,1},{1,0},{2,3},{3,2},{4,5},{5,4},{6,7},{7,6},{8,9},{9,8},{10,11... | collective-permute-start | bytes 884744 | tf_op jit(solution)/shard_map/ppermute | solution.py:47
  100.2 14.2 %collective-permute-start.26 = (bf16[30,1024]{1,0:T(8,128)(2,1)S(1)}, bf16[30,1024]{1,0:T(8,128)(2,1)S(1)}, u32[]{:S(2)}, u32[]{:S(2)}) collective-permute-start(bf16[30,1024]{1,0:T(8,128)(2,1)S(1)} %slice.252), channel_id=1, source_target_pairs={{0,2},{2,4},{4,6},{6,8},{8,10},{10,12},{12,14},{14,16},{16,18},{18... | collective-permute-start | bytes 184328 | tf_op jit(solution)/shard_map/ppermute | solution.py:403
  (29 other events, 242.5 us)
